TPU v7x, 32 devices: a whole 2x2x4 slice. The times are simulated.
32 devices in a mesh: ep: 8 (over z, y), tp: 4 (over x, core).
Axes of the slice: x: 2, y: 2, z: 4, core: 2. Of those that a mesh axis runs over, the one named last changes fastest.
Arguments:
- tokens: bfloat16 [1024, 2048], P('ep'), may hold values from -6 to 6
- norm_gain: bfloat16 [2048], replicated, may hold values from 0.099609375 to 1.8984375
- expert_ids: int32 [1024, 2], P('ep'), may hold values from 0 to 7, all different within a row; in each aligned block of 128 rows (0 to 127, 128 to 255, ...) at most 48 rows name the same one
- route_weights: float32 [1024, 2], P('ep'), may hold values from 0.2 to 1.5
- gate_weight: bfloat16 [8, 2048, 512], P('ep', None, 'tp'), may hold values from -0.125 to 0.125
- up_weight: bfloat16 [8, 2048, 512], P('ep', None, 'tp'), may hold values from -0.125 to 0.125
- down_weight: bfloat16 [8, 512, 2048], P('ep', 'tp'), may hold values from -0.25 to 0.25
- shared_gate: bfloat16 [2048, 512], P(None, 'tp'), may hold values from -0.125 to 0.125
- shared_up: bfloat16 [2048, 512], P(None, 'tp'), may hold values from -0.125 to 0.125
- shared_down: bfloat16 [512, 2048], P('tp'), may hold values from -0.25 to 0.25
Outputs:
- mixed: bfloat16 [1024, 2048], P('ep', 'tp')
Inputs may be any that keep to these rules, and one draw needn't show every extreme that they name: `expert_ids`: each row names 2 different experts. Among the rows of one index of ep (aligned blocks of 128 rows) no expert is named more than 48 times, a bound that some block reaches.
All inputs are finite; a program needn't handle non-finite values.
Results may differ from a plain program's by a relative error of at most 0.012.
Values may be sent and summed in bfloat16 or wider, within the bound.
No kernel may reach another device: no remote copies, remote signals or barrier semaphores. Data moves between devices by JAX's collectives and lax.ppermute only.
A program may use at most 64 MiB of HBM per device.

v0:
```python
import functools

import jax
import jax.numpy as jnp
from jax import lax
from jax.experimental import pallas as pl
from jax.experimental.pallas import tpu as pltpu
from jax.sharding import PartitionSpec as P

norm_eps = 1e-06
grant = 16 * 1024 * 1024
f32 = jnp.float32
bf16 = jnp.bfloat16

vmem = pl.BlockSpec(memory_space=pltpu.VMEM)


def call(body, outs, ins, flops, scratch=()):
    moved = sum(a.size * a.dtype.itemsize for a in ins)
    moved += sum(o.size * o.dtype.itemsize for o in outs)
    return pl.pallas_call(
        body,
        out_shape=outs,
        in_specs=[vmem] * len(ins),
        out_specs=[vmem] * len(outs),
        scratch_shapes=list(scratch),
        compiler_params=pltpu.CompilerParams(vmem_limit_bytes=grant),
        cost_estimate=pl.CostEstimate(flops=flops, bytes_accessed=moved, transcendentals=0),
    )(*ins)


def shape(rows, columns, dtype):
    return jax.ShapeDtypeStruct((rows, columns), dtype)


def route_body(half, experts, relabel, ids, gain, tokens, *outs):
    normed_out, slots_out = outs[0], outs[1]
    rows, width = tokens.shape
    values = tokens[...].astype(f32)
    scale = lax.rsqrt(jnp.mean(values * values, axis=-1, keepdims=True) + norm_eps)
    lanes = gain.shape[1]
    for c in range(width // lanes):
        at = slice(c * lanes, (c + 1) * lanes)
        normed_out[:, at] = (values[:, at] * scale * gain[c : c + 1].astype(f32)).astype(bf16)
    mixed = lax.axis_index("ep") if relabel else 0
    first = (lax.axis_index("tp") % 2) * half
    kinds = max(8, experts)
    kind = lax.broadcasted_iota(jnp.int32, (kinds, rows), 0)
    before = (
        lax.broadcasted_iota(jnp.int32, (rows, rows), 0)
        < lax.broadcasted_iota(jnp.int32, (rows, rows), 1)
    ).astype(bf16)
    base = jnp.zeros((kinds, 1), f32)
    total = sum(out.shape[0] for out in outs[2:])
    slot = lax.broadcasted_iota(jnp.int32, (total, rows), 0)
    hit = jnp.zeros((total, rows), f32)
    for j in range(ids.shape[0]):
        expert = ids[j : j + 1, :] ^ mixed
        onehot = (kind == expert).astype(f32)
        earlier = jnp.dot(onehot.astype(bf16), before, preferred_element_type=f32) + base
        rank = jnp.sum(earlier * onehot, axis=0, keepdims=True).astype(jnp.int32) - first
        base = base + jnp.sum(onehot, axis=1, keepdims=True)
        held = jnp.logical_and(rank >= 0, rank < half)
        where = jnp.where(held, expert * half + rank, -1)
        slots_out[j : j + 1, :] = where
        hit = jnp.where(slot == where, 1.0, hit)
    pick = hit.astype(bf16)
    normed = normed_out[...]
    at = 0
    for out in outs[2:]:
        n = out.shape[0]
        out[...] = jnp.dot(pick[at : at + n], normed, preferred_element_type=f32).astype(bf16)
        at += n


def product_body(blocks, sets, *refs):
    rows_in, weights = refs[:blocks], refs[blocks : blocks + 3 * sets]
    send, keep = refs[blocks + 3 * sets : blocks + 3 * sets + 2]
    if blocks > 1:
        gathered = refs[-1]
        at = 0
        for ref in rows_in:
            gathered[at : at + ref.shape[0]] = ref[...]
            at += ref.shape[0]
    else:
        gathered = rows_in[0]
    side = lax.axis_index("tp") // 2
    into = [w[...] for w in weights[::3]] + [w[...] for w in weights[1::3]]
    both = jnp.dot(gathered[...], jnp.concatenate(into, axis=1), preferred_element_type=f32)
    units = both.shape[1] // 2
    gate, up = both[:, :units], both[:, units:]
    hidden = (gate / (1.0 + jnp.exp(-gate)) * up).astype(bf16)
    width = keep.shape[1]
    for out, place in ((send, 1 - side), (keep, side)):
        columns = pl.ds(pl.multiple_of(place * width, width), width)
        down = jnp.concatenate([w[:, columns] for w in weights[2::3]], axis=0)
        out[...] = jnp.dot(hidden, down, preferred_element_type=f32).astype(out.dtype)


def products(rows, weights, width):
    n = sum(r.shape[0] for r in rows)
    full = rows[0].shape[1]
    hidden = sum(w.shape[1] for w in weights[::3])
    scratch = [pltpu.VMEM((n, full), bf16)] if len(rows) > 1 else []
    return call(
        functools.partial(product_body, len(rows), len(weights) // 3),
        [shape(n, width, bf16), shape(n, width, f32)],
        [*rows, *weights],
        6 * n * full * hidden,
        scratch,
    )


def add_body(keep, came, *outs):
    at = 0
    for out in outs:
        n = out.shape[0]
        out[...] = (keep[at : at + n] + came[at : at + n].astype(f32)).astype(out.dtype)
        at += n


def mix_body(blocks, slots, gains, *refs):
    rows_in, adds, outs = refs[:blocks], refs[blocks:-3], refs[-3:-1]
    gathered = refs[-1]
    at = 0
    for ref in rows_in:
        gathered[at : at + ref.shape[0]] = ref[...]
        at += ref.shape[0]
    tokens = slots.shape[1]
    slot = lax.broadcasted_iota(jnp.int32, (at, tokens), 0)
    weight = jnp.zeros((at, tokens), f32)
    for j in range(slots.shape[0]):
        weight = jnp.where(slot == slots[j : j + 1, :], gains[j : j + 1, :], weight)
    weight = weight.T
    high = weight.astype(bf16)
    low = (weight - high.astype(f32)).astype(bf16)
    width = outs[0].shape[1]
    core = lax.axis_index("tp") % 2
    for out, place in ((outs[0], core), (outs[1], 1 - core)):
        columns = pl.ds(pl.multiple_of(place * width, width), width)
        rows = gathered[:, columns]
        total = sum(a[:, columns].astype(f32) for a in adds)
        total += jnp.dot(high, rows, preferred_element_type=f32)
        out[...] = total + jnp.dot(low, rows, preferred_element_type=f32)


def local(
    tokens,
    norm_gain,
    expert_ids,
    route_weights,
    gate_weight,
    up_weight,
    down_weight,
    shared_gate,
    shared_up,
    shared_down,
):
    rows_here, width = tokens.shape
    chosen = expert_ids.shape[1]
    groups = lax.axis_size("ep")
    cuts = lax.axis_size("tp")
    local_experts = gate_weight.shape[0]
    assert local_experts == 1 and cuts == 4
    capacity = (3 * rows_here * chosen + 2 * groups - 1) // (2 * groups)
    half = -(-capacity // 2)
    wide, share = width // 2, width // 4
    direct = groups == 8
    sibling = [(i, i ^ 1) for i in range(cuts)]
    neighbour = [(i, i ^ 2) for i in range(cuts)]
    own = (gate_weight[0], up_weight[0], down_weight[0])
    other = tuple(lax.ppermute(w, "tp", sibling) for w in own)

    sizes = [half] * groups if direct else [half * groups]
    normed, slots, *sends = call(
        functools.partial(route_body, half, groups, direct),
        [shape(rows_here, width, bf16), shape(chosen, rows_here, jnp.int32)]
        + [shape(n, width, bf16) for n in sizes],
        [expert_ids.T, norm_gain.reshape(-1, 128), tokens],
        2 * rows_here * width * sum(sizes),
    )

    def exchange(k, block):
        if not direct:
            return lax.all_to_all(block, "ep", split_axis=0, concat_axis=0, tiled=True)
        if k == 0:
            return block
        return lax.ppermute(block, "ep", [(i, i ^ k) for i in range(groups)])

    parties = {"A": [4, 5], "N": [0, 1, 2, 3], "B": [6, 7]} if direct else {"A": [0]}
    arrived = [exchange(k, sends[k]) for k in range(len(sizes))]
    sh_send, sh_keep = products([normed], [shared_gate, shared_up, shared_down], wide)
    sh_came = lax.ppermute(sh_send, "tp", neighbour)

    returned = [None] * len(sizes)
    for names in parties.values():
        send, keep = products([arrived[k] for k in names], [*own, *other], wide)
        came = lax.ppermute(send, "tp", neighbour)
        outs = call(add_body, [shape(sizes[k], wide, bf16) for k in names], [keep, came], keep.size)
        for k, out in zip(names, outs):
            returned[k] = exchange(k, out)

    kept, sent = call(
        functools.partial(mix_body, len(returned)),
        [shape(rows_here, share, f32), shape(rows_here, share, f32)],
        [slots, route_weights.T, *returned, sh_keep, sh_came],
        4 * rows_here * wide * half * groups,
        [pltpu.VMEM((half * groups, wide), bf16)],
    )
    came = lax.ppermute(sent, "tp", sibling)
    (mixed,) = call(add_body, [shape(rows_here, share, bf16)], [kept, came], kept.size)
    return mixed


def solution(mesh):
    in_specs = (
        P("ep", None),
        P(),
        P("ep", None),
        P("ep", None),
        P("ep", None, "tp"),
        P("ep", None, "tp"),
        P("ep", "tp", None),
        P(None, "tp"),
        P(None, "tp"),
        P("tp", None),
    )
    out_specs = P("ep", "tp")

    return jax.shard_map(local, mesh=mesh, in_specs=in_specs, out_specs=out_specs, check_vma=False)
```

profile of v0, /device:TPU:0, one launch (start us, length us, event | category | flops | bytes accessed | tf_op | source)
XLA Modules:
  0.0 54.9 jit_solution(4021286500490802981)
XLA Ops:
  1.0 0.7 %copy-done.8 = s32[128,2]{0,1:T(2,128)S(1)} copy-done((s32[128,2]{0,1:T(2,128)S(1)}, s32[128,2]{0,1:T(2,128)}, u32[]{:S(2)}) %copy-start.8) | copy-done | bytes 1048
  1.7 1.0 %copy-done.3 = bf16[128,2048]{1,0:T(8,128)(2,1)S(1)} copy-done((bf16[128,2048]{1,0:T(8,128)(2,1)S(1)}, bf16[128,2048]{1,0:T(8,128)(2,1)}, u32[]{:S(2)}) %copy-start.3) | copy-done | bytes 524312
  2.7 1.0 %shard_map.100 = (bf16[128,2048]{1,0:T(8,128)(2,1)S(1)}, s32[2,128]{1,0:T(2,128)S(1)}, bf16[24,2048]{1,0:T(8,128)(2,1)S(1)}, bf16[24,2048]{1,0:T(8,128)(2,1)S(1)...) custom-call(s32[2,128]{1,0:T(2,128)S(1)} %bitcast.19, ...), custom_call_target="tpu_custom_call" | custom-call | flops 100663296 | bytes 1841152 | tf_op jit(solution)/shard_map/pallas_call | solution.py:21
  3.7 2.6 %collective-permute-start = (bf16[24,2048]{1,0:T(8,128)(2,1)S(1)}, bf16[24,2048]{1,0:T(8,128)(2,1)S(1)}, u32[]{:S(2)}, u32[]{:S(2)}) collective-permute-start(bf16[24,2048]{1,0:T(8,128)(2,1)S(1)} %get-tuple-element.35), channel_id=1, source_target_pairs={{0,4},{4,0},{8,12},{12,8},{16,20},{20,16},{24,28},{28,24},{1,5},{5... | collective-permute-start | bytes 294920 | tf_op jit(solution)/shard_map/ppermute | solution.py:188
  6.3 1.6 %collective-permute-start.1 = (bf16[24,2048]{1,0:T(8,128)(2,1)S(1)}, bf16[24,2048]{1,0:T(8,128)(2,1)S(1)}, u32[]{:S(2)}, u32[]{:S(2)}) collective-permute-start(bf16[24,2048]{1,0:T(8,128)(2,1)S(1)} %get-tuple-element.36), channel_id=1, source_target_pairs={{0,8},{4,12},{8,0},{12,4},{16,24},{20,28},{24,16},{28,20},{1,9},{5... | collective-permute-start | bytes 294920 | tf_op jit(solution)/shard_map/ppermute | solution.py:188
  7.9 1.8 %collective-permute-done.refs_1_ = bf16[24,2048]{1,0:T(8,128)(2,1)S(1)} collective-permute-done((bf16[24,2048]{1,0:T(8,128)(2,1)S(1)}, bf16[24,2048]{1,0:T(8,128)(2,1)S(1)}, u32[]{:S(2)}, u32[]{:S(2)}) %collective-permute-start) | collective-permute-done | bytes 98336 | tf_op jit(solution)/shard_map/ppermute | solution.py:188
  9.7 2.8 %collective-permute-start.2 = (bf16[24,2048]{1,0:T(8,128)(2,1)S(1)}, bf16[24,2048]{1,0:T(8,128)(2,1)S(1)}, u32[]{:S(2)}, u32[]{:S(2)}) collective-permute-start(bf16[24,2048]{1,0:T(8,128)(2,1)S(1)} %get-tuple-element.37), channel_id=1, source_target_pairs={{0,12},{4,8},{8,4},{12,0},{16,28},{20,24},{24,20},{28,16},{1,13},{... | collective-permute-start | bytes 294920 | tf_op jit(solution)/shard_map/ppermute | solution.py:188
  12.5 2.6 %collective-permute-start.10 = (bf16[24,2048]{1,0:T(8,128)(2,1)S(1)}, bf16[24,2048]{1,0:T(8,128)(2,1)S(1)}, u32[]{:S(2)}, u32[]{:S(2)}) collective-permute-start(bf16[24,2048]{1,0:T(8,128)(2,1)S(1)} %get-tuple-element.44), channel_id=1, source_target_pairs={{0,16},{4,20},{8,24},{12,28},{16,0},{20,4},{24,8},{28,12},{1,17},{... | collective-permute-start | bytes 294920 | tf_op jit(solution)/shard_map/ppermute | solution.py:188
  15.1 1.0 %copy-done.5 = bf16[2048,128]{1,0:T(8,128)(2,1)S(1)} copy-done((bf16[2048,128]{1,0:T(8,128)(2,1)S(1)}, bf16[2048,128]{1,0:T(8,128)(2,1)}, u32[]{:S(2)}) %copy-start.5) | copy-done | bytes 524312
  16.1 1.0 %copy-done.6 = bf16[128,2048]{1,0:T(8,128)(2,1)S(1)} copy-done((bf16[128,2048]{1,0:T(8,128)(2,1)S(1)}, bf16[128,2048]{1,0:T(8,128)(2,1)}, u32[]{:S(2)}) %copy-start.6) | copy-done | bytes 524312
  17.2 0.8 %shard_map.107 = (bf16[128,1024]{1,0:T(8,128)(2,1)S(1)}, f32[128,1024]{1,0:T(8,128)S(1)}) custom-call(bf16[128,2048]{1,0:T(8,128)(2,1)S(1)} %get-tuple-element.56.refs_0_, bf16[2048,128]{1,0:T(8,128)(2,1)S(1)} %copy-done.4, bf16[2048,128]{1,0:T(8,128)(2,1)S(1)} %copy-done.5, bf16[128,2048]{1,0:T(8,128)(2,1)S(1)} %copy-done.6), custom_call_target="tpu_custom_call" | custom-call | flops 201326592 | bytes 2883584 | tf_op jit(solution)/shard_map/pallas_call | solution.py:21
  18.0 1.6 %collective-permute-start.20 = (bf16[128,1024]{1,0:T(8,128)(2,1)S(1)}, bf16[128,1024]{1,0:T(8,128)(2,1)S(1)}, u32[]{:S(2)}, u32[]{:S(2)}) collective-permute-start(bf16[128,1024]{1,0:T(8,128)(2,1)S(1)} %get-tuple-element.58), channel_id=1, source_target_pairs={{0,2},{1,3},{2,0},{3,1},{4,6},{5,7},{6,4},{7,5},{8,10},{9,11},{10,... | collective-permute-start | bytes 786440 | tf_op jit(solution)/shard_map/ppermute | solution.py:193
  19.5 1.7 %collective-permute-start.11 = (bf16[24,2048]{1,0:T(8,128)(2,1)S(1)}, bf16[24,2048]{1,0:T(8,128)(2,1)S(1)}, u32[]{:S(2)}, u32[]{:S(2)}) collective-permute-start(bf16[24,2048]{1,0:T(8,128)(2,1)S(1)} %get-tuple-element.45), channel_id=1, source_target_pairs={{0,20},{4,16},{8,28},{12,24},{16,4},{20,0},{24,12},{28,8},{1,21},{... | collective-permute-start | bytes 294920 | tf_op jit(solution)/shard_map/ppermute | solution.py:188
  21.2 1.1 %collective-permute-start.15 = (bf16[24,2048]{1,0:T(8,128)(2,1)S(1)}, bf16[24,2048]{1,0:T(8,128)(2,1)S(1)}, u32[]{:S(2)}, u32[]{:S(2)}) collective-permute-start(bf16[24,2048]{1,0:T(8,128)(2,1)S(1)} %get-tuple-element.50), channel_id=1, source_target_pairs={{0,24},{4,28},{8,16},{12,20},{16,8},{20,12},{24,0},{28,4},{1,25},{... | collective-permute-start | bytes 294920 | tf_op jit(solution)/shard_map/ppermute | solution.py:188
  22.3 2.7 %collective-permute-start.16 = (bf16[24,2048]{1,0:T(8,128)(2,1)S(1)}, bf16[24,2048]{1,0:T(8,128)(2,1)S(1)}, u32[]{:S(2)}, u32[]{:S(2)}) collective-permute-start(bf16[24,2048]{1,0:T(8,128)(2,1)S(1)} %get-tuple-element.51), channel_id=1, source_target_pairs={{0,28},{4,24},{8,20},{12,16},{16,12},{20,8},{24,4},{28,0},{1,29},{... | collective-permute-start | bytes 294920 | tf_op jit(solution)/shard_map/ppermute | solution.py:188
  25.0 0.7 %shard_map.101 = (bf16[96,1024]{1,0:T(8,128)(2,1)S(1)}, f32[96,1024]{1,0:T(8,128)S(1)}) custom-call(bf16[24,2048]{1,0:T(8,128)(2,1)S(1)} %get-tuple-element.34.refs_0_, bf16[24,2048]{1,0:T(8,128)(2,1)S(1)} %collective-permute-done.refs_1_, bf16[24,2048]{1,0:T(8,128)(2,1)S(1)} %collective-permute-done.1.refs_2_, ...), custom_call_target="tpu_custom_call" | custom-call | flops 301989888 | bytes 4128768 | tf_op jit(solution)/shard_map/pallas_call | solution.py:21
  25.8 0.6 %collective-permute-start.6 = (bf16[96,1024]{1,0:T(8,128)(2,1)S(1)}, bf16[96,1024]{1,0:T(8,128)(2,1)S(1)}, u32[]{:S(2)}, u32[]{:S(2)}) collective-permute-start(bf16[96,1024]{1,0:T(8,128)(2,1)S(1)} %get-tuple-element.39), channel_id=1, source_target_pairs={{0,2},{1,3},{2,0},{3,1},{4,6},{5,7},{6,4},{7,5},{8,10},{9,11},{10,... | collective-permute-start | bytes 589832 | tf_op jit(solution)/shard_map/ppermute | solution.py:198
  26.4 4.7 %collective-permute-done.11.refs_1_ = bf16[24,2048]{1,0:T(8,128)(2,1)S(1)} collective-permute-done((bf16[24,2048]{1,0:T(8,128)(2,1)S(1)}, bf16[24,2048]{1,0:T(8,128)(2,1)S(1)}, u32[]{:S(2)}, u32[]{:S(2)}) %collective-permute-start.11) | collective-permute-done | bytes 98336 | tf_op jit(solution)/shard_map/ppermute | solution.py:188
  31.1 0.7 %shard_map.103 = (bf16[48,1024]{1,0:T(8,128)(2,1)S(1)}, f32[48,1024]{1,0:T(8,128)S(1)}) custom-call(bf16[24,2048]{1,0:T(8,128)(2,1)S(1)} %collective-permute-done.10.refs_0_, bf16[24,2048]{1,0:T(8,128)(2,1)S(1)} %collective-permute-done.11.refs_1_, bf16[2048,128]{1,0:T(8,128)(2,1)S(1)} %bitcast.8, bf16[2048,128]{1,0:T(8,128)(2,1)S(1)} %bitcast.12, ...), custom_call_target="tpu_custom_call" | custom-call | flops 150994944 | bytes 3637248 | tf_op jit(solution)/shard_map/pallas_call | solution.py:21
  31.8 0.6 %collective-permute-start.12 = (bf16[48,1024]{1,0:T(8,128)(2,1)S(1)}, bf16[48,1024]{1,0:T(8,128)(2,1)S(1)}, u32[]{:S(2)}, u32[]{:S(2)}) collective-permute-start(bf16[48,1024]{1,0:T(8,128)(2,1)S(1)} %get-tuple-element.47), channel_id=1, source_target_pairs={{0,2},{1,3},{2,0},{3,1},{4,6},{5,7},{6,4},{7,5},{8,10},{9,11},{10,... | collective-permute-start | bytes 294920 | tf_op jit(solution)/shard_map/ppermute | solution.py:198
  32.4 0.7 %shard_map.105 = (bf16[48,1024]{1,0:T(8,128)(2,1)S(1)}, f32[48,1024]{1,0:T(8,128)S(1)}) custom-call(bf16[24,2048]{1,0:T(8,128)(2,1)S(1)} %collective-permute-done.15.refs_0_, bf16[24,2048]{1,0:T(8,128)(2,1)S(1)} %collective-permute-done.16.refs_1_, bf16[2048,128]{1,0:T(8,128)(2,1)S(1)} %bitcast.9, bf16[2048,128]{1,0:T(8,128)(2,1)S(1)} %bitcast.13, ...), custom_call_target="tpu_custom_call" | custom-call | flops 150994944 | bytes 3637248 | tf_op jit(solution)/shard_map/pallas_call | solution.py:21
  33.2 1.5 %collective-permute-start.17 = (bf16[48,1024]{1,0:T(8,128)(2,1)S(1)}, bf16[48,1024]{1,0:T(8,128)(2,1)S(1)}, u32[]{:S(2)}, u32[]{:S(2)}) collective-permute-start(bf16[48,1024]{1,0:T(8,128)(2,1)S(1)} %get-tuple-element.53), channel_id=1, source_target_pairs={{0,2},{1,3},{2,0},{3,1},{4,6},{5,7},{6,4},{7,5},{8,10},{9,11},{10,... | collective-permute-start | bytes 294920 | tf_op jit(solution)/shard_map/ppermute | solution.py:198
  34.7 2.8 %collective-permute-done.12.came = bf16[48,1024]{1,0:T(8,128)(2,1)S(1)} collective-permute-done((bf16[48,1024]{1,0:T(8,128)(2,1)S(1)}, bf16[48,1024]{1,0:T(8,128)(2,1)S(1)}, u32[]{:S(2)}, u32[]{:S(2)}) %collective-permute-start.12) | collective-permute-done | bytes 98336 | tf_op jit(solution)/shard_map/ppermute | solution.py:198
  37.6 2.9 %collective-permute-start.14 = (bf16[24,1024]{1,0:T(8,128)(2,1)S(1)}, bf16[24,1024]{1,0:T(8,128)(2,1)S(1)}, u32[]{:S(2)}, u32[]{:S(2)}) collective-permute-start(bf16[24,1024]{1,0:T(8,128)(2,1)S(1)} %get-tuple-element.49), channel_id=1, source_target_pairs={{0,20},{4,16},{8,28},{12,24},{16,4},{20,0},{24,12},{28,8},{1,21},{... | collective-permute-start | bytes 147464 | tf_op jit(solution)/shard_map/ppermute | solution.py:188
  40.5 1.8 %collective-permute-start.18 = (bf16[24,1024]{1,0:T(8,128)(2,1)S(1)}, bf16[24,1024]{1,0:T(8,128)(2,1)S(1)}, u32[]{:S(2)}, u32[]{:S(2)}) collective-permute-start(bf16[24,1024]{1,0:T(8,128)(2,1)S(1)} %get-tuple-element.54), channel_id=1, source_target_pairs={{0,24},{4,28},{8,16},{12,20},{16,8},{20,12},{24,0},{28,4},{1,25},{... | collective-permute-start | bytes 147464 | tf_op jit(solution)/shard_map/ppermute | solution.py:188
  42.3 3.0 %collective-permute-start.19 = (bf16[24,1024]{1,0:T(8,128)(2,1)S(1)}, bf16[24,1024]{1,0:T(8,128)(2,1)S(1)}, u32[]{:S(2)}, u32[]{:S(2)}) collective-permute-start(bf16[24,1024]{1,0:T(8,128)(2,1)S(1)} %get-tuple-element.55), channel_id=1, source_target_pairs={{0,28},{4,24},{8,20},{12,16},{16,12},{20,8},{24,4},{28,0},{1,29},{... | collective-permute-start | bytes 147464 | tf_op jit(solution)/shard_map/ppermute | solution.py:188
  45.4 0.6 %collective-permute-start.7 = (bf16[24,1024]{1,0:T(8,128)(2,1)S(1)}, bf16[24,1024]{1,0:T(8,128)(2,1)S(1)}, u32[]{:S(2)}, u32[]{:S(2)}) collective-permute-start(bf16[24,1024]{1,0:T(8,128)(2,1)S(1)} %get-tuple-element.41), channel_id=1, source_target_pairs={{0,4},{4,0},{8,12},{12,8},{16,20},{20,16},{24,28},{28,24},{1,5},{5... | collective-permute-start | bytes 147464 | tf_op jit(solution)/shard_map/ppermute | solution.py:188
  46.0 3.0 %collective-permute-start.9 = (bf16[24,1024]{1,0:T(8,128)(2,1)S(1)}, bf16[24,1024]{1,0:T(8,128)(2,1)S(1)}, u32[]{:S(2)}, u32[]{:S(2)}) collective-permute-start(bf16[24,1024]{1,0:T(8,128)(2,1)S(1)} %get-tuple-element.43), channel_id=1, source_target_pairs={{0,12},{4,8},{8,4},{12,0},{16,28},{20,24},{24,20},{28,16},{1,13},{... | collective-permute-start | bytes 147464 | tf_op jit(solution)/shard_map/ppermute | solution.py:188
  50.1 1.5 %collective-permute-done.9.refs_3_ = bf16[24,1024]{1,0:T(8,128)(2,1)S(1)} collective-permute-done((bf16[24,1024]{1,0:T(8,128)(2,1)S(1)}, bf16[24,1024]{1,0:T(8,128)(2,1)S(1)}, u32[]{:S(2)}, u32[]{:S(2)}) %collective-permute-start.9) | collective-permute-done | bytes 49184 | tf_op jit(solution)/shard_map/ppermute | solution.py:188
  51.5 0.7 %copy-done.9 = f32[128,2]{0,1:T(2,128)S(1)} copy-done((f32[128,2]{0,1:T(2,128)S(1)}, f32[128,2]{0,1:T(2,128)}, u32[]{:S(2)}) %copy-start.9) | copy-done | bytes 1048
  52.7 1.5 %collective-permute-done.21.came = f32[128,512]{1,0:T(8,128)S(1)} collective-permute-done((f32[128,512]{1,0:T(8,128)S(1)}, f32[128,512]{1,0:T(8,128)S(1)}, u32[]{:S(2)}, u32[]{:S(2)}) %collective-permute-start.21) | collective-permute-done | bytes 262176 | tf_op jit(solution)/shard_map/ppermute | solution.py:210
  54.2 0.7 %shard_map.109 = bf16[128,512]{1,0:T(8,128)(2,1)} custom-call(f32[128,512]{1,0:T(8,128)S(1)} %get-tuple-element.59.keep, f32[128,512]{1,0:T(8,128)S(1)} %collective-permute-done.21.came), custom_call_target="tpu_custom_call" | custom-call | flops 65536 | bytes 655360 | tf_op jit(solution)/shard_map/pallas_call | solution.py:21
  (42 shorter events, 2.7 us)
Async XLA Ops:
  0.0 1.0 %copy-start.7 = (bf16[2048]{0:T(1024)(128)(2,1)S(1)}, bf16[2048]{0:T(1024)(128)(2,1)}, u32[]{:S(2)}) copy-start(bf16[2048]{0:T(1024)(128)(2,1)} %param.11) | copy-start | bytes 12292
  0.0 19.5 %collective-permute-start.3 = (bf16[2048,128]{1,0:T(8,128)(2,1)}, bf16[2048,128]{1,0:T(8,128)(2,1)S(1)}, u32[]{:S(2)}, u32[]{:S(2)}) collective-permute-start(bf16[2048,128]{1,0:T(8,128)(2,1)} %bitcast.6), channel_id=1, source_target_pairs={{0,1},{1,0},{2,3},{3,2},{4,5},{5,4},{6,7},{7,6},{8,9},{9,8},{10,11... | collective-permute-start | bytes 1572872 | tf_op jit(solution)/shard_map/ppermute | solution.py:172
  0.5 20.7 %collective-permute-start.4 = (bf16[2048,128]{1,0:T(8,128)(2,1)}, bf16[2048,128]{1,0:T(8,128)(2,1)S(1)}, u32[]{:S(2)}, u32[]{:S(2)}) collective-permute-start(bf16[2048,128]{1,0:T(8,128)(2,1)} %bitcast.10), channel_id=1, source_target_pairs={{0,1},{1,0},{2,3},{3,2},{4,5},{5,4},{6,7},{7,6},{8,9},{9,8},{10,11... | collective-permute-start | bytes 1572872 | tf_op jit(solution)/shard_map/ppermute | solution.py:172
  0.6 21.7 %collective-permute-start.5 = (bf16[128,2048]{1,0:T(8,128)(2,1)}, bf16[128,2048]{1,0:T(8,128)(2,1)S(1)}, u32[]{:S(2)}, u32[]{:S(2)}) collective-permute-start(bf16[128,2048]{1,0:T(8,128)(2,1)} %bitcast.14), channel_id=1, source_target_pairs={{0,1},{1,0},{2,3},{3,2},{4,5},{5,4},{6,7},{7,6},{8,9},{9,8},{10,11... | collective-permute-start | bytes 1572872 | tf_op jit(solution)/shard_map/ppermute | solution.py:172
  1.0 0.7 %copy-start.8 = (s32[128,2]{0,1:T(2,128)S(1)}, s32[128,2]{0,1:T(2,128)}, u32[]{:S(2)}) copy-start(s32[128,2]{0,1:T(2,128)} %param.12) | copy-start | bytes 3076
  1.7 1.0 %copy-start.3 = (bf16[128,2048]{1,0:T(8,128)(2,1)S(1)}, bf16[128,2048]{1,0:T(8,128)(2,1)}, u32[]{:S(2)}) copy-start(bf16[128,2048]{1,0:T(8,128)(2,1)} %tokens.1) | copy-start | bytes 1572868
  2.7 12.3 %copy-start.4 = (bf16[2048,128]{1,0:T(8,128)(2,1)S(1)}, bf16[2048,128]{1,0:T(8,128)(2,1)}, u32[]{:S(2)}) copy-start(bf16[2048,128]{1,0:T(8,128)(2,1)} %refs_1_.1) | copy-start | bytes 1572868
  3.7 6.0 %collective-permute-start = (bf16[24,2048]{1,0:T(8,128)(2,1)S(1)}, bf16[24,2048]{1,0:T(8,128)(2,1)S(1)}, u32[]{:S(2)}, u32[]{:S(2)}) collective-permute-start(bf16[24,2048]{1,0:T(8,128)(2,1)S(1)} %get-tuple-element.35), channel_id=1, source_target_pairs={{0,4},{4,0},{8,12},{12,8},{16,20},{20,16},{24,28},{28,24},{1,5},{5... | collective-permute-start | bytes 294920 | tf_op jit(solution)/shard_map/ppermute | solution.py:188
  6.3 6.2 %collective-permute-start.1 = (bf16[24,2048]{1,0:T(8,128)(2,1)S(1)}, bf16[24,2048]{1,0:T(8,128)(2,1)S(1)}, u32[]{:S(2)}, u32[]{:S(2)}) collective-permute-start(bf16[24,2048]{1,0:T(8,128)(2,1)S(1)} %get-tuple-element.36), channel_id=1, source_target_pairs={{0,8},{4,12},{8,0},{12,4},{16,24},{20,28},{24,16},{28,20},{1,9},{5... | collective-permute-start | bytes 294920 | tf_op jit(solution)/shard_map/ppermute | solution.py:188
  9.7 8.2 %collective-permute-start.2 = (bf16[24,2048]{1,0:T(8,128)(2,1)S(1)}, bf16[24,2048]{1,0:T(8,128)(2,1)S(1)}, u32[]{:S(2)}, u32[]{:S(2)}) collective-permute-start(bf16[24,2048]{1,0:T(8,128)(2,1)S(1)} %get-tuple-element.37), channel_id=1, source_target_pairs={{0,12},{4,8},{8,4},{12,0},{16,28},{20,24},{24,20},{28,16},{1,13},{... | collective-permute-start | bytes 294920 | tf_op jit(solution)/shard_map/ppermute | solution.py:188
  12.5 13.3 %collective-permute-start.10 = (bf16[24,2048]{1,0:T(8,128)(2,1)S(1)}, bf16[24,2048]{1,0:T(8,128)(2,1)S(1)}, u32[]{:S(2)}, u32[]{:S(2)}) collective-permute-start(bf16[24,2048]{1,0:T(8,128)(2,1)S(1)} %get-tuple-element.44), channel_id=1, source_target_pairs={{0,16},{4,20},{8,24},{12,28},{16,0},{20,4},{24,8},{28,12},{1,17},{... | collective-permute-start | bytes 294920 | tf_op jit(solution)/shard_map/ppermute | solution.py:188
  15.1 1.0 %copy-start.5 = (bf16[2048,128]{1,0:T(8,128)(2,1)S(1)}, bf16[2048,128]{1,0:T(8,128)(2,1)}, u32[]{:S(2)}) copy-start(bf16[2048,128]{1,0:T(8,128)(2,1)} %refs_2_.1) | copy-start | bytes 1572868
  16.1 1.0 %copy-start.6 = (bf16[128,2048]{1,0:T(8,128)(2,1)S(1)}, bf16[128,2048]{1,0:T(8,128)(2,1)}, u32[]{:S(2)}) copy-start(bf16[128,2048]{1,0:T(8,128)(2,1)} %refs_3_.1) | copy-start | bytes 1572868
  17.2 7.8 %copy-start = (bf16[1,2048,128]{2,1,0:T(8,128)(2,1)S(1)}, bf16[1,2048,128]{2,1,0:T(8,128)(2,1)}, u32[]{:S(2)}) copy-start(bf16[1,2048,128]{2,1,0:T(8,128)(2,1)} %param.14) | copy-start | bytes 1572868
  17.2 7.8 %copy-start.1 = (bf16[1,2048,128]{2,1,0:T(8,128)(2,1)S(1)}, bf16[1,2048,128]{2,1,0:T(8,128)(2,1)}, u32[]{:S(2)}) copy-start(bf16[1,2048,128]{2,1,0:T(8,128)(2,1)} %param.15) | copy-start | bytes 1572868
  17.2 7.8 %copy-start.2 = (bf16[1,128,2048]{2,1,0:T(8,128)(2,1)S(1)}, bf16[1,128,2048]{2,1,0:T(8,128)(2,1)}, u32[]{:S(2)}) copy-start(bf16[1,128,2048]{2,1,0:T(8,128)(2,1)} %param.16) | copy-start | bytes 1572868
  18.0 27.4 %collective-permute-start.20 = (bf16[128,1024]{1,0:T(8,128)(2,1)S(1)}, bf16[128,1024]{1,0:T(8,128)(2,1)S(1)}, u32[]{:S(2)}, u32[]{:S(2)}) collective-permute-start(bf16[128,1024]{1,0:T(8,128)(2,1)S(1)} %get-tuple-element.58), channel_id=1, source_target_pairs={{0,2},{1,3},{2,0},{3,1},{4,6},{5,7},{6,4},{7,5},{8,10},{9,11},{10,... | collective-permute-start | bytes 786440 | tf_op jit(solution)/shard_map/ppermute | solution.py:193
  19.5 11.6 %collective-permute-start.11 = (bf16[24,2048]{1,0:T(8,128)(2,1)S(1)}, bf16[24,2048]{1,0:T(8,128)(2,1)S(1)}, u32[]{:S(2)}, u32[]{:S(2)}) collective-permute-start(bf16[24,2048]{1,0:T(8,128)(2,1)S(1)} %get-tuple-element.45), channel_id=1, source_target_pairs={{0,20},{4,16},{8,28},{12,24},{16,4},{20,0},{24,12},{28,8},{1,21},{... | collective-permute-start | bytes 294920 | tf_op jit(solution)/shard_map/ppermute | solution.py:188
  21.2 11.2 %collective-permute-start.15 = (bf16[24,2048]{1,0:T(8,128)(2,1)S(1)}, bf16[24,2048]{1,0:T(8,128)(2,1)S(1)}, u32[]{:S(2)}, u32[]{:S(2)}) collective-permute-start(bf16[24,2048]{1,0:T(8,128)(2,1)S(1)} %get-tuple-element.50), channel_id=1, source_target_pairs={{0,24},{4,28},{8,16},{12,20},{16,8},{20,12},{24,0},{28,4},{1,25},{... | collective-permute-start | bytes 294920 | tf_op jit(solution)/shard_map/ppermute | solution.py:188
  22.3 10.1 %collective-permute-start.16 = (bf16[24,2048]{1,0:T(8,128)(2,1)S(1)}, bf16[24,2048]{1,0:T(8,128)(2,1)S(1)}, u32[]{:S(2)}, u32[]{:S(2)}) collective-permute-start(bf16[24,2048]{1,0:T(8,128)(2,1)S(1)} %get-tuple-element.51), channel_id=1, source_target_pairs={{0,28},{4,24},{8,20},{12,16},{16,12},{20,8},{24,4},{28,0},{1,29},{... | collective-permute-start | bytes 294920 | tf_op jit(solution)/shard_map/ppermute | solution.py:188
  25.8 16.5 %collective-permute-start.6 = (bf16[96,1024]{1,0:T(8,128)(2,1)S(1)}, bf16[96,1024]{1,0:T(8,128)(2,1)S(1)}, u32[]{:S(2)}, u32[]{:S(2)}) collective-permute-start(bf16[96,1024]{1,0:T(8,128)(2,1)S(1)} %get-tuple-element.39), channel_id=1, source_target_pairs={{0,2},{1,3},{2,0},{3,1},{4,6},{5,7},{6,4},{7,5},{8,10},{9,11},{10,... | collective-permute-start | bytes 589832 | tf_op jit(solution)/shard_map/ppermute | solution.py:198
  31.8 5.7 %collective-permute-start.12 = (bf16[48,1024]{1,0:T(8,128)(2,1)S(1)}, bf16[48,1024]{1,0:T(8,128)(2,1)S(1)}, u32[]{:S(2)}, u32[]{:S(2)}) collective-permute-start(bf16[48,1024]{1,0:T(8,128)(2,1)S(1)} %get-tuple-element.47), channel_id=1, source_target_pairs={{0,2},{1,3},{2,0},{3,1},{4,6},{5,7},{6,4},{7,5},{8,10},{9,11},{10,... | collective-permute-start | bytes 294920 | tf_op jit(solution)/shard_map/ppermute | solution.py:198
  33.2 7.3 %collective-permute-start.17 = (bf16[48,1024]{1,0:T(8,128)(2,1)S(1)}, bf16[48,1024]{1,0:T(8,128)(2,1)S(1)}, u32[]{:S(2)}, u32[]{:S(2)}) collective-permute-start(bf16[48,1024]{1,0:T(8,128)(2,1)S(1)} %get-tuple-element.53), channel_id=1, source_target_pairs={{0,2},{1,3},{2,0},{3,1},{4,6},{5,7},{6,4},{7,5},{8,10},{9,11},{10,... | collective-permute-start | bytes 294920 | tf_op jit(solution)/shard_map/ppermute | solution.py:198
  37.5 8.4 %collective-permute-start.13 = (bf16[24,1024]{1,0:T(8,128)(2,1)S(1)}, bf16[24,1024]{1,0:T(8,128)(2,1)S(1)}, u32[]{:S(2)}, u32[]{:S(2)}) collective-permute-start(bf16[24,1024]{1,0:T(8,128)(2,1)S(1)} %get-tuple-element.48), channel_id=1, source_target_pairs={{0,16},{4,20},{8,24},{12,28},{16,0},{20,4},{24,8},{28,12},{1,17},{... | collective-permute-start | bytes 147464 | tf_op jit(solution)/shard_map/ppermute | solution.py:188
  37.6 8.4 %collective-permute-start.14 = (bf16[24,1024]{1,0:T(8,128)(2,1)S(1)}, bf16[24,1024]{1,0:T(8,128)(2,1)S(1)}, u32[]{:S(2)}, u32[]{:S(2)}) collective-permute-start(bf16[24,1024]{1,0:T(8,128)(2,1)S(1)} %get-tuple-element.49), channel_id=1, source_target_pairs={{0,20},{4,16},{8,28},{12,24},{16,4},{20,0},{24,12},{28,8},{1,21},{... | collective-permute-start | bytes 147464 | tf_op jit(solution)/shard_map/ppermute | solution.py:188
  40.5 8.5 %collective-permute-start.18 = (bf16[24,1024]{1,0:T(8,128)(2,1)S(1)}, bf16[24,1024]{1,0:T(8,128)(2,1)S(1)}, u32[]{:S(2)}, u32[]{:S(2)}) collective-permute-start(bf16[24,1024]{1,0:T(8,128)(2,1)S(1)} %get-tuple-element.54), channel_id=1, source_target_pairs={{0,24},{4,28},{8,16},{12,20},{16,8},{20,12},{24,0},{28,4},{1,25},{... | collective-permute-start | bytes 147464 | tf_op jit(solution)/shard_map/ppermute | solution.py:188
  42.3 6.8 %collective-permute-start.19 = (bf16[24,1024]{1,0:T(8,128)(2,1)S(1)}, bf16[24,1024]{1,0:T(8,128)(2,1)S(1)}, u32[]{:S(2)}, u32[]{:S(2)}) collective-permute-start(bf16[24,1024]{1,0:T(8,128)(2,1)S(1)} %get-tuple-element.55), channel_id=1, source_target_pairs={{0,28},{4,24},{8,20},{12,16},{16,12},{20,8},{24,4},{28,0},{1,29},{... | collective-permute-start | bytes 147464 | tf_op jit(solution)/shard_map/ppermute | solution.py:188
  45.4 4.2 %collective-permute-start.7 = (bf16[24,1024]{1,0:T(8,128)(2,1)S(1)}, bf16[24,1024]{1,0:T(8,128)(2,1)S(1)}, u32[]{:S(2)}, u32[]{:S(2)}) collective-permute-start(bf16[24,1024]{1,0:T(8,128)(2,1)S(1)} %get-tuple-element.41), channel_id=1, source_target_pairs={{0,4},{4,0},{8,12},{12,8},{16,20},{20,16},{24,28},{28,24},{1,5},{5... | collective-permute-start | bytes 147464 | tf_op jit(solution)/shard_map/ppermute | solution.py:188
  46.0 4.1 %collective-permute-start.8 = (bf16[24,1024]{1,0:T(8,128)(2,1)S(1)}, bf16[24,1024]{1,0:T(8,128)(2,1)S(1)}, u32[]{:S(2)}, u32[]{:S(2)}) collective-permute-start(bf16[24,1024]{1,0:T(8,128)(2,1)S(1)} %get-tuple-element.42), channel_id=1, source_target_pairs={{0,8},{4,12},{8,0},{12,4},{16,24},{20,28},{24,16},{28,20},{1,9},{5... | collective-permute-start | bytes 147464 | tf_op jit(solution)/shard_map/ppermute | solution.py:188
  46.0 5.6 %collective-permute-start.9 = (bf16[24,1024]{1,0:T(8,128)(2,1)S(1)}, bf16[24,1024]{1,0:T(8,128)(2,1)S(1)}, u32[]{:S(2)}, u32[]{:S(2)}) collective-permute-start(bf16[24,1024]{1,0:T(8,128)(2,1)S(1)} %get-tuple-element.43), channel_id=1, source_target_pairs={{0,12},{4,8},{8,4},{12,0},{16,28},{20,24},{24,20},{28,16},{1,13},{... | collective-permute-start | bytes 147464 | tf_op jit(solution)/shard_map/ppermute | solution.py:188
  51.5 0.7 %copy-start.9 = (f32[128,2]{0,1:T(2,128)S(1)}, f32[128,2]{0,1:T(2,128)}, u32[]{:S(2)}) copy-start(f32[128,2]{0,1:T(2,128)} %param.13) | copy-start | bytes 3076
  52.6 1.6 %collective-permute-start.21 = (f32[128,512]{1,0:T(8,128)S(1)}, f32[128,512]{1,0:T(8,128)S(1)}, u32[]{:S(2)}, u32[]{:S(2)}) collective-permute-start(f32[128,512]{1,0:T(8,128)S(1)} %get-tuple-element.60), channel_id=1, source_target_pairs={{0,1},{1,0},{2,3},{3,2},{4,5},{5,4},{6,7},{7,6},{8,9},{9,8},{10,11... | collective-permute-start | bytes 786440 | tf_op jit(solution)/shard_map/ppermute | solution.py:210
where the time goes:
time: 55.2 us; the launch traced here: 54.9 us
  starting transfers between devices  31.7 us (57%)
  waiting for transfers between devices  13.5 us (24%)
  Pallas kernels  5.11 us (9%)
  local copies, waits for them, and re-layouts  4.5 us (8%)
    ppermute x14, starting transfers between devices, exchange(): return lax.ppermute(block, 'ep', [(i, i ^ k) for i in range(groups)])  26.3 us
    ppermute x14, waiting for transfers between devices, exchange(): return lax.ppermute(block, 'ep', [(i, i ^ k) for i in range(groups)])  9.16 us
    pallas_call x10, Pallas kernels, call(): pl.pallas_call(body, out_shape=outs, in_specs=[vmem] * len(ins), out_spec...  5.11 us
    unnamed x20, local copies, waits for them, and re-layouts  4.5 us
    ppermute x3, waiting for transfers between devices, local(): came = lax.ppermute(send, 'tp', neighbour)  2.82 us
    ppermute x3, starting transfers between devices, local(): came = lax.ppermute(send, 'tp', neighbour)  2.71 us
    ppermute x1, starting transfers between devices, local(): sh_came = lax.ppermute(sh_send, 'tp', neighbour)  1.56 us
    ppermute x1, waiting for transfers between devices, local(): came = lax.ppermute(sent, 'tp', sibling)  1.52 us
  transfers between devices with their start and end apart: 22, of which 8 were waited for; matrix products, arithmetic and copies ran while one was open for 0% of the time, Pallas kernels for 7%

commit v1 on v0

v1 whole, which is shorter than its diff:
```python
import functools

import jax
import jax.numpy as jnp
from jax import lax
from jax.experimental import pallas as pl
from jax.experimental.pallas import tpu as pltpu
from jax.sharding import PartitionSpec as P

norm_eps = 1e-06
grant = 16 * 1024 * 1024
f32 = jnp.float32
bf16 = jnp.bfloat16

vmem = pl.BlockSpec(memory_space=pltpu.VMEM)
hbm = pl.BlockSpec(memory_space=pltpu.HBM)


def call(body, outs, ins, flops, scratch=(), far=()):
    moved = sum(a.size * a.dtype.itemsize for a in ins)
    moved += sum(o.size * o.dtype.itemsize for o in outs)
    ins = [
        pltpu.with_memory_space_constraint(a, pltpu.HBM) if i in far else a for i, a in enumerate(ins)
    ]
    return pl.pallas_call(
        body,
        out_shape=outs,
        in_specs=[hbm if i in far else vmem for i in range(len(ins))],
        out_specs=[vmem] * len(outs),
        scratch_shapes=list(scratch),
        compiler_params=pltpu.CompilerParams(vmem_limit_bytes=grant),
        cost_estimate=pl.CostEstimate(flops=flops, bytes_accessed=moved, transcendentals=0),
    )(*ins)


def landing(arrays):
    return [pltpu.VMEM(a.shape, a.dtype) for a in arrays] + [pltpu.SemaphoreType.DMA((len(arrays),))]


def fetch(sources, targets, sems):
    copies = [
        pltpu.make_async_copy(s, t, sems.at[i]) for i, (s, t) in enumerate(zip(sources, targets))
    ]
    for copy in copies:
        copy.start()
    return copies


def shape(rows, columns, dtype):
    return jax.ShapeDtypeStruct((rows, columns), dtype)


def route_body(half, experts, far, kept, ids_in, gain_in, tokens_in, *refs):
    outs, (ids, gain, tokens, sems) = refs[:-4], refs[-4:]
    copies = fetch((ids_in, gain_in, tokens_in), (ids, gain, tokens), sems)
    normed_out, slots_out = outs[0], outs[1]
    rows, width = tokens.shape
    mixed = lax.axis_index("ep") if far else 0
    side = lax.axis_index("tp") // 2
    first = (lax.axis_index("tp") % 2) * half
    kinds = max(8, experts)
    kind = lax.broadcasted_iota(jnp.int32, (kinds, rows), 0)
    before = (
        lax.broadcasted_iota(jnp.int32, (rows, rows), 0)
        < lax.broadcasted_iota(jnp.int32, (rows, rows), 1)
    ).astype(bf16)
    base = jnp.zeros((kinds, 1), f32)
    total = experts * half
    slot = lax.broadcasted_iota(jnp.int32, (total, rows), 0)
    hit = jnp.zeros((total, rows), f32)
    copies[0].wait()
    for j in range(ids.shape[0]):
        label = ids[j : j + 1, :] ^ mixed
        if far:
            label = jnp.where(label >= far, label ^ side, label)
        onehot = (kind == label).astype(f32)
        earlier = jnp.dot(onehot.astype(bf16), before, preferred_element_type=f32) + base
        rank = jnp.sum(earlier * onehot, axis=0, keepdims=True).astype(jnp.int32) - first
        base = base + jnp.sum(onehot, axis=1, keepdims=True)
        held = jnp.logical_and(rank >= 0, rank < half)
        where = jnp.where(held, label * half + rank, -1)
        slots_out[j : j + 1, :] = where
        hit = jnp.where(slot == where, 1.0, hit)
    pick = hit.astype(bf16)
    copies[1].wait()
    copies[2].wait()
    values = tokens[...].astype(f32)
    scale = lax.rsqrt(jnp.mean(values * values, axis=-1, keepdims=True) + norm_eps)
    lanes = gain.shape[1]
    for c in range(width // lanes):
        at = slice(c * lanes, (c + 1) * lanes)
        normed_out[:, at] = (values[:, at] * scale * gain[c : c + 1].astype(f32)).astype(bf16)
    normed = normed_out[...]
    for k, out in zip(kept, outs[2:]):
        n = out.shape[0]
        part = pick[k * n : (k + 1) * n]
        out[...] = jnp.dot(part, normed, preferred_element_type=f32).astype(bf16)


def product_body(blocks, sets, swap, fetched, *refs):
    rows_in, weights = refs[:blocks], refs[blocks : blocks + 3 * sets]
    send, keep = refs[blocks + 3 * sets : blocks + 3 * sets + 2]
    rest = refs[blocks + 3 * sets + 2 :]
    if fetched:
        copies = fetch(weights, rest[:-1], rest[-1])
        weights = rest[:-1]
    if blocks > 1:
        gathered = rest[0]
        at = 0
        for ref in rows_in:
            gathered[at : at + ref.shape[0]] = ref[...]
            at += ref.shape[0]
    else:
        gathered = rows_in[0]
    side = lax.axis_index("tp") // 2
    if fetched:
        for copy in copies:
            copy.wait()
    into = [w[...] for w in weights[::3]] + [w[...] for w in weights[1::3]]
    both = jnp.dot(gathered[...], jnp.concatenate(into, axis=1), preferred_element_type=f32)
    units = both.shape[1] // 2
    gate, up = both[:, :units], both[:, units:]
    hidden = (gate / (1.0 + jnp.exp(-gate)) * up).astype(bf16)
    width = keep.shape[1]
    step = rows_in[0].shape[0]
    for out, place in ((send, 1 - side), (keep, side)):
        columns = pl.ds(pl.multiple_of(place * width, width), width)
        down = jnp.concatenate([w[:, columns] for w in weights[2::3]], axis=0)
        total = jnp.dot(hidden, down, preferred_element_type=f32).astype(out.dtype)
        if out is send and blocks > 1:
            for b in range(blocks):
                c = b ^ 1 if swap[b] else b
                out[c * step : (c + 1) * step] = total[b * step : (b + 1) * step]
        else:
            out[...] = total


def products(rows, weights, width, swap=(), fetched=False):
    n = sum(r.shape[0] for r in rows)
    full = rows[0].shape[1]
    hidden = sum(w.shape[1] for w in weights[::3])
    scratch = [pltpu.VMEM((n, full), bf16)] if len(rows) > 1 else []
    far = ()
    if fetched:
        scratch = landing(weights)
        far = range(len(rows), len(rows) + len(weights))
    return call(
        functools.partial(product_body, len(rows), len(weights) // 3, swap, fetched),
        [shape(n, width, bf16), shape(n, width, f32)],
        [*rows, *weights],
        6 * n * full * hidden,
        scratch,
        far,
    )


def add_body(keep, came, *outs):
    at = 0
    for out in outs:
        n = out.shape[0]
        out[...] = (keep[at : at + n] + came[at : at + n].astype(f32)).astype(out.dtype)
        at += n


def plan_body(slots, gains_in, high_out, low_out, gains, sems):
    (copy,) = fetch((gains_in,), (gains,), sems)
    slot = lax.broadcasted_iota(jnp.int32, high_out.shape[::-1], 0)
    weight = jnp.zeros(slot.shape, f32)
    copy.wait()
    for j in range(slots.shape[0]):
        weight = jnp.where(slot == slots[j : j + 1, :], gains[j : j + 1, :], weight)
    weight = weight.T
    high = weight.astype(bf16)
    high_out[...] = high
    low_out[...] = (weight - high.astype(f32)).astype(bf16)


def mix_body(blocks, high, low, *refs):
    rows_in, adds, outs = refs[:blocks], refs[blocks:-3], refs[-3:-1]
    gathered = refs[-1]
    at = 0
    for ref in rows_in:
        gathered[at : at + ref.shape[0]] = ref[...]
        at += ref.shape[0]
    width = outs[0].shape[1]
    core = lax.axis_index("tp") % 2
    for out, place in ((outs[0], core), (outs[1], 1 - core)):
        columns = pl.ds(pl.multiple_of(place * width, width), width)
        rows = gathered[:, columns]
        total = sum(a[:, columns].astype(f32) for a in adds)
        total += jnp.dot(high[...], rows, preferred_element_type=f32)
        out[...] = total + jnp.dot(low[...], rows, preferred_element_type=f32)


def local(
    tokens,
    norm_gain,
    expert_ids,
    route_weights,
    gate_weight,
    up_weight,
    down_weight,
    shared_gate,
    shared_up,
    shared_down,
):
    rows_here, width = tokens.shape
    chosen = expert_ids.shape[1]
    groups = lax.axis_size("ep")
    cuts = lax.axis_size("tp")
    local_experts = gate_weight.shape[0]
    assert local_experts == 1 and cuts == 4
    capacity = (3 * rows_here * chosen + 2 * groups - 1) // (2 * groups)
    half = -(-capacity // 2)
    wide, share = width // 2, width // 4
    direct = groups == 8
    far = groups // 2 if direct else 0
    sibling = [(i, i ^ 1) for i in range(cuts)]
    neighbour = [(i, i ^ 2) for i in range(cuts)]
    own = (gate_weight[0], up_weight[0], down_weight[0])
    other = tuple(lax.ppermute(w, "tp", sibling) for w in own)

    def hop(k, block):
        if not direct:
            return lax.all_to_all(block, "ep", split_axis=0, concat_axis=0, tiled=True)
        if k == 0:
            return block
        pairs = []
        for i in range(groups):
            for t in range(cuts):
                to = i ^ (k ^ (t // 2) if k >= far else k)
                pairs.append((i * cuts + t, to * cuts + t))
        return lax.ppermute(block, ("ep", "tp"), pairs)

    sizes = [half] * groups if direct else [half * groups]
    kept = [0, 1, 2, 3, 4, 7] if direct else [0]
    args = [expert_ids.T, norm_gain.reshape(-1, 128), tokens]
    normed, slots, *sends = call(
        functools.partial(route_body, half, groups, far, kept),
        [shape(rows_here, width, bf16), shape(chosen, rows_here, jnp.int32)]
        + [shape(sizes[k], width, bf16) for k in kept],
        args,
        2 * rows_here * width * half * groups,
        landing(args),
        range(3),
    )
    arrived = {k: hop(k, block) for k, block in zip(kept, sends)}
    if direct:
        arrived[5] = lax.ppermute(arrived[4], "tp", neighbour)
        arrived[6] = lax.ppermute(arrived[7], "tp", neighbour)
    sh_send, sh_keep = products([normed], [shared_gate, shared_up, shared_down], wide, fetched=True)
    sh_came = lax.ppermute(sh_send, "tp", neighbour)
    gains = route_weights.T
    high, low = call(
        plan_body,
        [shape(rows_here, half * groups, bf16)] * 2,
        [slots, gains],
        rows_here * half * groups,
        landing([gains]),
        [1],
    )

    returned = [None] * len(sizes)
    for names in (parties if direct else {"A": [0]}).values():
        swap = [far > 0 and k >= far for k in names]
        send, keep = products([arrived[k] for k in names], [*own, *other], wide, swap)
        came = lax.ppermute(send, "tp", neighbour)
        outs = call(add_body, [shape(sizes[k], wide, bf16) for k in names], [keep, came], keep.size)
        for k, out in zip(names, outs):
            returned[k] = hop(k, out)

    mine, sent = call(
        functools.partial(mix_body, len(returned)),
        [shape(rows_here, share, f32), shape(rows_here, share, f32)],
        [high, low, *returned, sh_keep, sh_came],
        4 * rows_here * wide * half * groups,
        [pltpu.VMEM((half * groups, wide), bf16)],
    )
    came = lax.ppermute(sent, "tp", sibling)
    (mixed,) = call(add_body, [shape(rows_here, share, bf16)], [mine, came], mine.size)
    return mixed


parties = {"N": [0, 1, 2, 3], "A": [4, 5], "B": [6, 7]}


def solution(mesh):
    in_specs = (
        P("ep", None),
        P(),
        P("ep", None),
        P("ep", None),
        P("ep", None, "tp"),
        P("ep", None, "tp"),
        P("ep", "tp", None),
        P(None, "tp"),
        P(None, "tp"),
        P("tp", None),
    )
    out_specs = P("ep", "tp")

    return jax.shard_map(local, mesh=mesh, in_specs=in_specs, out_specs=out_specs, check_vma=False)
```

time: 55.2 us -> 55.9 us (1.013)
  local copies, waits for them, and re-layouts: 4.5 us -> 0.01 us
  Pallas kernels: 5.11 us -> 8.24 us
  starting transfers between devices: 31.7 us -> 34.2 us
    unnamed x20 -> x6, local copies, waits for them, and re-layouts: 4.5 us -> 0.01 us
    pallas_call x10 -> x11, Pallas kernels: 5.11 us -> 8.24 us  [call(): pl.pallas_call(body, out_shape=outs, in_specs=[hbm if i in far else vmem...]
    ppermute x3, starting transfers between devices: 2.71 us -> 4.34 us  [local(): came = lax.ppermute(send, 'tp', neighbour)]
    ppermute x1, starting transfers between devices: 1.56 us -> 2.75 us  [local(): sh_came = lax.ppermute(sh_send, 'tp', neighbour)]
    ppermute x3, waiting for transfers between devices: 2.82 us -> 1.77 us  [local(): came = lax.ppermute(send, 'tp', neighbour)]
    ppermute x14, waiting for transfers between devices: 9.16 us -> 9.84 us  [the longest x1 5.52 us: local(): arrived[6] = lax.ppermute(arrived[7], 'tp', neighbour)]
  transfers between devices with their start and end apart: 22 -> 22, of which waited for: 8 -> 7; matrix products, arithmetic and copies ran while one was open for 0% -> 0% of each run, Pallas kernels for 7% -> 13%
where the time goes in v1:
time: 55.9 us; the launch traced here: 55.7 us
  starting transfers between devices  34.2 us (61%)
  waiting for transfers between devices  13.1 us (23%)
  Pallas kernels  8.24 us (15%)
    ppermute x12, starting transfers between devices, hop(): return lax.ppermute(block, ('ep', 'tp'), pairs)  24 us
    pallas_call x11, Pallas kernels, call(): pl.pallas_call(body, out_shape=outs, in_specs=[hbm if i in far else vmem...  8.24 us
    ppermute x1, waiting for transfers between devices, local(): arrived[6] = lax.ppermute(arrived[7], 'tp', neighbour)  5.52 us
    ppermute x3, starting transfers between devices, local(): came = lax.ppermute(send, 'tp', neighbour)  4.34 us
    ppermute x12, waiting for transfers between devices, hop(): return lax.ppermute(block, ('ep', 'tp'), pairs)  4.32 us
    ppermute x1, starting transfers between devices, local(): sh_came = lax.ppermute(sh_send, 'tp', neighbour)  2.75 us
    ppermute x3, waiting for transfers between devices, local(): came = lax.ppermute(send, 'tp', neighbour)  1.77 us
    ppermute x1, starting transfers between devices, local(): arrived[5] = lax.ppermute(arrived[4], 'tp', neighbour)  1.64 us
  transfers between devices with their start and end apart: 22, of which 7 were waited for; matrix products, arithmetic and copies ran while one was open for 0% of the time, Pallas kernels for 13%

profile of v1, /device:TPU:0, one launch (start us, length us, event | category | flops | bytes accessed | tf_op | source)
XLA Modules:
  0.0 55.7 jit_solution(17557742247805393227)
XLA Ops:
  0.0 0.5 collective-permute-start.3
  0.5 0.5 collective-permute-start.5
  1.0 1.9 %shard_map.100 = (bf16[128,2048]{1,0:T(8,128)(2,1)S(1)}, s32[2,128]{1,0:T(2,128)S(1)}, bf16[24,2048]{1,0:T(8,128)(2,1)S(1)}, bf16[24,2048]{1,0:T(8,128)(2,1)S(1)...) custom-call(s32[2,128]{1,0:T(2,128)} %bitcast.19, ...), custom_call_target="tpu_custom_call" | custom-call | flops 100663296 | bytes 1644544 | tf_op jit(solution)/shard_map/pallas_call | solution.py:25
  2.9 2.6 %collective-permute-start = (bf16[24,2048]{1,0:T(8,128)(2,1)S(1)}, bf16[24,2048]{1,0:T(8,128)(2,1)S(1)}, u32[]{:S(2)}, u32[]{:S(2)}) collective-permute-start(bf16[24,2048]{1,0:T(8,128)(2,1)S(1)} %get-tuple-element.37), channel_id=1, source_target_pairs={{0,4},{1,5},{2,6},{3,7},{4,0},{5,1},{6,2},{7,3},{8,12},{9,13},{10,... | collective-permute-start | bytes 294920 | tf_op jit(solution)/shard_map/ppermute | solution.py:233
  5.4 1.6 %collective-permute-start.1 = (bf16[24,2048]{1,0:T(8,128)(2,1)S(1)}, bf16[24,2048]{1,0:T(8,128)(2,1)S(1)}, u32[]{:S(2)}, u32[]{:S(2)}) collective-permute-start(bf16[24,2048]{1,0:T(8,128)(2,1)S(1)} %get-tuple-element.38), channel_id=1, source_target_pairs={{0,8},{1,9},{2,10},{3,11},{4,12},{5,13},{6,14},{7,15},{8,0},{9,1},... | collective-permute-start | bytes 294920 | tf_op jit(solution)/shard_map/ppermute | solution.py:233
  7.0 1.9 %collective-permute-done.refs_1_ = bf16[24,2048]{1,0:T(8,128)(2,1)S(1)} collective-permute-done((bf16[24,2048]{1,0:T(8,128)(2,1)S(1)}, bf16[24,2048]{1,0:T(8,128)(2,1)S(1)}, u32[]{:S(2)}, u32[]{:S(2)}) %collective-permute-start) | collective-permute-done | bytes 98336 | tf_op jit(solution)/shard_map/ppermute | solution.py:233
  8.9 2.8 %collective-permute-start.2 = (bf16[24,2048]{1,0:T(8,128)(2,1)S(1)}, bf16[24,2048]{1,0:T(8,128)(2,1)S(1)}, u32[]{:S(2)}, u32[]{:S(2)}) collective-permute-start(bf16[24,2048]{1,0:T(8,128)(2,1)S(1)} %get-tuple-element.39), channel_id=1, source_target_pairs={{0,12},{1,13},{2,14},{3,15},{4,8},{5,9},{6,10},{7,11},{8,4},{9,5},... | collective-permute-start | bytes 294920 | tf_op jit(solution)/shard_map/ppermute | solution.py:233
  11.7 2.4 %collective-permute-start.15 = (bf16[24,2048]{1,0:T(8,128)(2,1)S(1)}, bf16[24,2048]{1,0:T(8,128)(2,1)S(1)}, u32[]{:S(2)}, u32[]{:S(2)}) collective-permute-start(bf16[24,2048]{1,0:T(8,128)(2,1)S(1)} %get-tuple-element.51), channel_id=1, source_target_pairs={{0,28},{1,29},{2,26},{3,27},{4,24},{5,25},{6,30},{7,31},{8,20},{9,... | collective-permute-start | bytes 294920 | tf_op jit(solution)/shard_map/ppermute | solution.py:233
  14.1 0.4 collective-permute-done.2.refs_3_
  14.4 3.4 %collective-permute-start.10 = (bf16[24,2048]{1,0:T(8,128)(2,1)S(1)}, bf16[24,2048]{1,0:T(8,128)(2,1)S(1)}, u32[]{:S(2)}, u32[]{:S(2)}) collective-permute-start(bf16[24,2048]{1,0:T(8,128)(2,1)S(1)} %get-tuple-element.46), channel_id=1, source_target_pairs={{0,16},{1,17},{2,22},{3,23},{4,20},{5,21},{6,18},{7,19},{8,24},{9,... | collective-permute-start | bytes 294920 | tf_op jit(solution)/shard_map/ppermute | solution.py:233
  17.8 2.3 %shard_map.108 = (bf16[128,1024]{1,0:T(8,128)(2,1)S(1)}, f32[128,1024]{1,0:T(8,128)S(1)}) custom-call(bf16[128,2048]{1,0:T(8,128)(2,1)S(1)} %get-tuple-element.56.refs_0_, bf16[2048,128]{1,0:T(8,128)(2,1)} %refs_1_.1, bf16[2048,128]{1,0:T(8,128)(2,1)} %refs_2_.1, bf16[128,2048]{1,0:T(8,128)(2,1)} %refs_3_.1), custom_call_target="tpu_custom_call" | custom-call | flops 201326592 | bytes 2883584 | tf_op jit(solution)/shard_map/pallas_call | solution.py:25
  20.1 2.8 %collective-permute-start.20 = (bf16[128,1024]{1,0:T(8,128)(2,1)S(1)}, bf16[128,1024]{1,0:T(8,128)(2,1)S(1)}, u32[]{:S(2)}, u32[]{:S(2)}) collective-permute-start(bf16[128,1024]{1,0:T(8,128)(2,1)S(1)} %get-tuple-element.58), channel_id=1, source_target_pairs={{0,2},{1,3},{2,0},{3,1},{4,6},{5,7},{6,4},{7,5},{8,10},{9,11},{10,... | collective-permute-start | bytes 786440 | tf_op jit(solution)/shard_map/ppermute | solution.py:252
  22.9 0.4 collective-permute-start.16
  23.3 1.6 %collective-permute-start.11 = (bf16[24,2048]{1,0:T(8,128)(2,1)S(1)}, bf16[24,2048]{1,0:T(8,128)(2,1)S(1)}, u32[]{:S(2)}, u32[]{:S(2)}) collective-permute-start(bf16[24,2048]{1,0:T(8,128)(2,1)S(1)} %collective-permute-done.10.refs_0_), channel_id=1, source_target_pairs={{0,2},{1,3},{2,0},{3,1},{4,6},{5,7},{6,4},{7,5},{8,10},{9,11},{10,... | collective-permute-start | bytes 294920 | tf_op jit(solution)/shard_map/ppermute | solution.py:249
  25.0 0.7 %shard_map.102 = (bf16[96,1024]{1,0:T(8,128)(2,1)S(1)}, f32[96,1024]{1,0:T(8,128)S(1)}) custom-call(bf16[24,2048]{1,0:T(8,128)(2,1)S(1)} %get-tuple-element.36.refs_0_, bf16[24,2048]{1,0:T(8,128)(2,1)S(1)} %collective-permute-done.refs_1_, bf16[24,2048]{1,0:T(8,128)(2,1)S(1)} %collective-permute-done.1.refs_2_, ...), custom_call_target="tpu_custom_call" | custom-call | flops 301989888 | bytes 4128768 | tf_op jit(solution)/shard_map/pallas_call | solution.py:25
  25.7 0.5 collective-permute-start.6
  26.2 5.5 %collective-permute-done.16.refs_0_ = bf16[24,2048]{1,0:T(8,128)(2,1)S(1)} collective-permute-done((bf16[24,2048]{1,0:T(8,128)(2,1)S(1)}, bf16[24,2048]{1,0:T(8,128)(2,1)S(1)}, u32[]{:S(2)}, u32[]{:S(2)}) %collective-permute-start.16) | collective-permute-done | bytes 98336 | tf_op jit(solution)/shard_map/ppermute | solution.py:250
  31.7 0.7 %shard_map.106 = (bf16[48,1024]{1,0:T(8,128)(2,1)S(1)}, f32[48,1024]{1,0:T(8,128)S(1)}) custom-call(bf16[24,2048]{1,0:T(8,128)(2,1)S(1)} %collective-permute-done.16.refs_0_, bf16[24,2048]{1,0:T(8,128)(2,1)S(1)} %collective-permute-done.15.refs_1_, bf16[2048,128]{1,0:T(8,128)(2,1)S(1)} %bitcast.8, bf16[2048,128]{1,0:T(8,128)(2,1)S(1)} %bitcast.12, ...), custom_call_target="tpu_custom_call" | custom-call | flops 150994944 | bytes 3637248 | tf_op jit(solution)/shard_map/pallas_call | solution.py:25
  32.4 2.5 %collective-permute-start.17 = (bf16[48,1024]{1,0:T(8,128)(2,1)S(1)}, bf16[48,1024]{1,0:T(8,128)(2,1)S(1)}, u32[]{:S(2)}, u32[]{:S(2)}) collective-permute-start(bf16[48,1024]{1,0:T(8,128)(2,1)S(1)} %get-tuple-element.53), channel_id=1, source_target_pairs={{0,2},{1,3},{2,0},{3,1},{4,6},{5,7},{6,4},{7,5},{8,10},{9,11},{10,... | collective-permute-start | bytes 294920 | tf_op jit(solution)/shard_map/ppermute | solution.py:267
  34.9 0.7 %shard_map.104 = (bf16[48,1024]{1,0:T(8,128)(2,1)S(1)}, f32[48,1024]{1,0:T(8,128)S(1)}) custom-call(bf16[24,2048]{1,0:T(8,128)(2,1)S(1)} %collective-permute-done.10.refs_0_, bf16[24,2048]{1,0:T(8,128)(2,1)S(1)} %collective-permute-done.11.refs_1_, bf16[2048,128]{1,0:T(8,128)(2,1)S(1)} %bitcast.9, bf16[2048,128]{1,0:T(8,128)(2,1)S(1)} %bitcast.13, ...), custom_call_target="tpu_custom_call" | custom-call | flops 150994944 | bytes 3637248 | tf_op jit(solution)/shard_map/pallas_call | solution.py:25
  35.7 1.4 %collective-permute-start.12 = (bf16[48,1024]{1,0:T(8,128)(2,1)S(1)}, bf16[48,1024]{1,0:T(8,128)(2,1)S(1)}, u32[]{:S(2)}, u32[]{:S(2)}) collective-permute-start(bf16[48,1024]{1,0:T(8,128)(2,1)S(1)} %get-tuple-element.48), channel_id=1, source_target_pairs={{0,2},{1,3},{2,0},{3,1},{4,6},{5,7},{6,4},{7,5},{8,10},{9,11},{10,... | collective-permute-start | bytes 294920 | tf_op jit(solution)/shard_map/ppermute | solution.py:267
  37.1 1.8 %collective-permute-done.17.came = bf16[48,1024]{1,0:T(8,128)(2,1)S(1)} collective-permute-done((bf16[48,1024]{1,0:T(8,128)(2,1)S(1)}, bf16[48,1024]{1,0:T(8,128)(2,1)S(1)}, u32[]{:S(2)}, u32[]{:S(2)}) %collective-permute-start.17) | collective-permute-done | bytes 98336 | tf_op jit(solution)/shard_map/ppermute | solution.py:267
  38.8 1.1 %collective-permute-start.18 = (bf16[24,1024]{1,0:T(8,128)(2,1)S(1)}, bf16[24,1024]{1,0:T(8,128)(2,1)S(1)}, u32[]{:S(2)}, u32[]{:S(2)}) collective-permute-start(bf16[24,1024]{1,0:T(8,128)(2,1)S(1)} %get-tuple-element.54), channel_id=1, source_target_pairs={{0,24},{1,25},{2,30},{3,31},{4,28},{5,29},{6,26},{7,27},{8,16},{9,... | collective-permute-start | bytes 147464 | tf_op jit(solution)/shard_map/ppermute | solution.py:233
  40.0 3.5 %collective-permute-start.19 = (bf16[24,1024]{1,0:T(8,128)(2,1)S(1)}, bf16[24,1024]{1,0:T(8,128)(2,1)S(1)}, u32[]{:S(2)}, u32[]{:S(2)}) collective-permute-start(bf16[24,1024]{1,0:T(8,128)(2,1)S(1)} %get-tuple-element.55), channel_id=1, source_target_pairs={{0,28},{1,29},{2,26},{3,27},{4,24},{5,25},{6,30},{7,31},{8,20},{9,... | collective-permute-start | bytes 147464 | tf_op jit(solution)/shard_map/ppermute | solution.py:233
  43.6 3.1 %collective-permute-start.14 = (bf16[24,1024]{1,0:T(8,128)(2,1)S(1)}, bf16[24,1024]{1,0:T(8,128)(2,1)S(1)}, u32[]{:S(2)}, u32[]{:S(2)}) collective-permute-start(bf16[24,1024]{1,0:T(8,128)(2,1)S(1)} %get-tuple-element.50), channel_id=1, source_target_pairs={{0,20},{1,21},{2,18},{3,19},{4,16},{5,17},{6,22},{7,23},{8,28},{9,... | collective-permute-start | bytes 147464 | tf_op jit(solution)/shard_map/ppermute | solution.py:233
  46.7 1.4 %collective-permute-start.7 = (bf16[24,1024]{1,0:T(8,128)(2,1)S(1)}, bf16[24,1024]{1,0:T(8,128)(2,1)S(1)}, u32[]{:S(2)}, u32[]{:S(2)}) collective-permute-start(bf16[24,1024]{1,0:T(8,128)(2,1)S(1)} %get-tuple-element.43), channel_id=1, source_target_pairs={{0,4},{1,5},{2,6},{3,7},{4,0},{5,1},{6,2},{7,3},{8,12},{9,13},{10,... | collective-permute-start | bytes 147464 | tf_op jit(solution)/shard_map/ppermute | solution.py:233
  48.1 2.2 %collective-permute-start.9 = (bf16[24,1024]{1,0:T(8,128)(2,1)S(1)}, bf16[24,1024]{1,0:T(8,128)(2,1)S(1)}, u32[]{:S(2)}, u32[]{:S(2)}) collective-permute-start(bf16[24,1024]{1,0:T(8,128)(2,1)S(1)} %get-tuple-element.45), channel_id=1, source_target_pairs={{0,12},{1,13},{2,14},{3,15},{4,8},{5,9},{6,10},{7,11},{8,4},{9,5},... | collective-permute-start | bytes 147464 | tf_op jit(solution)/shard_map/ppermute | solution.py:233
  50.3 0.8 %shard_map.101 = (bf16[128,192]{1,0:T(8,128)(2,1)S(1)}, bf16[128,192]{1,0:T(8,128)(2,1)S(1)}) custom-call(s32[2,128]{1,0:T(2,128)S(1)} %get-tuple-element.33.slots, f32[2,128]{1,0:T(2,128)} %bitcast.20), custom_call_target="tpu_custom_call" | custom-call | flops 24576 | bytes 100352 | tf_op jit(solution)/shard_map/pallas_call | solution.py:25
  51.1 1.1 %collective-permute-done.8.refs_2_ = bf16[24,1024]{1,0:T(8,128)(2,1)S(1)} collective-permute-done((bf16[24,1024]{1,0:T(8,128)(2,1)S(1)}, bf16[24,1024]{1,0:T(8,128)(2,1)S(1)}, u32[]{:S(2)}, u32[]{:S(2)}) %collective-permute-start.8) | collective-permute-done | bytes 49184 | tf_op jit(solution)/shard_map/ppermute | solution.py:233
  52.1 1.0 %collective-permute-done.9.refs_3_ = bf16[24,1024]{1,0:T(8,128)(2,1)S(1)} collective-permute-done((bf16[24,1024]{1,0:T(8,128)(2,1)S(1)}, bf16[24,1024]{1,0:T(8,128)(2,1)S(1)}, u32[]{:S(2)}, u32[]{:S(2)}) %collective-permute-start.9) | collective-permute-done | bytes 49184 | tf_op jit(solution)/shard_map/ppermute | solution.py:233
  53.5 1.5 %collective-permute-done.21.came = f32[128,512]{1,0:T(8,128)S(1)} collective-permute-done((f32[128,512]{1,0:T(8,128)S(1)}, f32[128,512]{1,0:T(8,128)S(1)}, u32[]{:S(2)}, u32[]{:S(2)}) %collective-permute-start.21) | collective-permute-done | bytes 262176 | tf_op jit(solution)/shard_map/ppermute | solution.py:279
  55.1 0.7 %shard_map.110 = bf16[128,512]{1,0:T(8,128)(2,1)} custom-call(f32[128,512]{1,0:T(8,128)S(1)} %get-tuple-element.59.keep, f32[128,512]{1,0:T(8,128)S(1)} %collective-permute-done.21.came), custom_call_target="tpu_custom_call" | custom-call | flops 65536 | bytes 655360 | tf_op jit(solution)/shard_map/pallas_call | solution.py:25
  (29 shorter events, 0.6 us)
Async XLA Ops:
  0.0 23.3 %collective-permute-start.3 = (bf16[2048,128]{1,0:T(8,128)(2,1)}, bf16[2048,128]{1,0:T(8,128)(2,1)S(1)}, u32[]{:S(2)}, u32[]{:S(2)}) collective-permute-start(bf16[2048,128]{1,0:T(8,128)(2,1)} %bitcast.6), channel_id=1, source_target_pairs={{0,1},{1,0},{2,3},{3,2},{4,5},{5,4},{6,7},{7,6},{8,9},{9,8},{10,11... | collective-permute-start | bytes 1572872 | tf_op jit(solution)/shard_map/ppermute | solution.py:221
  0.5 24.4 %collective-permute-start.4 = (bf16[2048,128]{1,0:T(8,128)(2,1)}, bf16[2048,128]{1,0:T(8,128)(2,1)S(1)}, u32[]{:S(2)}, u32[]{:S(2)}) collective-permute-start(bf16[2048,128]{1,0:T(8,128)(2,1)} %bitcast.10), channel_id=1, source_target_pairs={{0,1},{1,0},{2,3},{3,2},{4,5},{5,4},{6,7},{7,6},{8,9},{9,8},{10,11... | collective-permute-start | bytes 1572872 | tf_op jit(solution)/shard_map/ppermute | solution.py:221
  0.5 24.4 %collective-permute-start.5 = (bf16[128,2048]{1,0:T(8,128)(2,1)}, bf16[128,2048]{1,0:T(8,128)(2,1)S(1)}, u32[]{:S(2)}, u32[]{:S(2)}) collective-permute-start(bf16[128,2048]{1,0:T(8,128)(2,1)} %bitcast.14), channel_id=1, source_target_pairs={{0,1},{1,0},{2,3},{3,2},{4,5},{5,4},{6,7},{7,6},{8,9},{9,8},{10,11... | collective-permute-start | bytes 1572872 | tf_op jit(solution)/shard_map/ppermute | solution.py:221
  2.9 6.0 %collective-permute-start = (bf16[24,2048]{1,0:T(8,128)(2,1)S(1)}, bf16[24,2048]{1,0:T(8,128)(2,1)S(1)}, u32[]{:S(2)}, u32[]{:S(2)}) collective-permute-start(bf16[24,2048]{1,0:T(8,128)(2,1)S(1)} %get-tuple-element.37), channel_id=1, source_target_pairs={{0,4},{1,5},{2,6},{3,7},{4,0},{5,1},{6,2},{7,3},{8,12},{9,13},{10,... | collective-permute-start | bytes 294920 | tf_op jit(solution)/shard_map/ppermute | solution.py:233
  5.4 6.2 %collective-permute-start.1 = (bf16[24,2048]{1,0:T(8,128)(2,1)S(1)}, bf16[24,2048]{1,0:T(8,128)(2,1)S(1)}, u32[]{:S(2)}, u32[]{:S(2)}) collective-permute-start(bf16[24,2048]{1,0:T(8,128)(2,1)S(1)} %get-tuple-element.38), channel_id=1, source_target_pairs={{0,8},{1,9},{2,10},{3,11},{4,12},{5,13},{6,14},{7,15},{8,0},{9,1},... | collective-permute-start | bytes 294920 | tf_op jit(solution)/shard_map/ppermute | solution.py:233
  8.9 5.5 %collective-permute-start.2 = (bf16[24,2048]{1,0:T(8,128)(2,1)S(1)}, bf16[24,2048]{1,0:T(8,128)(2,1)S(1)}, u32[]{:S(2)}, u32[]{:S(2)}) collective-permute-start(bf16[24,2048]{1,0:T(8,128)(2,1)S(1)} %get-tuple-element.39), channel_id=1, source_target_pairs={{0,12},{1,13},{2,14},{3,15},{4,8},{5,9},{6,10},{7,11},{8,4},{9,5},... | collective-permute-start | bytes 294920 | tf_op jit(solution)/shard_map/ppermute | solution.py:233
  11.7 8.4 %collective-permute-start.15 = (bf16[24,2048]{1,0:T(8,128)(2,1)S(1)}, bf16[24,2048]{1,0:T(8,128)(2,1)S(1)}, u32[]{:S(2)}, u32[]{:S(2)}) collective-permute-start(bf16[24,2048]{1,0:T(8,128)(2,1)S(1)} %get-tuple-element.51), channel_id=1, source_target_pairs={{0,28},{1,29},{2,26},{3,27},{4,24},{5,25},{6,30},{7,31},{8,20},{9,... | collective-permute-start | bytes 294920 | tf_op jit(solution)/shard_map/ppermute | solution.py:233
  14.4 8.5 %collective-permute-start.10 = (bf16[24,2048]{1,0:T(8,128)(2,1)S(1)}, bf16[24,2048]{1,0:T(8,128)(2,1)S(1)}, u32[]{:S(2)}, u32[]{:S(2)}) collective-permute-start(bf16[24,2048]{1,0:T(8,128)(2,1)S(1)} %get-tuple-element.46), channel_id=1, source_target_pairs={{0,16},{1,17},{2,22},{3,23},{4,20},{5,21},{6,18},{7,19},{8,24},{9,... | collective-permute-start | bytes 294920 | tf_op jit(solution)/shard_map/ppermute | solution.py:233
  17.8 7.1 %copy-start = (bf16[1,2048,128]{2,1,0:T(8,128)(2,1)S(1)}, bf16[1,2048,128]{2,1,0:T(8,128)(2,1)}, u32[]{:S(2)}) copy-start(bf16[1,2048,128]{2,1,0:T(8,128)(2,1)} %param.14) | copy-start | bytes 1572868
  17.8 7.1 %copy-start.1 = (bf16[1,2048,128]{2,1,0:T(8,128)(2,1)S(1)}, bf16[1,2048,128]{2,1,0:T(8,128)(2,1)}, u32[]{:S(2)}) copy-start(bf16[1,2048,128]{2,1,0:T(8,128)(2,1)} %param.15) | copy-start | bytes 1572868
  17.8 7.1 %copy-start.2 = (bf16[1,128,2048]{2,1,0:T(8,128)(2,1)S(1)}, bf16[1,128,2048]{2,1,0:T(8,128)(2,1)}, u32[]{:S(2)}) copy-start(bf16[1,128,2048]{2,1,0:T(8,128)(2,1)} %param.16) | copy-start | bytes 1572868
  20.1 26.6 %collective-permute-start.20 = (bf16[128,1024]{1,0:T(8,128)(2,1)S(1)}, bf16[128,1024]{1,0:T(8,128)(2,1)S(1)}, u32[]{:S(2)}, u32[]{:S(2)}) collective-permute-start(bf16[128,1024]{1,0:T(8,128)(2,1)S(1)} %get-tuple-element.58), channel_id=1, source_target_pairs={{0,2},{1,3},{2,0},{3,1},{4,6},{5,7},{6,4},{7,5},{8,10},{9,11},{10,... | collective-permute-start | bytes 786440 | tf_op jit(solution)/shard_map/ppermute | solution.py:252
  22.9 8.8 %collective-permute-start.16 = (bf16[24,2048]{1,0:T(8,128)(2,1)S(1)}, bf16[24,2048]{1,0:T(8,128)(2,1)S(1)}, u32[]{:S(2)}, u32[]{:S(2)}) collective-permute-start(bf16[24,2048]{1,0:T(8,128)(2,1)S(1)} %collective-permute-done.15.refs_1_), channel_id=1, source_target_pairs={{0,2},{1,3},{2,0},{3,1},{4,6},{5,7},{6,4},{7,5},{8,10},{9,11},{10,... | collective-permute-start | bytes 294920 | tf_op jit(solution)/shard_map/ppermute | solution.py:250
  23.3 11.7 %collective-permute-start.11 = (bf16[24,2048]{1,0:T(8,128)(2,1)S(1)}, bf16[24,2048]{1,0:T(8,128)(2,1)S(1)}, u32[]{:S(2)}, u32[]{:S(2)}) collective-permute-start(bf16[24,2048]{1,0:T(8,128)(2,1)S(1)} %collective-permute-done.10.refs_0_), channel_id=1, source_target_pairs={{0,2},{1,3},{2,0},{3,1},{4,6},{5,7},{6,4},{7,5},{8,10},{9,11},{10,... | collective-permute-start | bytes 294920 | tf_op jit(solution)/shard_map/ppermute | solution.py:249
  25.7 17.9 %collective-permute-start.6 = (bf16[96,1024]{1,0:T(8,128)(2,1)S(1)}, bf16[96,1024]{1,0:T(8,128)(2,1)S(1)}, u32[]{:S(2)}, u32[]{:S(2)}) collective-permute-start(bf16[96,1024]{1,0:T(8,128)(2,1)S(1)} %get-tuple-element.41), channel_id=1, source_target_pairs={{0,2},{1,3},{2,0},{3,1},{4,6},{5,7},{6,4},{7,5},{8,10},{9,11},{10,... | collective-permute-start | bytes 589832 | tf_op jit(solution)/shard_map/ppermute | solution.py:267
  32.4 6.4 %collective-permute-start.17 = (bf16[48,1024]{1,0:T(8,128)(2,1)S(1)}, bf16[48,1024]{1,0:T(8,128)(2,1)S(1)}, u32[]{:S(2)}, u32[]{:S(2)}) collective-permute-start(bf16[48,1024]{1,0:T(8,128)(2,1)S(1)} %get-tuple-element.53), channel_id=1, source_target_pairs={{0,2},{1,3},{2,0},{3,1},{4,6},{5,7},{6,4},{7,5},{8,10},{9,11},{10,... | collective-permute-start | bytes 294920 | tf_op jit(solution)/shard_map/ppermute | solution.py:267
  35.7 7.8 %collective-permute-start.12 = (bf16[48,1024]{1,0:T(8,128)(2,1)S(1)}, bf16[48,1024]{1,0:T(8,128)(2,1)S(1)}, u32[]{:S(2)}, u32[]{:S(2)}) collective-permute-start(bf16[48,1024]{1,0:T(8,128)(2,1)S(1)} %get-tuple-element.48), channel_id=1, source_target_pairs={{0,2},{1,3},{2,0},{3,1},{4,6},{5,7},{6,4},{7,5},{8,10},{9,11},{10,... | collective-permute-start | bytes 294920 | tf_op jit(solution)/shard_map/ppermute | solution.py:267
  38.8 9.2 %collective-permute-start.18 = (bf16[24,1024]{1,0:T(8,128)(2,1)S(1)}, bf16[24,1024]{1,0:T(8,128)(2,1)S(1)}, u32[]{:S(2)}, u32[]{:S(2)}) collective-permute-start(bf16[24,1024]{1,0:T(8,128)(2,1)S(1)} %get-tuple-element.54), channel_id=1, source_target_pairs={{0,24},{1,25},{2,30},{3,31},{4,28},{5,29},{6,26},{7,27},{8,16},{9,... | collective-permute-start | bytes 147464 | tf_op jit(solution)/shard_map/ppermute | solution.py:233
  40.0 8.1 %collective-permute-start.19 = (bf16[24,1024]{1,0:T(8,128)(2,1)S(1)}, bf16[24,1024]{1,0:T(8,128)(2,1)S(1)}, u32[]{:S(2)}, u32[]{:S(2)}) collective-permute-start(bf16[24,1024]{1,0:T(8,128)(2,1)S(1)} %get-tuple-element.55), channel_id=1, source_target_pairs={{0,28},{1,29},{2,26},{3,27},{4,24},{5,25},{6,30},{7,31},{8,20},{9,... | collective-permute-start | bytes 147464 | tf_op jit(solution)/shard_map/ppermute | solution.py:233
  43.5 7.6 %collective-permute-start.13 = (bf16[24,1024]{1,0:T(8,128)(2,1)S(1)}, bf16[24,1024]{1,0:T(8,128)(2,1)S(1)}, u32[]{:S(2)}, u32[]{:S(2)}) collective-permute-start(bf16[24,1024]{1,0:T(8,128)(2,1)S(1)} %get-tuple-element.49), channel_id=1, source_target_pairs={{0,16},{1,17},{2,22},{3,23},{4,20},{5,21},{6,18},{7,19},{8,24},{9,... | collective-permute-start | bytes 147464 | tf_op jit(solution)/shard_map/ppermute | solution.py:233
  43.6 7.5 %collective-permute-start.14 = (bf16[24,1024]{1,0:T(8,128)(2,1)S(1)}, bf16[24,1024]{1,0:T(8,128)(2,1)S(1)}, u32[]{:S(2)}, u32[]{:S(2)}) collective-permute-start(bf16[24,1024]{1,0:T(8,128)(2,1)S(1)} %get-tuple-element.50), channel_id=1, source_target_pairs={{0,20},{1,21},{2,18},{3,19},{4,16},{5,17},{6,22},{7,23},{8,28},{9,... | collective-permute-start | bytes 147464 | tf_op jit(solution)/shard_map/ppermute | solution.py:233
  46.7 4.4 %collective-permute-start.7 = (bf16[24,1024]{1,0:T(8,128)(2,1)S(1)}, bf16[24,1024]{1,0:T(8,128)(2,1)S(1)}, u32[]{:S(2)}, u32[]{:S(2)}) collective-permute-start(bf16[24,1024]{1,0:T(8,128)(2,1)S(1)} %get-tuple-element.43), channel_id=1, source_target_pairs={{0,4},{1,5},{2,6},{3,7},{4,0},{5,1},{6,2},{7,3},{8,12},{9,13},{10,... | collective-permute-start | bytes 147464 | tf_op jit(solution)/shard_map/ppermute | solution.py:233
  48.1 4.1 %collective-permute-start.8 = (bf16[24,1024]{1,0:T(8,128)(2,1)S(1)}, bf16[24,1024]{1,0:T(8,128)(2,1)S(1)}, u32[]{:S(2)}, u32[]{:S(2)}) collective-permute-start(bf16[24,1024]{1,0:T(8,128)(2,1)S(1)} %get-tuple-element.44), channel_id=1, source_target_pairs={{0,8},{1,9},{2,10},{3,11},{4,12},{5,13},{6,14},{7,15},{8,0},{9,1},... | collective-permute-start | bytes 147464 | tf_op jit(solution)/shard_map/ppermute | solution.py:233
  48.1 5.1 %collective-permute-start.9 = (bf16[24,1024]{1,0:T(8,128)(2,1)S(1)}, bf16[24,1024]{1,0:T(8,128)(2,1)S(1)}, u32[]{:S(2)}, u32[]{:S(2)}) collective-permute-start(bf16[24,1024]{1,0:T(8,128)(2,1)S(1)} %get-tuple-element.45), channel_id=1, source_target_pairs={{0,12},{1,13},{2,14},{3,15},{4,8},{5,9},{6,10},{7,11},{8,4},{9,5},... | collective-permute-start | bytes 147464 | tf_op jit(solution)/shard_map/ppermute | solution.py:233
  53.5 1.6 %collective-permute-start.21 = (f32[128,512]{1,0:T(8,128)S(1)}, f32[128,512]{1,0:T(8,128)S(1)}, u32[]{:S(2)}, u32[]{:S(2)}) collective-permute-start(f32[128,512]{1,0:T(8,128)S(1)} %get-tuple-element.60), channel_id=1, source_target_pairs={{0,1},{1,0},{2,3},{3,2},{4,5},{5,4},{6,7},{7,6},{8,9},{9,8},{10,11... | collective-permute-start | bytes 786440 | tf_op jit(solution)/shard_map/ppermute | solution.py:279

commit v2 on v1

v2 whole, which is shorter than its diff:
```python
import functools

import jax
import jax.numpy as jnp
from jax import lax
from jax.experimental import pallas as pl
from jax.experimental.pallas import tpu as pltpu
from jax.sharding import PartitionSpec as P

norm_eps = 1e-06
grant = 16 * 1024 * 1024
f32 = jnp.float32
bf16 = jnp.bfloat16

vmem = pl.BlockSpec(memory_space=pltpu.VMEM)
hbm = pl.BlockSpec(memory_space=pltpu.HBM)


def call(body, outs, ins, flops, scratch=(), far=()):
    moved = sum(a.size * a.dtype.itemsize for a in ins)
    moved += sum(o.size * o.dtype.itemsize for o in outs)
    ins = [
        pltpu.with_memory_space_constraint(a, pltpu.HBM) if i in far else a for i, a in enumerate(ins)
    ]
    return pl.pallas_call(
        body,
        out_shape=outs,
        in_specs=[hbm if i in far else vmem for i in range(len(ins))],
        out_specs=[vmem] * len(outs),
        scratch_shapes=list(scratch),
        compiler_params=pltpu.CompilerParams(vmem_limit_bytes=grant),
        cost_estimate=pl.CostEstimate(flops=flops, bytes_accessed=moved, transcendentals=0),
    )(*ins)


def landing(arrays):
    return [pltpu.VMEM(a.shape, a.dtype) for a in arrays] + [pltpu.SemaphoreType.DMA((len(arrays),))]


def fetch(sources, targets, sems):
    copies = [
        pltpu.make_async_copy(s, t, sems.at[i]) for i, (s, t) in enumerate(zip(sources, targets))
    ]
    for copy in copies:
        copy.start()
    return copies


def shape(rows, columns, dtype):
    return jax.ShapeDtypeStruct((rows, columns), dtype)


def slot_of(label, rank, capacity, direct):
    core, side = lax.axis_index("tp") % 2, lax.axis_index("tp") // 2
    if direct:
        near = label < 4
        holder = jnp.where(near, (label ^ (label >> 1)) & 1, (label >> 1) & 1)
        first = jnp.where((label ^ side) == 4 + 3 * core, 2, 3)
        block = jnp.where(near, label >> 1, first)
        return jnp.where(holder == core, block * capacity + rank, -1)
    half = -(-capacity // 2)
    rank = rank - core * half
    held = jnp.logical_and(rank >= 0, rank < half)
    return jnp.where(held, label * half + rank, -1)


def route_body(capacity, experts, direct, ids_in, gain_in, tokens_in, *refs):
    outs, (ids, gain, tokens, sems) = refs[:-4], refs[-4:]
    copies = fetch((ids_in, gain_in, tokens_in), (ids, gain, tokens), sems)
    normed_out, slots_out = outs[0], outs[1]
    rows, width = tokens.shape
    kinds = max(8, experts)
    kind = lax.broadcasted_iota(jnp.int32, (kinds, rows), 0)
    before = (
        lax.broadcasted_iota(jnp.int32, (rows, rows), 0)
        < lax.broadcasted_iota(jnp.int32, (rows, rows), 1)
    ).astype(bf16)
    base = jnp.zeros((kinds, 1), f32)
    total = sum(out.shape[0] for out in outs[2:])
    slot = lax.broadcasted_iota(jnp.int32, (total, rows), 0)
    hit = jnp.zeros((total, rows), f32)
    copies[0].wait()
    for j in range(ids.shape[0]):
        label = ids[j : j + 1, :]
        if direct:
            label = label ^ lax.axis_index("ep")
        onehot = (kind == label).astype(f32)
        earlier = jnp.dot(onehot.astype(bf16), before, preferred_element_type=f32) + base
        rank = jnp.sum(earlier * onehot, axis=0, keepdims=True).astype(jnp.int32)
        base = base + jnp.sum(onehot, axis=1, keepdims=True)
        where = slot_of(label, rank, capacity, direct)
        slots_out[j : j + 1, :] = where
        hit = jnp.where(slot == where, 1.0, hit)
    pick = hit.astype(bf16)
    copies[1].wait()
    copies[2].wait()
    values = tokens[...].astype(f32)
    scale = lax.rsqrt(jnp.mean(values * values, axis=-1, keepdims=True) + norm_eps)
    lanes = gain.shape[1]
    for c in range(width // lanes):
        at = slice(c * lanes, (c + 1) * lanes)
        normed_out[:, at] = (values[:, at] * scale * gain[c : c + 1].astype(f32)).astype(bf16)
    normed = normed_out[...]
    at = 0
    for out in outs[2:]:
        n = out.shape[0]
        part = pick[at : at + n]
        out[...] = jnp.dot(part, normed, preferred_element_type=f32).astype(bf16)
        at += n


def units_of(rows, weights):
    into = [w[...] for w in weights[::3]] + [w[...] for w in weights[1::3]]
    both = jnp.dot(rows, jnp.concatenate(into, axis=1), preferred_element_type=f32)
    units = both.shape[1] // 2
    gate, up = both[:, :units], both[:, units:]
    return (gate / (1.0 + jnp.exp(-gate)) * up).astype(bf16)


def shared_body(slots, rows, gains_in, *refs):
    weights_in, (send, keep, high_out, low_out) = refs[:3], refs[3:7]
    gains, weights, sems = refs[7], refs[8:11], refs[11]
    copies = fetch((gains_in, *weights_in), (gains, *weights), sems)
    slot = lax.broadcasted_iota(jnp.int32, high_out.shape[::-1], 0)
    weight = jnp.zeros(slot.shape, f32)
    copies[0].wait()
    for j in range(slots.shape[0]):
        weight = jnp.where(slot == slots[j : j + 1, :], gains[j : j + 1, :], weight)
    weight = weight.T
    high = weight.astype(bf16)
    high_out[...] = high
    low_out[...] = (weight - high.astype(f32)).astype(bf16)
    for copy in copies[1:]:
        copy.wait()
    columns_out(units_of(rows[...], weights), weights, send, keep)


def columns_out(hidden, weights, send, keep):
    side = lax.axis_index("tp") // 2
    width = keep.shape[1]
    for out, place in ((send, 1 - side), (keep, side)):
        columns = pl.ds(pl.multiple_of(place * width, width), width)
        down = jnp.concatenate([w[:, columns] for w in weights[2::3]], axis=0)
        out[...] = jnp.dot(hidden, down, preferred_element_type=f32).astype(out.dtype)


def product_body(blocks, *refs):
    rows_in, weights = refs[:blocks], refs[blocks : blocks + 6]
    send, keep = refs[blocks + 6 : blocks + 8]
    gathered = rows_in[0]
    if blocks > 1:
        gathered = refs[-1]
        at = 0
        for ref in rows_in:
            gathered[at : at + ref.shape[0]] = ref[...]
            at += ref.shape[0]
    columns_out(units_of(gathered[...], weights), weights, send, keep)


def products(rows, weights, width):
    n = sum(r.shape[0] for r in rows)
    full = rows[0].shape[1]
    hidden = sum(w.shape[1] for w in weights[::3])
    return call(
        functools.partial(product_body, len(rows)),
        [shape(n, width, bf16), shape(n, width, f32)],
        [*rows, *weights],
        6 * n * full * hidden,
        [pltpu.VMEM((n, full), bf16)] if len(rows) > 1 else [],
    )


def add_body(keep, came, *outs):
    at = 0
    for out in outs:
        n = out.shape[0]
        out[...] = (keep[at : at + n] + came[at : at + n].astype(f32)).astype(out.dtype)
        at += n


def mix_body(blocks, high, low, *refs):
    rows_in, adds, outs = refs[:blocks], refs[blocks:-3], refs[-3:-1]
    gathered = refs[-1]
    at = 0
    for ref in rows_in:
        gathered[at : at + ref.shape[0]] = ref[...]
        at += ref.shape[0]
    width = outs[0].shape[1]
    core = lax.axis_index("tp") % 2
    for out, place in ((outs[0], core), (outs[1], 1 - core)):
        columns = pl.ds(pl.multiple_of(place * width, width), width)
        rows = gathered[:, columns]
        total = sum(a[:, columns].astype(f32) for a in adds)
        total += jnp.dot(high[...], rows, preferred_element_type=f32)
        out[...] = total + jnp.dot(low[...], rows, preferred_element_type=f32)


def local(
    tokens,
    norm_gain,
    expert_ids,
    route_weights,
    gate_weight,
    up_weight,
    down_weight,
    shared_gate,
    shared_up,
    shared_down,
):
    rows_here, width = tokens.shape
    chosen = expert_ids.shape[1]
    groups = lax.axis_size("ep")
    cuts = lax.axis_size("tp")
    local_experts = gate_weight.shape[0]
    assert local_experts == 1 and cuts == 4
    capacity = (3 * rows_here * chosen + 2 * groups - 1) // (2 * groups)
    wide, share = width // 2, width // 4
    direct = groups == 8
    sibling = [(i, i ^ 1) for i in range(cuts)]
    neighbour = [(i, i ^ 2) for i in range(cuts)]
    own = (gate_weight[0], up_weight[0], down_weight[0])
    other = tuple(lax.ppermute(w, "tp", sibling) for w in own)

    def hop(block, between):
        if not direct:
            return lax.all_to_all(block, "ep", split_axis=0, concat_axis=0, tiled=True)
        pairs = []
        for i in range(groups):
            for t in range(cuts):
                pairs.append((i * cuts + t, (i ^ between(t // 2, t % 2)) * cuts + t))
        return lax.ppermute(block, ("ep", "tp"), pairs)

    distances = {
        "P": lambda x, c: c,
        "Q": lambda x, c: 3 - c,
        "A": lambda x, c: (4 + 3 * c) ^ x,
        "B": lambda x, c: (4 + 3 * c) ^ x ^ 1,
    }
    half = -(-capacity // 2)
    sizes = {k: capacity for k in distances} if direct else {"P": half * groups}
    sent_here = [k for k in sizes if k != "B"]
    total = sum(sizes.values())
    args = [expert_ids.T, norm_gain.reshape(-1, 128), tokens]
    normed, slots, *sends = call(
        functools.partial(route_body, capacity, groups, direct),
        [shape(rows_here, width, bf16), shape(chosen, rows_here, jnp.int32)]
        + [shape(sizes[k], width, bf16) for k in sent_here],
        args,
        2 * rows_here * width * total,
        landing(args),
        range(3),
    )
    arrived = {k: hop(block, distances[k]) for k, block in zip(sent_here, sends)}
    if direct:
        arrived["B"] = lax.ppermute(arrived["A"], "tp", neighbour)

    args = [slots, normed, route_weights.T, shared_gate, shared_up, shared_down]
    sh_send, sh_keep, high, low = call(
        shared_body,
        [shape(rows_here, wide, bf16), shape(rows_here, wide, f32)]
        + [shape(rows_here, total, bf16)] * 2,
        args,
        6 * rows_here * width * shared_gate.shape[1],
        landing(args[2:]),
        range(2, 6),
    )
    sh_came = lax.ppermute(sh_send, "tp", neighbour)

    parties = {"A": ("A",), "B": ("B",), "N": ("P", "Q")} if direct else {"N": ("P",)}
    partner = {"A": "B", "B": "A", "N": "N"}
    kept, came = {}, {}
    for p, names in parties.items():
        send, kept[p] = products([arrived[k] for k in names], [*own, *other], wide)
        came[partner[p]] = lax.ppermute(send, "tp", neighbour)
    returned = {}
    for p, names in parties.items():
        outs = [shape(sizes[k], wide, bf16) for k in names]
        outs = call(add_body, outs, [kept[p], came[p]], came[p].size)
        for k, out in zip(names, outs):
            returned[k] = hop(out, distances[k])

    mine, sent = call(
        functools.partial(mix_body, len(sizes)),
        [shape(rows_here, share, f32), shape(rows_here, share, f32)],
        [high, low, *[returned[k] for k in sizes], sh_keep, sh_came],
        4 * rows_here * wide * total,
        [pltpu.VMEM((total, wide), bf16)],
    )
    came = lax.ppermute(sent, "tp", sibling)
    (mixed,) = call(add_body, [shape(rows_here, share, bf16)], [mine, came], mine.size)
    return mixed


def solution(mesh):
    in_specs = (
        P("ep", None),
        P(),
        P("ep", None),
        P("ep", None),
        P("ep", None, "tp"),
        P("ep", None, "tp"),
        P("ep", "tp", None),
        P(None, "tp"),
        P(None, "tp"),
        P("tp", None),
    )
    out_specs = P("ep", "tp")

    return jax.shard_map(local, mesh=mesh, in_specs=in_specs, out_specs=out_specs, check_vma=False)
```

time: 55.9 us -> 51.5 us (0.921)
  starting transfers between devices: 34.2 us -> 22.4 us
  waiting for transfers between devices: 13.1 us -> 19.3 us
  local copies, waits for them, and re-layouts: 0.01 us -> 2.09 us
  Pallas kernels: 8.24 us -> 7.3 us
    ppermute x12 -> x7, starting transfers between devices: 24 us -> 13 us  [hop(): return lax.ppermute(block, ('ep', 'tp'), pairs)]
    ppermute x12 -> x7, waiting for transfers between devices: 4.32 us -> 9.88 us  [hop(): return lax.ppermute(block, ('ep', 'tp'), pairs)]
    unnamed x6 -> x10, local copies, waits for them, and re-layouts: 0.01 us -> 2.09 us
    ppermute x1, starting transfers between devices: 2.75 us -> 1.53 us  [local(): sh_came = lax.ppermute(sh_send, 'tp', neighbour)]
    ppermute x5 -> x4, waiting for transfers between devices: 7.29 us -> 8.28 us  [the longest x3 8.27 us: local(): came[partner[p]] = lax.ppermute(send, 'tp', neighbour)]
    pallas_call x11 -> x10, Pallas kernels: 8.24 us -> 7.3 us  [call(): pl.pallas_call(body, out_shape=outs, in_specs=[hbm if i in far else vmem...]
    ppermute x5 -> x4, starting transfers between devices: 6.37 us -> 6.27 us  [the longest x1 3.54 us: local(): arrived['B'] = lax.ppermute(arrived['A'], 'tp', neighbour)]
  transfers between devices with their start and end apart: 22 -> 16, of which waited for: 7 -> 6; matrix products, arithmetic and copies ran while one was open for 0% -> 0% of each run, Pallas kernels for 13% -> 12%
where the time goes in v2:
time: 51.5 us; the launch traced here: 51.2 us
  starting transfers between devices  22.4 us (43%)
  waiting for transfers between devices  19.3 us (37%)
  Pallas kernels  7.3 us (14%)
  local copies, waits for them, and re-layouts  2.09 us (4%)
    ppermute x7, starting transfers between devices, hop(): return lax.ppermute(block, ('ep', 'tp'), pairs)  13 us
    ppermute x7, waiting for transfers between devices, hop(): return lax.ppermute(block, ('ep', 'tp'), pairs)  9.88 us
    ppermute x3, waiting for transfers between devices, local(): came[partner[p]] = lax.ppermute(send, 'tp', neighbour)  8.27 us
    pallas_call x10, Pallas kernels, call(): pl.pallas_call(body, out_shape=outs, in_specs=[hbm if i in far else vmem...  7.3 us
    ppermute x1, starting transfers between devices, local(): arrived['B'] = lax.ppermute(arrived['A'], 'tp', neighbour)  3.54 us
    ppermute x3, starting transfers between devices, local(): came[partner[p]] = lax.ppermute(send, 'tp', neighbour)  2.73 us
    unnamed x10, local copies, waits for them, and re-layouts  2.09 us
    ppermute x1, starting transfers between devices, local(): sh_came = lax.ppermute(sh_send, 'tp', neighbour)  1.53 us
  transfers between devices with their start and end apart: 16, of which 6 were waited for; matrix products, arithmetic and copies ran while one was open for 0% of the time, Pallas kernels for 12%

profile of v2, /device:TPU:0, one launch (start us, length us, event | category | flops | bytes accessed | tf_op | source)
XLA Modules:
  0.0 51.2 jit_solution(9140943051424029709)
XLA Ops:
  0.0 0.5 collective-permute-start.2
  0.5 0.1 collective-permute-start.3
  0.6 0.4 collective-permute-start.4
  1.0 1.7 %shard_map.100 = (bf16[128,2048]{1,0:T(8,128)(2,1)S(1)}, s32[2,128]{1,0:T(2,128)S(1)}, bf16[48,2048]{1,0:T(8,128)(2,1)S(1)}, bf16[48,2048]{1,0:T(8,128)(2,1)S(1)}, bf16[48,2048]{1,0:T(8,128)(2,1)S(1)}) custom-call(s32[2,128]{1,0:T(2,128)} %bitcast.20, bf16[16,128]{1,0:T(8,128)(2,1)} %bitcast.18, bf16[128,2048]{1,0:T(8,128)(2,1)} %tokens_in.1), custom_call_target="tpu_custom_call" | custom-call | flops 100663296 | bytes 1644544 | tf_op jit(solution)/shard_map/pallas_call | solution.py:25
  2.7 0.7 %collective-permute-start = (bf16[48,2048]{1,0:T(8,128)(2,1)S(1)}, bf16[48,2048]{1,0:T(8,128)(2,1)S(1)}, u32[]{:S(2)}, u32[]{:S(2)}) collective-permute-start(bf16[48,2048]{1,0:T(8,128)(2,1)S(1)} %get-tuple-element.28), channel_id=1, source_target_pairs={{0,0},{1,5},{2,2},{3,7},{4,4},{5,1},{6,6},{7,3},{8,8},{9,13},{10,1... | collective-permute-start | bytes 589832 | tf_op jit(solution)/shard_map/ppermute | solution.py:231
  3.4 3.7 %collective-permute-start.8 = (bf16[48,2048]{1,0:T(8,128)(2,1)S(1)}, bf16[48,2048]{1,0:T(8,128)(2,1)S(1)}, u32[]{:S(2)}, u32[]{:S(2)}) collective-permute-start(bf16[48,2048]{1,0:T(8,128)(2,1)S(1)} %get-tuple-element.34), channel_id=1, source_target_pairs={{0,16},{1,29},{2,22},{3,27},{4,20},{5,25},{6,18},{7,31},{8,24},{9,... | collective-permute-start | bytes 589832 | tf_op jit(solution)/shard_map/ppermute | solution.py:231
  7.1 2.5 %collective-permute-start.1 = (bf16[48,2048]{1,0:T(8,128)(2,1)S(1)}, bf16[48,2048]{1,0:T(8,128)(2,1)S(1)}, u32[]{:S(2)}, u32[]{:S(2)}) collective-permute-start(bf16[48,2048]{1,0:T(8,128)(2,1)S(1)} %get-tuple-element.29), channel_id=1, source_target_pairs={{0,12},{1,9},{2,14},{3,11},{4,8},{5,13},{6,10},{7,15},{8,4},{9,1},... | collective-permute-start | bytes 589832 | tf_op jit(solution)/shard_map/ppermute | solution.py:231
  9.6 5.5 %collective-permute-done.8.refs_0_ = bf16[48,2048]{1,0:T(8,128)(2,1)S(1)} collective-permute-done((bf16[48,2048]{1,0:T(8,128)(2,1)S(1)}, bf16[48,2048]{1,0:T(8,128)(2,1)S(1)}, u32[]{:S(2)}, u32[]{:S(2)}) %collective-permute-start.8) | collective-permute-done | bytes 196640 | tf_op jit(solution)/shard_map/ppermute | solution.py:231
  15.1 3.5 %collective-permute-start.9 = (bf16[48,2048]{1,0:T(8,128)(2,1)S(1)}, bf16[48,2048]{1,0:T(8,128)(2,1)S(1)}, u32[]{:S(2)}, u32[]{:S(2)}) collective-permute-start(bf16[48,2048]{1,0:T(8,128)(2,1)S(1)} %collective-permute-done.8.refs_0_), channel_id=1, source_target_pairs={{0,2},{1,3},{2,0},{3,1},{4,6},{5,7},{6,4},{7,5},{8,10},{9,11},{10,... | collective-permute-start | bytes 589832 | tf_op jit(solution)/shard_map/ppermute | solution.py:255
  18.7 0.0 copy-start.1
  18.7 1.0 %copy-done.1 = bf16[1,2048,128]{2,1,0:T(8,128)(2,1)S(1)} copy-done((bf16[1,2048,128]{2,1,0:T(8,128)(2,1)S(1)}, bf16[1,2048,128]{2,1,0:T(8,128)(2,1)}, u32[]{:S(2)}) %copy-start.1) | copy-done | bytes 524312
  19.7 1.0 %copy-done.3 = bf16[1,128,2048]{2,1,0:T(8,128)(2,1)S(1)} copy-done((bf16[1,128,2048]{2,1,0:T(8,128)(2,1)S(1)}, bf16[1,128,2048]{2,1,0:T(8,128)(2,1)}, u32[]{:S(2)}) %copy-start.3) | copy-done | bytes 524312
  20.8 0.8 %shard_map.102 = (bf16[96,1024]{1,0:T(8,128)(2,1)S(1)}, f32[96,1024]{1,0:T(8,128)S(1)}) custom-call(bf16[48,2048]{1,0:T(8,128)(2,1)S(1)} %collective-permute-done.refs_0_, bf16[48,2048]{1,0:T(8,128)(2,1)S(1)} %collective-permute-done.1.refs_1_, bf16[2048,128]{1,0:T(8,128)(2,1)S(1)} %bitcast.7, bf16[2048,128]{1,0:T(8,128)(2,1)S(1)} %bitcast.11, ...), custom_call_target="tpu_custom_call" | custom-call | flops 301989888 | bytes 4128768 | tf_op jit(solution)/shard_map/pallas_call | solution.py:25
  21.5 0.6 %collective-permute-start.5 = (bf16[96,1024]{1,0:T(8,128)(2,1)S(1)}, bf16[96,1024]{1,0:T(8,128)(2,1)S(1)}, u32[]{:S(2)}, u32[]{:S(2)}) collective-permute-start(bf16[96,1024]{1,0:T(8,128)(2,1)S(1)} %get-tuple-element.31), channel_id=1, source_target_pairs={{0,2},{1,3},{2,0},{3,1},{4,6},{5,7},{6,4},{7,5},{8,10},{9,11},{10,... | collective-permute-start | bytes 589832 | tf_op jit(solution)/shard_map/ppermute | solution.py:274
  22.2 2.3 %shard_map.101 = (bf16[128,1024]{1,0:T(8,128)(2,1)S(1)}, f32[128,1024]{1,0:T(8,128)S(1)}, bf16[128,192]{1,0:T(8,128)(2,1)S(1)}, bf16[128,192]{1,0:T(8,128)(2,1)S(1)}) custom-call(s32[2,128]{1,0:T(2,128)S(1)} %get-tuple-element.24.slots, bf16[128,2048]{1,0:T(8,128)(2,1)S(1)} %get-tuple-element.25.rows, f32[2,128]{1,0:T(2,128)} %bitcast.19, ...), custom_call_target="tpu_custom_call" | custom-call | flops 201326592 | bytes 2983936 | tf_op jit(solution)/shard_map/pallas_call | solution.py:25
  24.5 1.5 %collective-permute-start.14 = (bf16[128,1024]{1,0:T(8,128)(2,1)S(1)}, bf16[128,1024]{1,0:T(8,128)(2,1)S(1)}, u32[]{:S(2)}, u32[]{:S(2)}) collective-permute-start(bf16[128,1024]{1,0:T(8,128)(2,1)S(1)} %get-tuple-element.40), channel_id=1, source_target_pairs={{0,2},{1,3},{2,0},{3,1},{4,6},{5,7},{6,4},{7,5},{8,10},{9,11},{10,... | collective-permute-start | bytes 786440 | tf_op jit(solution)/shard_map/ppermute | solution.py:267
  26.0 0.8 %shard_map.105 = (bf16[48,1024]{1,0:T(8,128)(2,1)S(1)}, f32[48,1024]{1,0:T(8,128)S(1)}) custom-call(bf16[48,2048]{1,0:T(8,128)(2,1)S(1)} %collective-permute-done.9.refs_0_, bf16[2048,128]{1,0:T(8,128)(2,1)S(1)} %bitcast.8, bf16[2048,128]{1,0:T(8,128)(2,1)S(1)} %bitcast.12, bf16[128,2048]{1,0:T(8,128)(2,1)S(1)} %bitcast.16, ...), custom_call_target="tpu_custom_call" | custom-call | flops 150994944 | bytes 3637248 | tf_op jit(solution)/shard_map/pallas_call | solution.py:25
  26.8 0.6 %collective-permute-start.10 = (bf16[48,1024]{1,0:T(8,128)(2,1)S(1)}, bf16[48,1024]{1,0:T(8,128)(2,1)S(1)}, u32[]{:S(2)}, u32[]{:S(2)}) collective-permute-start(bf16[48,1024]{1,0:T(8,128)(2,1)S(1)} %get-tuple-element.36), channel_id=1, source_target_pairs={{0,2},{1,3},{2,0},{3,1},{4,6},{5,7},{6,4},{7,5},{8,10},{9,11},{10,... | collective-permute-start | bytes 294920 | tf_op jit(solution)/shard_map/ppermute | solution.py:274
  27.4 0.7 %shard_map.104 = (bf16[48,1024]{1,0:T(8,128)(2,1)S(1)}, f32[48,1024]{1,0:T(8,128)S(1)}) custom-call(bf16[48,2048]{1,0:T(8,128)(2,1)S(1)} %collective-permute-done.8.refs_0_, bf16[2048,128]{1,0:T(8,128)(2,1)S(1)} %bitcast.9, bf16[2048,128]{1,0:T(8,128)(2,1)S(1)} %bitcast.13, bf16[128,2048]{1,0:T(8,128)(2,1)S(1)} %bitcast.17, ...), custom_call_target="tpu_custom_call" | custom-call | flops 150994944 | bytes 3637248 | tf_op jit(solution)/shard_map/pallas_call | solution.py:25
  28.1 1.5 %collective-permute-start.12 = (bf16[48,1024]{1,0:T(8,128)(2,1)S(1)}, bf16[48,1024]{1,0:T(8,128)(2,1)S(1)}, u32[]{:S(2)}, u32[]{:S(2)}) collective-permute-start(bf16[48,1024]{1,0:T(8,128)(2,1)S(1)} %get-tuple-element.38), channel_id=1, source_target_pairs={{0,2},{1,3},{2,0},{3,1},{4,6},{5,7},{6,4},{7,5},{8,10},{9,11},{10,... | collective-permute-start | bytes 294920 | tf_op jit(solution)/shard_map/ppermute | solution.py:274
  29.6 6.6 %collective-permute-done.10.came = bf16[48,1024]{1,0:T(8,128)(2,1)S(1)} collective-permute-done((bf16[48,1024]{1,0:T(8,128)(2,1)S(1)}, bf16[48,1024]{1,0:T(8,128)(2,1)S(1)}, u32[]{:S(2)}, u32[]{:S(2)}) %collective-permute-start.10) | collective-permute-done | bytes 98336 | tf_op jit(solution)/shard_map/ppermute | solution.py:274
  36.3 0.1 collective-permute-start.11
  36.4 1.6 %collective-permute-done.12.came = bf16[48,1024]{1,0:T(8,128)(2,1)S(1)} collective-permute-done((bf16[48,1024]{1,0:T(8,128)(2,1)S(1)}, bf16[48,1024]{1,0:T(8,128)(2,1)S(1)}, u32[]{:S(2)}, u32[]{:S(2)}) %collective-permute-start.12) | collective-permute-done | bytes 98336 | tf_op jit(solution)/shard_map/ppermute | solution.py:274
  38.0 2.0 %collective-permute-start.13 = (bf16[48,1024]{1,0:T(8,128)(2,1)S(1)}, bf16[48,1024]{1,0:T(8,128)(2,1)S(1)}, u32[]{:S(2)}, u32[]{:S(2)}) collective-permute-start(bf16[48,1024]{1,0:T(8,128)(2,1)S(1)} %shard_map.107), channel_id=1, source_target_pairs={{0,20},{1,25},{2,18},{3,31},{4,16},{5,29},{6,22},{7,27},{8,28},{9,... | collective-permute-start | bytes 294920 | tf_op jit(solution)/shard_map/ppermute | solution.py:231
  40.1 0.7 %collective-permute-start.6 = (bf16[48,1024]{1,0:T(8,128)(2,1)S(1)}, bf16[48,1024]{1,0:T(8,128)(2,1)S(1)}, u32[]{:S(2)}, u32[]{:S(2)}) collective-permute-start(bf16[48,1024]{1,0:T(8,128)(2,1)S(1)} %get-tuple-element.32), channel_id=1, source_target_pairs={{0,0},{1,5},{2,2},{3,7},{4,4},{5,1},{6,6},{7,3},{8,8},{9,13},{10,1... | collective-permute-start | bytes 294920 | tf_op jit(solution)/shard_map/ppermute | solution.py:231
  40.8 3.4 %collective-permute-start.7 = (bf16[48,1024]{1,0:T(8,128)(2,1)S(1)}, bf16[48,1024]{1,0:T(8,128)(2,1)S(1)}, u32[]{:S(2)}, u32[]{:S(2)}) collective-permute-start(bf16[48,1024]{1,0:T(8,128)(2,1)S(1)} %get-tuple-element.33), channel_id=1, source_target_pairs={{0,12},{1,9},{2,14},{3,11},{4,8},{5,13},{6,10},{7,15},{8,4},{9,1},... | collective-permute-start | bytes 294920 | tf_op jit(solution)/shard_map/ppermute | solution.py:231
  44.1 1.9 %collective-permute-done.11.refs_2_ = bf16[48,1024]{1,0:T(8,128)(2,1)S(1)} collective-permute-done((bf16[48,1024]{1,0:T(8,128)(2,1)S(1)}, bf16[48,1024]{1,0:T(8,128)(2,1)S(1)}, u32[]{:S(2)}, u32[]{:S(2)}) %collective-permute-start.11) | collective-permute-done | bytes 98336 | tf_op jit(solution)/shard_map/ppermute | solution.py:231
  46.0 2.5 %collective-permute-done.13.refs_3_ = bf16[48,1024]{1,0:T(8,128)(2,1)S(1)} collective-permute-done((bf16[48,1024]{1,0:T(8,128)(2,1)S(1)}, bf16[48,1024]{1,0:T(8,128)(2,1)S(1)}, u32[]{:S(2)}, u32[]{:S(2)}) %collective-permute-start.13) | collective-permute-done | bytes 98336 | tf_op jit(solution)/shard_map/ppermute | solution.py:231
  48.5 0.3 shard_map.108
  48.8 0.6 %collective-permute-start.15 = (f32[128,512]{1,0:T(8,128)S(1)}, f32[128,512]{1,0:T(8,128)S(1)}, u32[]{:S(2)}, u32[]{:S(2)}) collective-permute-start(f32[128,512]{1,0:T(8,128)S(1)} %get-tuple-element.42), channel_id=1, source_target_pairs={{0,1},{1,0},{2,3},{3,2},{4,5},{5,4},{6,7},{7,6},{8,9},{9,8},{10,11... | collective-permute-start | bytes 786440 | tf_op jit(solution)/shard_map/ppermute | solution.py:289
  49.4 1.2 %collective-permute-done.15.came = f32[128,512]{1,0:T(8,128)S(1)} collective-permute-done((f32[128,512]{1,0:T(8,128)S(1)}, f32[128,512]{1,0:T(8,128)S(1)}, u32[]{:S(2)}, u32[]{:S(2)}) %collective-permute-start.15) | collective-permute-done | bytes 262176 | tf_op jit(solution)/shard_map/ppermute | solution.py:289
  50.6 0.7 %shard_map.109 = bf16[128,512]{1,0:T(8,128)(2,1)} custom-call(f32[128,512]{1,0:T(8,128)S(1)} %get-tuple-element.41.keep, f32[128,512]{1,0:T(8,128)S(1)} %collective-permute-done.15.came), custom_call_target="tpu_custom_call" | custom-call | flops 65536 | bytes 655360 | tf_op jit(solution)/shard_map/pallas_call | solution.py:25
  (20 shorter events, 0.1 us)
Async XLA Ops:
  0.0 18.7 %copy-start = (bf16[1,2048,128]{2,1,0:T(8,128)(2,1)S(1)}, bf16[1,2048,128]{2,1,0:T(8,128)(2,1)}, u32[]{:S(2)}) copy-start(bf16[1,2048,128]{2,1,0:T(8,128)(2,1)} %param.14) | copy-start | bytes 1572868
  0.0 18.7 %collective-permute-start.2 = (bf16[2048,128]{1,0:T(8,128)(2,1)}, bf16[2048,128]{1,0:T(8,128)(2,1)S(1)}, u32[]{:S(2)}, u32[]{:S(2)}) collective-permute-start(bf16[2048,128]{1,0:T(8,128)(2,1)} %bitcast.6), channel_id=1, source_target_pairs={{0,1},{1,0},{2,3},{3,2},{4,5},{5,4},{6,7},{7,6},{8,9},{9,8},{10,11... | collective-permute-start | bytes 1572872 | tf_op jit(solution)/shard_map/ppermute | solution.py:222
  0.5 18.2 %collective-permute-start.3 = (bf16[2048,128]{1,0:T(8,128)(2,1)}, bf16[2048,128]{1,0:T(8,128)(2,1)S(1)}, u32[]{:S(2)}, u32[]{:S(2)}) collective-permute-start(bf16[2048,128]{1,0:T(8,128)(2,1)} %bitcast.10), channel_id=1, source_target_pairs={{0,1},{1,0},{2,3},{3,2},{4,5},{5,4},{6,7},{7,6},{8,9},{9,8},{10,11... | collective-permute-start | bytes 1572872 | tf_op jit(solution)/shard_map/ppermute | solution.py:222
  0.6 18.1 %collective-permute-start.4 = (bf16[128,2048]{1,0:T(8,128)(2,1)}, bf16[128,2048]{1,0:T(8,128)(2,1)S(1)}, u32[]{:S(2)}, u32[]{:S(2)}) collective-permute-start(bf16[128,2048]{1,0:T(8,128)(2,1)} %bitcast.14), channel_id=1, source_target_pairs={{0,1},{1,0},{2,3},{3,2},{4,5},{5,4},{6,7},{7,6},{8,9},{9,8},{10,11... | collective-permute-start | bytes 1572872 | tf_op jit(solution)/shard_map/ppermute | solution.py:222
  2.7 4.4 %collective-permute-start = (bf16[48,2048]{1,0:T(8,128)(2,1)S(1)}, bf16[48,2048]{1,0:T(8,128)(2,1)S(1)}, u32[]{:S(2)}, u32[]{:S(2)}) collective-permute-start(bf16[48,2048]{1,0:T(8,128)(2,1)S(1)} %get-tuple-element.28), channel_id=1, source_target_pairs={{0,0},{1,5},{2,2},{3,7},{4,4},{5,1},{6,6},{7,3},{8,8},{9,13},{10,1... | collective-permute-start | bytes 589832 | tf_op jit(solution)/shard_map/ppermute | solution.py:231
  3.4 11.8 %collective-permute-start.8 = (bf16[48,2048]{1,0:T(8,128)(2,1)S(1)}, bf16[48,2048]{1,0:T(8,128)(2,1)S(1)}, u32[]{:S(2)}, u32[]{:S(2)}) collective-permute-start(bf16[48,2048]{1,0:T(8,128)(2,1)S(1)} %get-tuple-element.34), channel_id=1, source_target_pairs={{0,16},{1,29},{2,22},{3,27},{4,20},{5,25},{6,18},{7,31},{8,24},{9,... | collective-permute-start | bytes 589832 | tf_op jit(solution)/shard_map/ppermute | solution.py:231
  7.1 11.6 %collective-permute-start.1 = (bf16[48,2048]{1,0:T(8,128)(2,1)S(1)}, bf16[48,2048]{1,0:T(8,128)(2,1)S(1)}, u32[]{:S(2)}, u32[]{:S(2)}) collective-permute-start(bf16[48,2048]{1,0:T(8,128)(2,1)S(1)} %get-tuple-element.29), channel_id=1, source_target_pairs={{0,12},{1,9},{2,14},{3,11},{4,8},{5,13},{6,10},{7,15},{8,4},{9,1},... | collective-permute-start | bytes 589832 | tf_op jit(solution)/shard_map/ppermute | solution.py:231
  15.1 10.9 %collective-permute-start.9 = (bf16[48,2048]{1,0:T(8,128)(2,1)S(1)}, bf16[48,2048]{1,0:T(8,128)(2,1)S(1)}, u32[]{:S(2)}, u32[]{:S(2)}) collective-permute-start(bf16[48,2048]{1,0:T(8,128)(2,1)S(1)} %collective-permute-done.8.refs_0_), channel_id=1, source_target_pairs={{0,2},{1,3},{2,0},{3,1},{4,6},{5,7},{6,4},{7,5},{8,10},{9,11},{10,... | collective-permute-start | bytes 589832 | tf_op jit(solution)/shard_map/ppermute | solution.py:255
  18.7 1.0 %copy-start.1 = (bf16[1,2048,128]{2,1,0:T(8,128)(2,1)S(1)}, bf16[1,2048,128]{2,1,0:T(8,128)(2,1)}, u32[]{:S(2)}) copy-start(bf16[1,2048,128]{2,1,0:T(8,128)(2,1)} %param.15) | copy-start | bytes 1572868
  19.7 1.0 %copy-start.3 = (bf16[1,128,2048]{2,1,0:T(8,128)(2,1)S(1)}, bf16[1,128,2048]{2,1,0:T(8,128)(2,1)}, u32[]{:S(2)}) copy-start(bf16[1,128,2048]{2,1,0:T(8,128)(2,1)} %param.16) | copy-start | bytes 1572868
  21.5 18.5 %collective-permute-start.5 = (bf16[96,1024]{1,0:T(8,128)(2,1)S(1)}, bf16[96,1024]{1,0:T(8,128)(2,1)S(1)}, u32[]{:S(2)}, u32[]{:S(2)}) collective-permute-start(bf16[96,1024]{1,0:T(8,128)(2,1)S(1)} %get-tuple-element.31), channel_id=1, source_target_pairs={{0,2},{1,3},{2,0},{3,1},{4,6},{5,7},{6,4},{7,5},{8,10},{9,11},{10,... | collective-permute-start | bytes 589832 | tf_op jit(solution)/shard_map/ppermute | solution.py:274
  22.2 3.8 %copy-start.2 = (bf16[1,2048,128]{2,1,0:T(8,128)(2,1)S(1)}, bf16[1,2048,128]{2,1,0:T(8,128)(2,1)}, u32[]{:S(2)}) copy-start(bf16[1,2048,128]{2,1,0:T(8,128)(2,1)} %param.15) | copy-start | bytes 1572868
  22.2 3.8 %copy-start.4 = (bf16[1,128,2048]{2,1,0:T(8,128)(2,1)S(1)}, bf16[1,128,2048]{2,1,0:T(8,128)(2,1)}, u32[]{:S(2)}) copy-start(bf16[1,128,2048]{2,1,0:T(8,128)(2,1)} %param.16) | copy-start | bytes 1572868
  24.5 19.7 %collective-permute-start.14 = (bf16[128,1024]{1,0:T(8,128)(2,1)S(1)}, bf16[128,1024]{1,0:T(8,128)(2,1)S(1)}, u32[]{:S(2)}, u32[]{:S(2)}) collective-permute-start(bf16[128,1024]{1,0:T(8,128)(2,1)S(1)} %get-tuple-element.40), channel_id=1, source_target_pairs={{0,2},{1,3},{2,0},{3,1},{4,6},{5,7},{6,4},{7,5},{8,10},{9,11},{10,... | collective-permute-start | bytes 786440 | tf_op jit(solution)/shard_map/ppermute | solution.py:267
  26.8 9.5 %collective-permute-start.10 = (bf16[48,1024]{1,0:T(8,128)(2,1)S(1)}, bf16[48,1024]{1,0:T(8,128)(2,1)S(1)}, u32[]{:S(2)}, u32[]{:S(2)}) collective-permute-start(bf16[48,1024]{1,0:T(8,128)(2,1)S(1)} %get-tuple-element.36), channel_id=1, source_target_pairs={{0,2},{1,3},{2,0},{3,1},{4,6},{5,7},{6,4},{7,5},{8,10},{9,11},{10,... | collective-permute-start | bytes 294920 | tf_op jit(solution)/shard_map/ppermute | solution.py:274
  28.1 9.9 %collective-permute-start.12 = (bf16[48,1024]{1,0:T(8,128)(2,1)S(1)}, bf16[48,1024]{1,0:T(8,128)(2,1)S(1)}, u32[]{:S(2)}, u32[]{:S(2)}) collective-permute-start(bf16[48,1024]{1,0:T(8,128)(2,1)S(1)} %get-tuple-element.38), channel_id=1, source_target_pairs={{0,2},{1,3},{2,0},{3,1},{4,6},{5,7},{6,4},{7,5},{8,10},{9,11},{10,... | collective-permute-start | bytes 294920 | tf_op jit(solution)/shard_map/ppermute | solution.py:274
  36.3 9.7 %collective-permute-start.11 = (bf16[48,1024]{1,0:T(8,128)(2,1)S(1)}, bf16[48,1024]{1,0:T(8,128)(2,1)S(1)}, u32[]{:S(2)}, u32[]{:S(2)}) collective-permute-start(bf16[48,1024]{1,0:T(8,128)(2,1)S(1)} %shard_map.106), channel_id=1, source_target_pairs={{0,16},{1,29},{2,22},{3,27},{4,20},{5,25},{6,18},{7,31},{8,24},{9,... | collective-permute-start | bytes 294920 | tf_op jit(solution)/shard_map/ppermute | solution.py:231
  38.0 10.5 %collective-permute-start.13 = (bf16[48,1024]{1,0:T(8,128)(2,1)S(1)}, bf16[48,1024]{1,0:T(8,128)(2,1)S(1)}, u32[]{:S(2)}, u32[]{:S(2)}) collective-permute-start(bf16[48,1024]{1,0:T(8,128)(2,1)S(1)} %shard_map.107), channel_id=1, source_target_pairs={{0,20},{1,25},{2,18},{3,31},{4,16},{5,29},{6,22},{7,27},{8,28},{9,... | collective-permute-start | bytes 294920 | tf_op jit(solution)/shard_map/ppermute | solution.py:231
  40.1 8.4 %collective-permute-start.6 = (bf16[48,1024]{1,0:T(8,128)(2,1)S(1)}, bf16[48,1024]{1,0:T(8,128)(2,1)S(1)}, u32[]{:S(2)}, u32[]{:S(2)}) collective-permute-start(bf16[48,1024]{1,0:T(8,128)(2,1)S(1)} %get-tuple-element.32), channel_id=1, source_target_pairs={{0,0},{1,5},{2,2},{3,7},{4,4},{5,1},{6,6},{7,3},{8,8},{9,13},{10,1... | collective-permute-start | bytes 294920 | tf_op jit(solution)/shard_map/ppermute | solution.py:231
  40.8 7.7 %collective-permute-start.7 = (bf16[48,1024]{1,0:T(8,128)(2,1)S(1)}, bf16[48,1024]{1,0:T(8,128)(2,1)S(1)}, u32[]{:S(2)}, u32[]{:S(2)}) collective-permute-start(bf16[48,1024]{1,0:T(8,128)(2,1)S(1)} %get-tuple-element.33), channel_id=1, source_target_pairs={{0,12},{1,9},{2,14},{3,11},{4,8},{5,13},{6,10},{7,15},{8,4},{9,1},... | collective-permute-start | bytes 294920 | tf_op jit(solution)/shard_map/ppermute | solution.py:231
  48.8 1.7 %collective-permute-start.15 = (f32[128,512]{1,0:T(8,128)S(1)}, f32[128,512]{1,0:T(8,128)S(1)}, u32[]{:S(2)}, u32[]{:S(2)}) collective-permute-start(f32[128,512]{1,0:T(8,128)S(1)} %get-tuple-element.42), channel_id=1, source_target_pairs={{0,1},{1,0},{2,3},{3,2},{4,5},{5,4},{6,7},{7,6},{8,9},{9,8},{10,11... | collective-permute-start | bytes 786440 | tf_op jit(solution)/shard_map/ppermute | solution.py:289

commit v3 on v2

--- a/solution.py
+++ b/solution.py
@@ -64,9 +64,9 @@
     return jnp.where(held, label * half + rank, -1)
 
 
-def route_body(capacity, experts, direct, ids_in, gain_in, tokens_in, *refs):
-    outs, (ids, gain, tokens, sems) = refs[:-4], refs[-4:]
-    copies = fetch((ids_in, gain_in, tokens_in), (ids, gain, tokens), sems)
+def route_body(capacity, experts, direct, *refs):
+    sources, outs, (ids, gain, tokens, sems) = refs[:6], refs[6:-4], refs[-4:]
+    copies = fetch(sources, (ids, gain, tokens, *outs[2:5]), sems)
     normed_out, slots_out = outs[0], outs[1]
     rows, width = tokens.shape
     kinds = max(8, experts)
@@ -76,7 +76,7 @@
         < lax.broadcasted_iota(jnp.int32, (rows, rows), 1)
     ).astype(bf16)
     base = jnp.zeros((kinds, 1), f32)
-    total = sum(out.shape[0] for out in outs[2:])
+    total = sum(out.shape[0] for out in outs[5:])
     slot = lax.broadcasted_iota(jnp.int32, (total, rows), 0)
     hit = jnp.zeros((total, rows), f32)
     copies[0].wait()
@@ -102,11 +102,13 @@
         normed_out[:, at] = (values[:, at] * scale * gain[c : c + 1].astype(f32)).astype(bf16)
     normed = normed_out[...]
     at = 0
-    for out in outs[2:]:
+    for out in outs[5:]:
         n = out.shape[0]
         part = pick[at : at + n]
         out[...] = jnp.dot(part, normed, preferred_element_type=f32).astype(bf16)
         at += n
+    for copy in copies[3:]:
+        copy.wait()
 
 
 def units_of(rows, weights):
@@ -117,22 +119,74 @@
     return (gate / (1.0 + jnp.exp(-gate)) * up).astype(bf16)
 
 
-def shared_body(slots, rows, gains_in, *refs):
-    weights_in, (send, keep, high_out, low_out) = refs[:3], refs[3:7]
-    gains, weights, sems = refs[7], refs[8:11], refs[11]
-    copies = fetch((gains_in, *weights_in), (gains, *weights), sems)
-    slot = lax.broadcasted_iota(jnp.int32, high_out.shape[::-1], 0)
+def shared_body(slots, rows, *refs):
+    weights, gains_in, part, outs = refs[:3], refs[3], refs[4], refs[5:-2]
+    gains, sems = refs[-2:]
+    (copy,) = fetch((gains_in,), (gains,), sems)
+    hidden = units_of(rows[...], weights)
+    part[...] = jnp.dot(hidden, weights[2][...], preferred_element_type=f32)
+    total = sum(out.shape[1] for out in outs[::2])
+    slot = lax.broadcasted_iota(jnp.int32, (total, rows.shape[0]), 0)
     weight = jnp.zeros(slot.shape, f32)
-    copies[0].wait()
+    copy.wait()
     for j in range(slots.shape[0]):
         weight = jnp.where(slot == slots[j : j + 1, :], gains[j : j + 1, :], weight)
-    weight = weight.T
-    high = weight.astype(bf16)
-    high_out[...] = high
-    low_out[...] = (weight - high.astype(f32)).astype(bf16)
-    for copy in copies[1:]:
-        copy.wait()
-    columns_out(units_of(rows[...], weights), weights, send, keep)
+    at = 0
+    for high_out, low_out in zip(outs[::2], outs[1::2]):
+        n = high_out.shape[1]
+        turned = weight[at : at + n].T
+        high = turned.astype(bf16)
+        high_out[...] = high
+        low_out[...] = (turned - high.astype(f32)).astype(bf16)
+        at += n
+
+
+def near_body(blocks, *refs):
+    rows_in, weights = refs[:blocks], refs[blocks : blocks + 6]
+    outs = refs[blocks + 6 : 2 * blocks + 6]
+    gathered = gather_rows(rows_in, refs[-1])
+    down = jnp.concatenate([w[...] for w in weights[2::3]], axis=0)
+    hidden = units_of(gathered[...], weights)
+    total = jnp.dot(hidden, down, preferred_element_type=f32).astype(bf16)
+    at = 0
+    for out in outs:
+        out[...] = total[at : at + out.shape[0]]
+        at += out.shape[0]
+
+
+def gather_rows(rows_in, room):
+    if len(rows_in) == 1:
+        return rows_in[0]
+    at = 0
+    for ref in rows_in:
+        room[at : at + ref.shape[0]] = ref[...]
+        at += ref.shape[0]
+    return room
+
+
+def picked(high, low, rows):
+    total = jnp.dot(high[...], rows, preferred_element_type=f32)
+    return total + jnp.dot(low[...], rows, preferred_element_type=f32)
+
+
+def first_body(blocks, high, low, part, *refs):
+    rows_in, (send, keep) = refs[:blocks], refs[blocks : blocks + 2]
+    gathered = gather_rows(rows_in, refs[-1])
+    share = keep.shape[1] // 2
+    core = lax.axis_index("tp") % 2
+    for out, place in ((send, 1 - core), (keep, core)):
+        for x in range(2):
+            columns = pl.ds(pl.multiple_of((2 * x + place) * share, share), share)
+            total = part[:, columns] + picked(high, low, gathered[:, columns])
+            out[:, x * share : (x + 1) * share] = total.astype(out.dtype)
+
+
+def halve_body(keep, came, send, mine):
+    share = mine.shape[1]
+    side = lax.axis_index("tp") // 2
+    for out, place in ((send, 1 - side), (mine, side)):
+        columns = pl.ds(pl.multiple_of(place * share, share), share)
+        out[...] = (keep[:, columns] + came[:, columns].astype(f32)).astype(out.dtype)
 
 
 def columns_out(hidden, weights, send, keep):
@@ -144,30 +198,17 @@
         out[...] = jnp.dot(hidden, down, preferred_element_type=f32).astype(out.dtype)
 
 
-def product_body(blocks, *refs):
-    rows_in, weights = refs[:blocks], refs[blocks : blocks + 6]
-    send, keep = refs[blocks + 6 : blocks + 8]
-    gathered = rows_in[0]
-    if blocks > 1:
-        gathered = refs[-1]
-        at = 0
-        for ref in rows_in:
-            gathered[at : at + ref.shape[0]] = ref[...]
-            at += ref.shape[0]
-    columns_out(units_of(gathered[...], weights), weights, send, keep)
-
-
-def products(rows, weights, width):
+def product_body(*refs):
+    rows, weights, send, keep = refs[0], refs[1:7], refs[7], refs[8]
+    columns_out(units_of(rows[...], weights), weights, send, keep)
+
+
+def products(body, rows, weights, outs):
     n = sum(r.shape[0] for r in rows)
     full = rows[0].shape[1]
     hidden = sum(w.shape[1] for w in weights[::3])
-    return call(
-        functools.partial(product_body, len(rows)),
-        [shape(n, width, bf16), shape(n, width, f32)],
-        [*rows, *weights],
-        6 * n * full * hidden,
-        [pltpu.VMEM((n, full), bf16)] if len(rows) > 1 else [],
-    )
+    scratch = [pltpu.VMEM((n, full), bf16)] if len(rows) > 1 else []
+    return call(body, outs, [*rows, *weights], 6 * n * full * hidden, scratch)
 
 
 def add_body(keep, came, *outs):
@@ -178,21 +219,15 @@
         at += n
 
 
-def mix_body(blocks, high, low, *refs):
-    rows_in, adds, outs = refs[:blocks], refs[blocks:-3], refs[-3:-1]
-    gathered = refs[-1]
-    at = 0
-    for ref in rows_in:
-        gathered[at : at + ref.shape[0]] = ref[...]
-        at += ref.shape[0]
+def mix_body(high, low, first, second, mine, came, *refs):
+    outs, room = refs[:2], refs[2]
+    gathered = gather_rows((first, second), room)
     width = outs[0].shape[1]
     core = lax.axis_index("tp") % 2
     for out, place in ((outs[0], core), (outs[1], 1 - core)):
         columns = pl.ds(pl.multiple_of(place * width, width), width)
-        rows = gathered[:, columns]
-        total = sum(a[:, columns].astype(f32) for a in adds)
-        total += jnp.dot(high[...], rows, preferred_element_type=f32)
-        out[...] = total + jnp.dot(low[...], rows, preferred_element_type=f32)
+        total = picked(high, low, gathered[:, columns])
+        out[...] = total + mine[...] + came[...].astype(f32) if out is outs[0] else total
 
 
 def local(
@@ -241,52 +276,73 @@
     sent_here = [k for k in sizes if k != "B"]
     total = sum(sizes.values())
     args = [expert_ids.T, norm_gain.reshape(-1, 128), tokens]
-    normed, slots, *sends = call(
+    sh_weights = [shared_gate, shared_up, shared_down]
+    normed, slots, *rest = call(
         functools.partial(route_body, capacity, groups, direct),
         [shape(rows_here, width, bf16), shape(chosen, rows_here, jnp.int32)]
+        + [shape(*w.shape, w.dtype) for w in sh_weights]
         + [shape(sizes[k], width, bf16) for k in sent_here],
-        args,
+        args + sh_weights,
         2 * rows_here * width * total,
-        landing(args),
-        range(3),
-    )
+        landing(args)[:-1] + [pltpu.SemaphoreType.DMA((6,))],
+        range(6),
+    )
+    sh_weights, sends = rest[:3], rest[3:]
     arrived = {k: hop(block, distances[k]) for k, block in zip(sent_here, sends)}
     if direct:
         arrived["B"] = lax.ppermute(arrived["A"], "tp", neighbour)
-
-    args = [slots, normed, route_weights.T, shared_gate, shared_up, shared_down]
-    sh_send, sh_keep, high, low = call(
+    near = [k for k in sizes if k in ("P", "Q")]
+    spans = [sum(sizes[k] for k in near)]
+    if direct:
+        spans.append(total - spans[0])
+    gains = route_weights.T
+    part, *weights = call(
         shared_body,
-        [shape(rows_here, wide, bf16), shape(rows_here, wide, f32)]
-        + [shape(rows_here, total, bf16)] * 2,
-        args,
+        [shape(rows_here, width, f32)]
+        + [shape(rows_here, n, bf16) for n in spans for _ in range(2)],
+        [slots, normed, *sh_weights, gains],
         6 * rows_here * width * shared_gate.shape[1],
-        landing(args[2:]),
-        range(2, 6),
-    )
-    sh_came = lax.ppermute(sh_send, "tp", neighbour)
-
-    parties = {"A": ("A",), "B": ("B",), "N": ("P", "Q")} if direct else {"N": ("P",)}
-    partner = {"A": "B", "B": "A", "N": "N"}
-    kept, came = {}, {}
-    for p, names in parties.items():
-        send, kept[p] = products([arrived[k] for k in names], [*own, *other], wide)
-        came[partner[p]] = lax.ppermute(send, "tp", neighbour)
-    returned = {}
-    for p, names in parties.items():
-        outs = [shape(sizes[k], wide, bf16) for k in names]
-        outs = call(add_body, outs, [kept[p], came[p]], came[p].size)
-        for k, out in zip(names, outs):
+        landing([gains]),
+        [5],
+    )
+
+    outs = [shape(sizes[k], width, bf16) for k in near]
+    body = functools.partial(near_body, len(near))
+    outs = products(body, [arrived[k] for k in near], [*own, *other], outs)
+    returned = {k: hop(out, distances[k]) for k, out in zip(near, outs)}
+    send, keep = call(
+        functools.partial(first_body, len(near)),
+        [shape(rows_here, wide, bf16), shape(rows_here, wide, f32)],
+        [*weights[:2], part, *[returned[k] for k in near]],
+        4 * rows_here * width * spans[0],
+        [pltpu.VMEM((spans[0], width), bf16)] if direct else [],
+    )
+    send, mine = call(
+        halve_body,
+        [shape(rows_here, share, bf16), shape(rows_here, share, f32)],
+        [keep, lax.ppermute(send, "tp", sibling)],
+        keep.size,
+    )
+    came = lax.ppermute(send, "tp", neighbour)
+
+    if direct:
+        sent, kept = {}, {}
+        for k in "AB":
+            outs = [shape(capacity, wide, bf16), shape(capacity, wide, f32)]
+            sent[k], kept[k] = products(product_body, [arrived[k]], [*own, *other], outs)
+            sent[k] = lax.ppermute(sent[k], "tp", neighbour)
+        for k, other_k in ("AB", "BA"):
+            ins = [kept[k], sent[other_k]]
+            (out,) = call(add_body, [shape(capacity, wide, bf16)], ins, kept[k].size)
             returned[k] = hop(out, distances[k])
-
-    mine, sent = call(
-        functools.partial(mix_body, len(sizes)),
-        [shape(rows_here, share, f32), shape(rows_here, share, f32)],
-        [high, low, *[returned[k] for k in sizes], sh_keep, sh_came],
-        4 * rows_here * wide * total,
-        [pltpu.VMEM((total, wide), bf16)],
-    )
-    came = lax.ppermute(sent, "tp", sibling)
+        mine, send = call(
+            mix_body,
+            [shape(rows_here, share, f32), shape(rows_here, share, f32)],
+            [*weights[2:], returned["A"], returned["B"], mine, came],
+            4 * rows_here * wide * spans[1],
+            [pltpu.VMEM((spans[1], wide), bf16)],
+        )
+        came = lax.ppermute(send, "tp", sibling)
     (mixed,) = call(add_body, [shape(rows_here, share, bf16)], [mine, came], mine.size)
     return mixed
 

time: 51.5 us -> 47.6 us (0.924)
  local copies, waits for them, and re-layouts: 2.09 us -> 0.01 us
  Pallas kernels: 7.3 us -> 6.48 us
    ppermute x5, waiting for transfers between devices: 9.44 us -> 3.53 us  [the longest x2 2 us: local(): sent[k] = lax.ppermute(sent[k], 'tp', neighbour)]
    ppermute x7, waiting for transfers between devices: 9.88 us -> 15.2 us  [hop(): return lax.ppermute(block, ('ep', 'tp'), pairs)]
    ppermute x5, starting transfers between devices: 4.85 us -> 8.02 us  [the longest x2 3.87 us: local(): sent[k] = lax.ppermute(sent[k], 'tp', neighbour)]
    unnamed x10 -> x6, local copies, waits for them, and re-layouts: 2.09 us -> 0.01 us
    ppermute x1, starting transfers between devices: 3.54 us -> 1.49 us  [local(): arrived['B'] = lax.ppermute(arrived['A'], 'tp', neighbour)]
    ppermute x7, starting transfers between devices: 13 us -> 11.6 us  [hop(): return lax.ppermute(block, ('ep', 'tp'), pairs)]
    pallas_call x10 -> x11, Pallas kernels: 7.3 us -> 6.48 us  [call(): pl.pallas_call(body, out_shape=outs, in_specs=[hbm if i in far else vmem...]
  transfers between devices with their start and end apart: 16 -> 16, of which waited for: 6 -> 7; matrix products, arithmetic and copies ran while one was open for 0% -> 0% of each run, Pallas kernels for 12% -> 12%
where the time goes in v3:
time: 47.6 us; the launch traced here: 47.4 us
  starting transfers between devices  22.1 us (46%)
  waiting for transfers between devices  18.8 us (39%)
  Pallas kernels  6.48 us (14%)
    ppermute x7, waiting for transfers between devices, hop(): return lax.ppermute(block, ('ep', 'tp'), pairs)  15.2 us
    ppermute x7, starting transfers between devices, hop(): return lax.ppermute(block, ('ep', 'tp'), pairs)  11.6 us
    pallas_call x11, Pallas kernels, call(): pl.pallas_call(body, out_shape=outs, in_specs=[hbm if i in far else vmem...  6.48 us
    ppermute x2, starting transfers between devices, local(): sent[k] = lax.ppermute(sent[k], 'tp', neighbour)  3.87 us
    ppermute x1, starting transfers between devices, local(): came = lax.ppermute(send, 'tp', neighbour)  2.05 us
    ppermute x1, starting transfers between devices, local(): lax.ppermute(send, 'tp', sibling)  2.03 us
    ppermute x2, waiting for transfers between devices, local(): sent[k] = lax.ppermute(sent[k], 'tp', neighbour)  2 us
    ppermute x1, waiting for transfers between devices, local(): came = lax.ppermute(send, 'tp', sibling)  1.52 us
  transfers between devices with their start and end apart: 16, of which 7 were waited for; matrix products, arithmetic and copies ran while one was open for 0% of the time, Pallas kernels for 12%

profile of v3, /device:TPU:0, one launch (start us, length us, event | category | flops | bytes accessed | tf_op | source)
XLA Modules:
  0.0 47.4 jit_solution(6933927831072702795)
XLA Ops:
  0.0 0.5 %collective-permute-start.1 = (bf16[2048,128]{1,0:T(8,128)(2,1)}, bf16[2048,128]{1,0:T(8,128)(2,1)S(1)}, u32[]{:S(2)}, u32[]{:S(2)}) collective-permute-start(bf16[2048,128]{1,0:T(8,128)(2,1)} %bitcast.6), channel_id=1, source_target_pairs={{0,1},{1,0},{2,3},{3,2},{4,5},{5,4},{6,7},{7,6},{8,9},{9,8},{10,11... | collective-permute-start | bytes 1572872 | tf_op jit(solution)/shard_map/ppermute | solution.py:257
  0.5 0.0 collective-permute-start.2
  0.5 0.5 %collective-permute-start.3 = (bf16[128,2048]{1,0:T(8,128)(2,1)}, bf16[128,2048]{1,0:T(8,128)(2,1)S(1)}, u32[]{:S(2)}, u32[]{:S(2)}) collective-permute-start(bf16[128,2048]{1,0:T(8,128)(2,1)} %bitcast.14), channel_id=1, source_target_pairs={{0,1},{1,0},{2,3},{3,2},{4,5},{5,4},{6,7},{7,6},{8,9},{9,8},{10,11... | collective-permute-start | bytes 1572872 | tf_op jit(solution)/shard_map/ppermute | solution.py:257
  1.0 1.8 %shard_map.100 = (bf16[128,2048]{1,0:T(8,128)(2,1)S(1)}, s32[2,128]{1,0:T(2,128)S(1)}, bf16[2048,128]{1,0:T(8,128)(2,1)S(1)}, bf16[2048,128]{1,0:T(8,128)(2,1)S(...) custom-call(s32[2,128]{1,0:T(2,128)} %bitcast.20, ...), custom_call_target="tpu_custom_call" | custom-call | flops 100663296 | bytes 4790272 | tf_op jit(solution)/shard_map/pallas_call | solution.py:25
  2.8 0.7 %collective-permute-start.9 = (bf16[48,2048]{1,0:T(8,128)(2,1)S(1)}, bf16[48,2048]{1,0:T(8,128)(2,1)S(1)}, u32[]{:S(2)}, u32[]{:S(2)}) collective-permute-start(bf16[48,2048]{1,0:T(8,128)(2,1)S(1)} %get-tuple-element.45), channel_id=1, source_target_pairs={{0,0},{1,5},{2,2},{3,7},{4,4},{5,1},{6,6},{7,3},{8,8},{9,13},{10,1... | collective-permute-start | bytes 589832 | tf_op jit(solution)/shard_map/ppermute | solution.py:266
  3.5 3.6 %collective-permute-start.10 = (bf16[48,2048]{1,0:T(8,128)(2,1)S(1)}, bf16[48,2048]{1,0:T(8,128)(2,1)S(1)}, u32[]{:S(2)}, u32[]{:S(2)}) collective-permute-start(bf16[48,2048]{1,0:T(8,128)(2,1)S(1)} %get-tuple-element.46), channel_id=1, source_target_pairs={{0,12},{1,9},{2,14},{3,11},{4,8},{5,13},{6,10},{7,15},{8,4},{9,1},... | collective-permute-start | bytes 589832 | tf_op jit(solution)/shard_map/ppermute | solution.py:266
  7.1 2.6 %collective-permute-start = (bf16[48,2048]{1,0:T(8,128)(2,1)S(1)}, bf16[48,2048]{1,0:T(8,128)(2,1)S(1)}, u32[]{:S(2)}, u32[]{:S(2)}) collective-permute-start(bf16[48,2048]{1,0:T(8,128)(2,1)S(1)} %get-tuple-element.37), channel_id=1, source_target_pairs={{0,16},{1,29},{2,22},{3,27},{4,20},{5,25},{6,18},{7,31},{8,24},{9,... | collective-permute-start | bytes 589832 | tf_op jit(solution)/shard_map/ppermute | solution.py:266
  9.7 4.1 %collective-permute-done.10.refs_1_ = bf16[48,2048]{1,0:T(8,128)(2,1)S(1)} collective-permute-done((bf16[48,2048]{1,0:T(8,128)(2,1)S(1)}, bf16[48,2048]{1,0:T(8,128)(2,1)S(1)}, u32[]{:S(2)}, u32[]{:S(2)}) %collective-permute-start.10) | collective-permute-done | bytes 196640 | tf_op jit(solution)/shard_map/ppermute | solution.py:266
  13.8 0.7 %shard_map.106 = (bf16[48,2048]{1,0:T(8,128)(2,1)S(1)}, bf16[48,2048]{1,0:T(8,128)(2,1)S(1)}) custom-call(bf16[48,2048]{1,0:T(8,128)(2,1)S(1)} %collective-permute-done.9.refs_0_, bf16[48,2048]{1,0:T(8,128)(2,1)S(1)} %collective-permute-done.10.refs_1_, bf16[2048,128]{1,0:T(8,128)(2,1)S(1)} %bitcast.7, bf16[2048,128]{1,0:T(8,128)(2,1)S(1)} %bitcast.11, ...), custom_call_target="tpu_custom_call" | custom-call | flops 301989888 | bytes 3932160 | tf_op jit(solution)/shard_map/pallas_call | solution.py:25
  14.6 0.7 %collective-permute-start.11 = (bf16[48,2048]{1,0:T(8,128)(2,1)S(1)}, bf16[48,2048]{1,0:T(8,128)(2,1)S(1)}, u32[]{:S(2)}, u32[]{:S(2)}) collective-permute-start(bf16[48,2048]{1,0:T(8,128)(2,1)S(1)} %get-tuple-element.47), channel_id=1, source_target_pairs={{0,0},{1,5},{2,2},{3,7},{4,4},{5,1},{6,6},{7,3},{8,8},{9,13},{10,1... | collective-permute-start | bytes 589832 | tf_op jit(solution)/shard_map/ppermute | solution.py:266
  15.2 1.1 %collective-permute-start.12 = (bf16[48,2048]{1,0:T(8,128)(2,1)S(1)}, bf16[48,2048]{1,0:T(8,128)(2,1)S(1)}, u32[]{:S(2)}, u32[]{:S(2)}) collective-permute-start(bf16[48,2048]{1,0:T(8,128)(2,1)S(1)} %get-tuple-element.48), channel_id=1, source_target_pairs={{0,12},{1,9},{2,14},{3,11},{4,8},{5,13},{6,10},{7,15},{8,4},{9,1},... | collective-permute-start | bytes 589832 | tf_op jit(solution)/shard_map/ppermute | solution.py:266
  16.3 1.5 %collective-permute-start.4 = (bf16[48,2048]{1,0:T(8,128)(2,1)S(1)}, bf16[48,2048]{1,0:T(8,128)(2,1)S(1)}, u32[]{:S(2)}, u32[]{:S(2)}) collective-permute-start(bf16[48,2048]{1,0:T(8,128)(2,1)S(1)} %collective-permute-done.refs_0_), channel_id=1, source_target_pairs={{0,2},{1,3},{2,0},{3,1},{4,6},{5,7},{6,4},{7,5},{8,10},{9,11},{10,... | collective-permute-start | bytes 589832 | tf_op jit(solution)/shard_map/ppermute | solution.py:293
  17.8 0.9 %shard_map.101 = (f32[128,2048]{1,0:T(8,128)S(1)}, bf16[128,96]{1,0:T(8,128)(2,1)S(1)}, bf16[128,96]{1,0:T(8,128)(2,1)S(1)}, bf16[128,96]{1,0:T(8,128)(2,1)S(1)}, bf16[128,96]{1,0:T(8,128)(2,1)S(1)}) custom-call(s32[2,128]{1,0:T(2,128)S(1)} %get-tuple-element.30.slots, bf16[128,2048]{1,0:T(8,128)(2,1)S(1)} %get-tuple-element.31.rows, ...), custom_call_target="tpu_custom_call" | custom-call | flops 201326592 | bytes 3246080 | tf_op jit(solution)/shard_map/pallas_call | solution.py:25
  18.8 3.8 %collective-permute-done.12.refs_1_ = bf16[48,2048]{1,0:T(8,128)(2,1)S(1)} collective-permute-done((bf16[48,2048]{1,0:T(8,128)(2,1)S(1)}, bf16[48,2048]{1,0:T(8,128)(2,1)S(1)}, u32[]{:S(2)}, u32[]{:S(2)}) %collective-permute-start.12) | collective-permute-done | bytes 196640 | tf_op jit(solution)/shard_map/ppermute | solution.py:266
  22.6 0.5 shard_map.107
  23.0 2.0 %collective-permute-start.13 = (bf16[128,1024]{1,0:T(8,128)(2,1)S(1)}, bf16[128,1024]{1,0:T(8,128)(2,1)S(1)}, u32[]{:S(2)}, u32[]{:S(2)}) collective-permute-start(bf16[128,1024]{1,0:T(8,128)(2,1)S(1)} %get-tuple-element.50), channel_id=1, source_target_pairs={{0,1},{1,0},{2,3},{3,2},{4,5},{5,4},{6,7},{7,6},{8,9},{9,8},{10,11... | collective-permute-start | bytes 786440 | tf_op jit(solution)/shard_map/ppermute | solution.py:323
  25.1 0.7 %shard_map.103 = (bf16[48,1024]{1,0:T(8,128)(2,1)S(1)}, f32[48,1024]{1,0:T(8,128)S(1)}) custom-call(bf16[48,2048]{1,0:T(8,128)(2,1)S(1)} %collective-permute-done.4.refs_0_, bf16[2048,128]{1,0:T(8,128)(2,1)S(1)} %bitcast.8, bf16[2048,128]{1,0:T(8,128)(2,1)S(1)} %bitcast.12, bf16[128,2048]{1,0:T(8,128)(2,1)S(1)} %bitcast.16, ...), custom_call_target="tpu_custom_call" | custom-call | flops 150994944 | bytes 3637248 | tf_op jit(solution)/shard_map/pallas_call | solution.py:25
  25.8 3.8 %collective-permute-start.5 = (bf16[48,1024]{1,0:T(8,128)(2,1)S(1)}, bf16[48,1024]{1,0:T(8,128)(2,1)S(1)}, u32[]{:S(2)}, u32[]{:S(2)}) collective-permute-start(bf16[48,1024]{1,0:T(8,128)(2,1)S(1)} %get-tuple-element.39), channel_id=1, source_target_pairs={{0,2},{1,3},{2,0},{3,1},{4,6},{5,7},{6,4},{7,5},{8,10},{9,11},{10,... | collective-permute-start | bytes 294920 | tf_op jit(solution)/shard_map/ppermute | solution.py:333
  29.6 0.7 %shard_map.102 = (bf16[48,1024]{1,0:T(8,128)(2,1)S(1)}, f32[48,1024]{1,0:T(8,128)S(1)}) custom-call(bf16[48,2048]{1,0:T(8,128)(2,1)S(1)} %collective-permute-done.refs_0_, bf16[2048,128]{1,0:T(8,128)(2,1)S(1)} %bitcast.9, bf16[2048,128]{1,0:T(8,128)(2,1)S(1)} %bitcast.13, bf16[128,2048]{1,0:T(8,128)(2,1)S(1)} %bitcast.17, ...), custom_call_target="tpu_custom_call" | custom-call | flops 150994944 | bytes 3637248 | tf_op jit(solution)/shard_map/pallas_call | solution.py:25
  30.4 0.1 collective-permute-start.7
  30.4 0.1 shard_map.108
  30.5 2.1 %collective-permute-start.14 = (bf16[128,512]{1,0:T(8,128)(2,1)S(1)}, bf16[128,512]{1,0:T(8,128)(2,1)S(1)}, u32[]{:S(2)}, u32[]{:S(2)}) collective-permute-start(bf16[128,512]{1,0:T(8,128)(2,1)S(1)} %get-tuple-element.52), channel_id=1, source_target_pairs={{0,2},{1,3},{2,0},{3,1},{4,6},{5,7},{6,4},{7,5},{8,10},{9,11},{10,... | collective-permute-start | bytes 393224 | tf_op jit(solution)/shard_map/ppermute | solution.py:326
  32.5 0.3 collective-permute-done.5.came
  32.8 1.5 %collective-permute-start.6 = (bf16[48,1024]{1,0:T(8,128)(2,1)S(1)}, bf16[48,1024]{1,0:T(8,128)(2,1)S(1)}, u32[]{:S(2)}, u32[]{:S(2)}) collective-permute-start(bf16[48,1024]{1,0:T(8,128)(2,1)S(1)} %shard_map.104), channel_id=1, source_target_pairs={{0,16},{1,29},{2,22},{3,27},{4,20},{5,25},{6,18},{7,31},{8,24},{9,... | collective-permute-start | bytes 294920 | tf_op jit(solution)/shard_map/ppermute | solution.py:266
  34.3 1.7 %collective-permute-done.7.came = bf16[48,1024]{1,0:T(8,128)(2,1)S(1)} collective-permute-done((bf16[48,1024]{1,0:T(8,128)(2,1)S(1)}, bf16[48,1024]{1,0:T(8,128)(2,1)S(1)}, u32[]{:S(2)}, u32[]{:S(2)}) %collective-permute-start.7) | collective-permute-done | bytes 98336 | tf_op jit(solution)/shard_map/ppermute | solution.py:333
  36.1 1.4 %collective-permute-start.8 = (bf16[48,1024]{1,0:T(8,128)(2,1)S(1)}, bf16[48,1024]{1,0:T(8,128)(2,1)S(1)}, u32[]{:S(2)}, u32[]{:S(2)}) collective-permute-start(bf16[48,1024]{1,0:T(8,128)(2,1)S(1)} %shard_map.105), channel_id=1, source_target_pairs={{0,20},{1,25},{2,18},{3,31},{4,16},{5,29},{6,22},{7,27},{8,28},{9,... | collective-permute-start | bytes 294920 | tf_op jit(solution)/shard_map/ppermute | solution.py:266
  37.5 5.5 %collective-permute-done.6.first = bf16[48,1024]{1,0:T(8,128)(2,1)S(1)} collective-permute-done((bf16[48,1024]{1,0:T(8,128)(2,1)S(1)}, bf16[48,1024]{1,0:T(8,128)(2,1)S(1)}, u32[]{:S(2)}, u32[]{:S(2)}) %collective-permute-start.6) | collective-permute-done | bytes 98336 | tf_op jit(solution)/shard_map/ppermute | solution.py:266
  43.0 1.9 %collective-permute-done.8.second = bf16[48,1024]{1,0:T(8,128)(2,1)S(1)} collective-permute-done((bf16[48,1024]{1,0:T(8,128)(2,1)S(1)}, bf16[48,1024]{1,0:T(8,128)(2,1)S(1)}, u32[]{:S(2)}, u32[]{:S(2)}) %collective-permute-start.8) | collective-permute-done | bytes 98336 | tf_op jit(solution)/shard_map/ppermute | solution.py:266
  44.9 0.3 shard_map.109
  45.2 0.1 collective-permute-start.15
  45.2 1.5 %collective-permute-done.15.came = f32[128,512]{1,0:T(8,128)S(1)} collective-permute-done((f32[128,512]{1,0:T(8,128)S(1)}, f32[128,512]{1,0:T(8,128)S(1)}, u32[]{:S(2)}, u32[]{:S(2)}) %collective-permute-start.15) | collective-permute-done | bytes 262176 | tf_op jit(solution)/shard_map/ppermute | solution.py:345
  46.8 0.7 %shard_map.110 = bf16[128,512]{1,0:T(8,128)(2,1)} custom-call(f32[128,512]{1,0:T(8,128)S(1)} %get-tuple-element.53.keep, f32[128,512]{1,0:T(8,128)S(1)} %collective-permute-done.15.came), custom_call_target="tpu_custom_call" | custom-call | flops 65536 | bytes 655360 | tf_op jit(solution)/shard_map/pallas_call | solution.py:25
  (17 shorter events, 0.1 us)
Async XLA Ops:
  0.0 13.8 %collective-permute-start.1 = (bf16[2048,128]{1,0:T(8,128)(2,1)}, bf16[2048,128]{1,0:T(8,128)(2,1)S(1)}, u32[]{:S(2)}, u32[]{:S(2)}) collective-permute-start(bf16[2048,128]{1,0:T(8,128)(2,1)} %bitcast.6), channel_id=1, source_target_pairs={{0,1},{1,0},{2,3},{3,2},{4,5},{5,4},{6,7},{7,6},{8,9},{9,8},{10,11... | collective-permute-start | bytes 1572872 | tf_op jit(solution)/shard_map/ppermute | solution.py:257
  0.5 13.3 %collective-permute-start.2 = (bf16[2048,128]{1,0:T(8,128)(2,1)}, bf16[2048,128]{1,0:T(8,128)(2,1)S(1)}, u32[]{:S(2)}, u32[]{:S(2)}) collective-permute-start(bf16[2048,128]{1,0:T(8,128)(2,1)} %bitcast.10), channel_id=1, source_target_pairs={{0,1},{1,0},{2,3},{3,2},{4,5},{5,4},{6,7},{7,6},{8,9},{9,8},{10,11... | collective-permute-start | bytes 1572872 | tf_op jit(solution)/shard_map/ppermute | solution.py:257
  0.5 13.3 %collective-permute-start.3 = (bf16[128,2048]{1,0:T(8,128)(2,1)}, bf16[128,2048]{1,0:T(8,128)(2,1)S(1)}, u32[]{:S(2)}, u32[]{:S(2)}) collective-permute-start(bf16[128,2048]{1,0:T(8,128)(2,1)} %bitcast.14), channel_id=1, source_target_pairs={{0,1},{1,0},{2,3},{3,2},{4,5},{5,4},{6,7},{7,6},{8,9},{9,8},{10,11... | collective-permute-start | bytes 1572872 | tf_op jit(solution)/shard_map/ppermute | solution.py:257
  1.0 12.8 %copy-start = (bf16[1,2048,128]{2,1,0:T(8,128)(2,1)S(1)}, bf16[1,2048,128]{2,1,0:T(8,128)(2,1)}, u32[]{:S(2)}) copy-start(bf16[1,2048,128]{2,1,0:T(8,128)(2,1)} %param.14) | copy-start | bytes 1572868
  1.0 12.8 %copy-start.1 = (bf16[1,2048,128]{2,1,0:T(8,128)(2,1)S(1)}, bf16[1,2048,128]{2,1,0:T(8,128)(2,1)}, u32[]{:S(2)}) copy-start(bf16[1,2048,128]{2,1,0:T(8,128)(2,1)} %param.15) | copy-start | bytes 1572868
  1.0 12.8 %copy-start.2 = (bf16[1,128,2048]{2,1,0:T(8,128)(2,1)S(1)}, bf16[1,128,2048]{2,1,0:T(8,128)(2,1)}, u32[]{:S(2)}) copy-start(bf16[1,128,2048]{2,1,0:T(8,128)(2,1)} %param.16) | copy-start | bytes 1572868
  2.8 4.3 %collective-permute-start.9 = (bf16[48,2048]{1,0:T(8,128)(2,1)S(1)}, bf16[48,2048]{1,0:T(8,128)(2,1)S(1)}, u32[]{:S(2)}, u32[]{:S(2)}) collective-permute-start(bf16[48,2048]{1,0:T(8,128)(2,1)S(1)} %get-tuple-element.45), channel_id=1, source_target_pairs={{0,0},{1,5},{2,2},{3,7},{4,4},{5,1},{6,6},{7,3},{8,8},{9,13},{10,1... | collective-permute-start | bytes 589832 | tf_op jit(solution)/shard_map/ppermute | solution.py:266
  3.5 10.3 %collective-permute-start.10 = (bf16[48,2048]{1,0:T(8,128)(2,1)S(1)}, bf16[48,2048]{1,0:T(8,128)(2,1)S(1)}, u32[]{:S(2)}, u32[]{:S(2)}) collective-permute-start(bf16[48,2048]{1,0:T(8,128)(2,1)S(1)} %get-tuple-element.46), channel_id=1, source_target_pairs={{0,12},{1,9},{2,14},{3,11},{4,8},{5,13},{6,10},{7,15},{8,4},{9,1},... | collective-permute-start | bytes 589832 | tf_op jit(solution)/shard_map/ppermute | solution.py:266
  7.1 9.2 %collective-permute-start = (bf16[48,2048]{1,0:T(8,128)(2,1)S(1)}, bf16[48,2048]{1,0:T(8,128)(2,1)S(1)}, u32[]{:S(2)}, u32[]{:S(2)}) collective-permute-start(bf16[48,2048]{1,0:T(8,128)(2,1)S(1)} %get-tuple-element.37), channel_id=1, source_target_pairs={{0,16},{1,29},{2,22},{3,27},{4,20},{5,25},{6,18},{7,31},{8,24},{9,... | collective-permute-start | bytes 589832 | tf_op jit(solution)/shard_map/ppermute | solution.py:266
  14.6 4.2 %collective-permute-start.11 = (bf16[48,2048]{1,0:T(8,128)(2,1)S(1)}, bf16[48,2048]{1,0:T(8,128)(2,1)S(1)}, u32[]{:S(2)}, u32[]{:S(2)}) collective-permute-start(bf16[48,2048]{1,0:T(8,128)(2,1)S(1)} %get-tuple-element.47), channel_id=1, source_target_pairs={{0,0},{1,5},{2,2},{3,7},{4,4},{5,1},{6,6},{7,3},{8,8},{9,13},{10,1... | collective-permute-start | bytes 589832 | tf_op jit(solution)/shard_map/ppermute | solution.py:266
  15.2 7.3 %collective-permute-start.12 = (bf16[48,2048]{1,0:T(8,128)(2,1)S(1)}, bf16[48,2048]{1,0:T(8,128)(2,1)S(1)}, u32[]{:S(2)}, u32[]{:S(2)}) collective-permute-start(bf16[48,2048]{1,0:T(8,128)(2,1)S(1)} %get-tuple-element.48), channel_id=1, source_target_pairs={{0,12},{1,9},{2,14},{3,11},{4,8},{5,13},{6,10},{7,15},{8,4},{9,1},... | collective-permute-start | bytes 589832 | tf_op jit(solution)/shard_map/ppermute | solution.py:266
  16.3 8.7 %collective-permute-start.4 = (bf16[48,2048]{1,0:T(8,128)(2,1)S(1)}, bf16[48,2048]{1,0:T(8,128)(2,1)S(1)}, u32[]{:S(2)}, u32[]{:S(2)}) collective-permute-start(bf16[48,2048]{1,0:T(8,128)(2,1)S(1)} %collective-permute-done.refs_0_), channel_id=1, source_target_pairs={{0,2},{1,3},{2,0},{3,1},{4,6},{5,7},{6,4},{7,5},{8,10},{9,11},{10,... | collective-permute-start | bytes 589832 | tf_op jit(solution)/shard_map/ppermute | solution.py:293
  23.0 7.4 %collective-permute-start.13 = (bf16[128,1024]{1,0:T(8,128)(2,1)S(1)}, bf16[128,1024]{1,0:T(8,128)(2,1)S(1)}, u32[]{:S(2)}, u32[]{:S(2)}) collective-permute-start(bf16[128,1024]{1,0:T(8,128)(2,1)S(1)} %get-tuple-element.50), channel_id=1, source_target_pairs={{0,1},{1,0},{2,3},{3,2},{4,5},{5,4},{6,7},{7,6},{8,9},{9,8},{10,11... | collective-permute-start | bytes 786440 | tf_op jit(solution)/shard_map/ppermute | solution.py:323
  25.8 7.0 %collective-permute-start.5 = (bf16[48,1024]{1,0:T(8,128)(2,1)S(1)}, bf16[48,1024]{1,0:T(8,128)(2,1)S(1)}, u32[]{:S(2)}, u32[]{:S(2)}) collective-permute-start(bf16[48,1024]{1,0:T(8,128)(2,1)S(1)} %get-tuple-element.39), channel_id=1, source_target_pairs={{0,2},{1,3},{2,0},{3,1},{4,6},{5,7},{6,4},{7,5},{8,10},{9,11},{10,... | collective-permute-start | bytes 294920 | tf_op jit(solution)/shard_map/ppermute | solution.py:333
  30.4 5.7 %collective-permute-start.7 = (bf16[48,1024]{1,0:T(8,128)(2,1)S(1)}, bf16[48,1024]{1,0:T(8,128)(2,1)S(1)}, u32[]{:S(2)}, u32[]{:S(2)}) collective-permute-start(bf16[48,1024]{1,0:T(8,128)(2,1)S(1)} %get-tuple-element.41), channel_id=1, source_target_pairs={{0,2},{1,3},{2,0},{3,1},{4,6},{5,7},{6,4},{7,5},{8,10},{9,11},{10,... | collective-permute-start | bytes 294920 | tf_op jit(solution)/shard_map/ppermute | solution.py:333
  30.5 14.4 %collective-permute-start.14 = (bf16[128,512]{1,0:T(8,128)(2,1)S(1)}, bf16[128,512]{1,0:T(8,128)(2,1)S(1)}, u32[]{:S(2)}, u32[]{:S(2)}) collective-permute-start(bf16[128,512]{1,0:T(8,128)(2,1)S(1)} %get-tuple-element.52), channel_id=1, source_target_pairs={{0,2},{1,3},{2,0},{3,1},{4,6},{5,7},{6,4},{7,5},{8,10},{9,11},{10,... | collective-permute-start | bytes 393224 | tf_op jit(solution)/shard_map/ppermute | solution.py:326
  32.8 10.2 %collective-permute-start.6 = (bf16[48,1024]{1,0:T(8,128)(2,1)S(1)}, bf16[48,1024]{1,0:T(8,128)(2,1)S(1)}, u32[]{:S(2)}, u32[]{:S(2)}) collective-permute-start(bf16[48,1024]{1,0:T(8,128)(2,1)S(1)} %shard_map.104), channel_id=1, source_target_pairs={{0,16},{1,29},{2,22},{3,27},{4,20},{5,25},{6,18},{7,31},{8,24},{9,... | collective-permute-start | bytes 294920 | tf_op jit(solution)/shard_map/ppermute | solution.py:266
  36.1 8.8 %collective-permute-start.8 = (bf16[48,1024]{1,0:T(8,128)(2,1)S(1)}, bf16[48,1024]{1,0:T(8,128)(2,1)S(1)}, u32[]{:S(2)}, u32[]{:S(2)}) collective-permute-start(bf16[48,1024]{1,0:T(8,128)(2,1)S(1)} %shard_map.105), channel_id=1, source_target_pairs={{0,20},{1,25},{2,18},{3,31},{4,16},{5,29},{6,22},{7,27},{8,28},{9,... | collective-permute-start | bytes 294920 | tf_op jit(solution)/shard_map/ppermute | solution.py:266
  45.2 1.6 %collective-permute-start.15 = (f32[128,512]{1,0:T(8,128)S(1)}, f32[128,512]{1,0:T(8,128)S(1)}, u32[]{:S(2)}, u32[]{:S(2)}) collective-permute-start(f32[128,512]{1,0:T(8,128)S(1)} %get-tuple-element.54), channel_id=1, source_target_pairs={{0,1},{1,0},{2,3},{3,2},{4,5},{5,4},{6,7},{7,6},{8,9},{9,8},{10,11... | collective-permute-start | bytes 786440 | tf_op jit(solution)/shard_map/ppermute | solution.py:345

commit v4 on v3

--- a/solution.py
+++ b/solution.py
@@ -50,8 +50,8 @@
     return jax.ShapeDtypeStruct((rows, columns), dtype)
 
 
-def slot_of(label, rank, capacity, direct):
-    core, side = lax.axis_index("tp") % 2, lax.axis_index("tp") // 2
+def slot_of(label, rank, capacity, direct, flip=0):
+    core, side = (lax.axis_index("tp") % 2) ^ flip, lax.axis_index("tp") // 2
     if direct:
         near = label < 4
         holder = jnp.where(near, (label ^ (label >> 1)) & 1, (label >> 1) & 1)
@@ -90,6 +90,10 @@
         base = base + jnp.sum(onehot, axis=1, keepdims=True)
         where = slot_of(label, rank, capacity, direct)
         slots_out[j : j + 1, :] = where
+        if direct:
+            there = slot_of(label, rank, capacity, direct, 1)
+            there = jnp.where(there >= 2 * capacity, there + 2 * capacity, -1)
+            slots_out[j : j + 1, :] = jnp.maximum(where, there)
         hit = jnp.where(slot == where, 1.0, hit)
     pick = hit.astype(bf16)
     copies[1].wait()
@@ -212,22 +216,20 @@
 
 
 def add_body(keep, came, *outs):
-    at = 0
-    for out in outs:
-        n = out.shape[0]
-        out[...] = (keep[at : at + n] + came[at : at + n].astype(f32)).astype(out.dtype)
-        at += n
-
-
-def mix_body(high, low, first, second, mine, came, *refs):
-    outs, room = refs[:2], refs[2]
-    gathered = gather_rows((first, second), room)
+    if len(outs) == 1:
+        outs[0][...] = (keep[...] + came[...].astype(f32)).astype(outs[0].dtype)
+        return
     width = outs[0].shape[1]
     core = lax.axis_index("tp") % 2
     for out, place in ((outs[0], core), (outs[1], 1 - core)):
         columns = pl.ds(pl.multiple_of(place * width, width), width)
-        total = picked(high, low, gathered[:, columns])
-        out[...] = total + mine[...] + came[...].astype(f32) if out is outs[0] else total
+        out[...] = (keep[:, columns] + came[:, columns].astype(f32)).astype(out.dtype)
+
+
+def mix_body(high, low, mine, came, *refs):
+    out, room = refs[-2:]
+    rows = gather_rows(refs[:-2], room)[...]
+    out[...] = (picked(high, low, rows) + mine[...] + came[...].astype(f32)).astype(out.dtype)
 
 
 def local(
@@ -256,13 +258,14 @@
     own = (gate_weight[0], up_weight[0], down_weight[0])
     other = tuple(lax.ppermute(w, "tp", sibling) for w in own)
 
-    def hop(block, between):
+    def hop(block, between, flip=0):
         if not direct:
             return lax.all_to_all(block, "ep", split_axis=0, concat_axis=0, tiled=True)
         pairs = []
         for i in range(groups):
             for t in range(cuts):
-                pairs.append((i * cuts + t, (i ^ between(t // 2, t % 2)) * cuts + t))
+                to = i ^ between(t // 2, t % 2)
+                pairs.append((i * cuts + t, to * cuts + (t ^ flip)))
         return lax.ppermute(block, ("ep", "tp"), pairs)
 
     distances = {
@@ -294,7 +297,7 @@
     near = [k for k in sizes if k in ("P", "Q")]
     spans = [sum(sizes[k] for k in near)]
     if direct:
-        spans.append(total - spans[0])
+        spans.append(2 * (total - spans[0]))
     gains = route_weights.T
     part, *weights = call(
         shared_body,
@@ -331,18 +334,22 @@
             outs = [shape(capacity, wide, bf16), shape(capacity, wide, f32)]
             sent[k], kept[k] = products(product_body, [arrived[k]], [*own, *other], outs)
             sent[k] = lax.ppermute(sent[k], "tp", neighbour)
+        far_rows = {}
         for k, other_k in ("AB", "BA"):
             ins = [kept[k], sent[other_k]]
-            (out,) = call(add_body, [shape(capacity, wide, bf16)], ins, kept[k].size)
-            returned[k] = hop(out, distances[k])
-        mine, send = call(
+            outs = [shape(capacity, share, bf16)] * 2
+            outs = call(add_body, outs, ins, kept[k].size)
+            for flip, out in enumerate(outs):
+                far_rows[k, flip] = hop(out, distances[k], flip)
+        rows = [far_rows[k, flip] for flip in range(2) for k in "AB"]
+        (mixed,) = call(
             mix_body,
-            [shape(rows_here, share, f32), shape(rows_here, share, f32)],
-            [*weights[2:], returned["A"], returned["B"], mine, came],
-            4 * rows_here * wide * spans[1],
-            [pltpu.VMEM((spans[1], wide), bf16)],
+            [shape(rows_here, share, bf16)],
+            [*weights[2:], mine, came, *rows],
+            4 * rows_here * share * spans[1],
+            [pltpu.VMEM((spans[1], share), bf16)],
         )
-        came = lax.ppermute(send, "tp", sibling)
+        return mixed
     (mixed,) = call(add_body, [shape(rows_here, share, bf16)], [mine, came], mine.size)
     return mixed
 

time: 47.6 us -> 54.9 us (1.15)
  the two profiles are of different devices: /device:TPU:0 before, /device:TPU:1 now
where the time goes in v4:
time: 54.9 us; the launch traced here: 54.8 us
  starting transfers between devices  27.6 us (50%)
  waiting for transfers between devices  20.6 us (38%)
  Pallas kernels  6.42 us (12%)
    ppermute x9, starting transfers between devices, hop(): return lax.ppermute(block, ('ep', 'tp'), pairs)  22.7 us
    ppermute x9, waiting for transfers between devices, hop(): return lax.ppermute(block, ('ep', 'tp'), pairs)  16.8 us
    pallas_call x10, Pallas kernels, call(): pl.pallas_call(body, out_shape=outs, in_specs=[hbm if i in far else vmem...  6.42 us
    ppermute x1, waiting for transfers between devices, local(): arrived['B'] = lax.ppermute(arrived['A'], 'tp', neighbour)  3.77 us
    ppermute x2, starting transfers between devices, local(): sent[k] = lax.ppermute(sent[k], 'tp', neighbour)  1.55 us
    ppermute x1, starting transfers between devices, local(): arrived['B'] = lax.ppermute(arrived['A'], 'tp', neighbour)  1.55 us
    ppermute x1, starting transfers between devices, local(): came = lax.ppermute(send, 'tp', neighbour)  1.24 us
  transfers between devices with their start and end apart: 17, of which 8 were waited for; matrix products, arithmetic and copies ran while one was open for 0% of the time, Pallas kernels for 9%

profile of v4, /device:TPU:1, one launch (start us, length us, event | category | flops | bytes accessed | tf_op | source)
XLA Modules:
  0.0 54.8 jit_solution(13655248622226868111)
XLA Ops:
  0.0 0.5 collective-permute-start.3
  0.5 1.8 %shard_map.100 = (bf16[128,2048]{1,0:T(8,128)(2,1)S(1)}, s32[2,128]{1,0:T(2,128)S(1)}, bf16[2048,128]{1,0:T(8,128)(2,1)S(1)}, bf16[2048,128]{1,0:T(8,128)(2,1)S(...) custom-call(s32[2,128]{1,0:T(2,128)} %bitcast.20, ...), custom_call_target="tpu_custom_call" | custom-call | flops 100663296 | bytes 4790272 | tf_op jit(solution)/shard_map/pallas_call | solution.py:25
  2.4 4.6 %collective-permute-start = (bf16[48,2048]{1,0:T(8,128)(2,1)S(1)}, bf16[48,2048]{1,0:T(8,128)(2,1)S(1)}, u32[]{:S(2)}, u32[]{:S(2)}) collective-permute-start(bf16[48,2048]{1,0:T(8,128)(2,1)S(1)} %get-tuple-element.42), channel_id=1, source_target_pairs={{0,0},{1,5},{2,2},{3,7},{4,4},{5,1},{6,6},{7,3},{8,8},{9,13},{10,1... | collective-permute-start | bytes 589832 | tf_op jit(solution)/shard_map/ppermute | solution.py:269
  7.0 1.4 %collective-permute-start.1 = (bf16[48,2048]{1,0:T(8,128)(2,1)S(1)}, bf16[48,2048]{1,0:T(8,128)(2,1)S(1)}, u32[]{:S(2)}, u32[]{:S(2)}) collective-permute-start(bf16[48,2048]{1,0:T(8,128)(2,1)S(1)} %get-tuple-element.43), channel_id=1, source_target_pairs={{0,12},{1,9},{2,14},{3,11},{4,8},{5,13},{6,10},{7,15},{8,4},{9,1},... | collective-permute-start | bytes 589832 | tf_op jit(solution)/shard_map/ppermute | solution.py:269
  8.4 3.8 %collective-permute-done.refs_0_ = bf16[48,2048]{1,0:T(8,128)(2,1)S(1)} collective-permute-done((bf16[48,2048]{1,0:T(8,128)(2,1)S(1)}, bf16[48,2048]{1,0:T(8,128)(2,1)S(1)}, u32[]{:S(2)}, u32[]{:S(2)}) %collective-permute-start) | collective-permute-done | bytes 196640 | tf_op jit(solution)/shard_map/ppermute | solution.py:269
  12.1 0.5 collective-permute-done.1.refs_1_
  12.7 0.7 %shard_map.102 = (bf16[48,2048]{1,0:T(8,128)(2,1)S(1)}, bf16[48,2048]{1,0:T(8,128)(2,1)S(1)}) custom-call(bf16[48,2048]{1,0:T(8,128)(2,1)S(1)} %collective-permute-done.refs_0_, bf16[48,2048]{1,0:T(8,128)(2,1)S(1)} %collective-permute-done.1.refs_1_, bf16[2048,128]{1,0:T(8,128)(2,1)S(1)} %bitcast.7, bf16[2048,128]{1,0:T(8,128)(2,1)S(1)} %bitcast.11, ...), custom_call_target="tpu_custom_call" | custom-call | flops 301989888 | bytes 3932160 | tf_op jit(solution)/shard_map/pallas_call | solution.py:25
  13.5 2.8 %collective-permute-start.5 = (bf16[48,2048]{1,0:T(8,128)(2,1)S(1)}, bf16[48,2048]{1,0:T(8,128)(2,1)S(1)}, u32[]{:S(2)}, u32[]{:S(2)}) collective-permute-start(bf16[48,2048]{1,0:T(8,128)(2,1)S(1)} %get-tuple-element.44), channel_id=1, source_target_pairs={{0,0},{1,5},{2,2},{3,7},{4,4},{5,1},{6,6},{7,3},{8,8},{9,13},{10,1... | collective-permute-start | bytes 589832 | tf_op jit(solution)/shard_map/ppermute | solution.py:269
  16.3 1.4 %collective-permute-start.6 = (bf16[48,2048]{1,0:T(8,128)(2,1)S(1)}, bf16[48,2048]{1,0:T(8,128)(2,1)S(1)}, u32[]{:S(2)}, u32[]{:S(2)}) collective-permute-start(bf16[48,2048]{1,0:T(8,128)(2,1)S(1)} %get-tuple-element.45), channel_id=1, source_target_pairs={{0,12},{1,9},{2,14},{3,11},{4,8},{5,13},{6,10},{7,15},{8,4},{9,1},... | collective-permute-start | bytes 589832 | tf_op jit(solution)/shard_map/ppermute | solution.py:269
  17.7 2.5 %collective-permute-start.9 = (bf16[48,2048]{1,0:T(8,128)(2,1)S(1)}, bf16[48,2048]{1,0:T(8,128)(2,1)S(1)}, u32[]{:S(2)}, u32[]{:S(2)}) collective-permute-start(bf16[48,2048]{1,0:T(8,128)(2,1)S(1)} %get-tuple-element.50), channel_id=1, source_target_pairs={{0,16},{1,29},{2,22},{3,27},{4,20},{5,25},{6,18},{7,31},{8,24},{9,... | collective-permute-start | bytes 589832 | tf_op jit(solution)/shard_map/ppermute | solution.py:269
  20.1 0.9 %shard_map.101 = (f32[128,2048]{1,0:T(8,128)S(1)}, bf16[128,96]{1,0:T(8,128)(2,1)S(1)}, bf16[128,96]{1,0:T(8,128)(2,1)S(1)}, bf16[128,192]{1,0:T(8,128)(2,1)S(1)}, bf16[128,192]{1,0:T(8,128)(2,1)S(1)}) custom-call(s32[2,128]{1,0:T(2,128)S(1)} %get-tuple-element.32.slots, bf16[128,2048]{1,0:T(8,128)(2,1)S(1)} %get-tuple-element.33.rows, ...), custom_call_target="tpu_custom_call" | custom-call | flops 201326592 | bytes 3295232 | tf_op jit(solution)/shard_map/pallas_call | solution.py:25
  21.1 0.6 %collective-permute-done.5.refs_0_ = bf16[48,2048]{1,0:T(8,128)(2,1)S(1)} collective-permute-done((bf16[48,2048]{1,0:T(8,128)(2,1)S(1)}, bf16[48,2048]{1,0:T(8,128)(2,1)S(1)}, u32[]{:S(2)}, u32[]{:S(2)}) %collective-permute-start.5) | collective-permute-done | bytes 196640 | tf_op jit(solution)/shard_map/ppermute | solution.py:269
  21.7 2.5 %collective-permute-done.6.refs_1_ = bf16[48,2048]{1,0:T(8,128)(2,1)S(1)} collective-permute-done((bf16[48,2048]{1,0:T(8,128)(2,1)S(1)}, bf16[48,2048]{1,0:T(8,128)(2,1)S(1)}, u32[]{:S(2)}, u32[]{:S(2)}) %collective-permute-start.6) | collective-permute-done | bytes 196640 | tf_op jit(solution)/shard_map/ppermute | solution.py:269
  24.3 0.5 shard_map.103
  24.7 0.1 collective-permute-start.7
  24.8 3.4 %collective-permute-done.9.refs_0_ = bf16[48,2048]{1,0:T(8,128)(2,1)S(1)} collective-permute-done((bf16[48,2048]{1,0:T(8,128)(2,1)S(1)}, bf16[48,2048]{1,0:T(8,128)(2,1)S(1)}, u32[]{:S(2)}, u32[]{:S(2)}) %collective-permute-start.9) | collective-permute-done | bytes 196640 | tf_op jit(solution)/shard_map/ppermute | solution.py:269
  28.2 1.5 %collective-permute-start.10 = (bf16[48,2048]{1,0:T(8,128)(2,1)S(1)}, bf16[48,2048]{1,0:T(8,128)(2,1)S(1)}, u32[]{:S(2)}, u32[]{:S(2)}) collective-permute-start(bf16[48,2048]{1,0:T(8,128)(2,1)S(1)} %collective-permute-done.9.refs_0_), channel_id=1, source_target_pairs={{0,2},{1,3},{2,0},{3,1},{4,6},{5,7},{6,4},{7,5},{8,10},{9,11},{10,... | collective-permute-start | bytes 589832 | tf_op jit(solution)/shard_map/ppermute | solution.py:296
  29.7 3.8 %collective-permute-done.10.refs_0_ = bf16[48,2048]{1,0:T(8,128)(2,1)S(1)} collective-permute-done((bf16[48,2048]{1,0:T(8,128)(2,1)S(1)}, bf16[48,2048]{1,0:T(8,128)(2,1)S(1)}, u32[]{:S(2)}, u32[]{:S(2)}) %collective-permute-start.10) | collective-permute-done | bytes 196640 | tf_op jit(solution)/shard_map/ppermute | solution.py:296
  33.5 0.7 %shard_map.106 = (bf16[48,1024]{1,0:T(8,128)(2,1)S(1)}, f32[48,1024]{1,0:T(8,128)S(1)}) custom-call(bf16[48,2048]{1,0:T(8,128)(2,1)S(1)} %collective-permute-done.10.refs_0_, bf16[2048,128]{1,0:T(8,128)(2,1)S(1)} %bitcast.8, bf16[2048,128]{1,0:T(8,128)(2,1)S(1)} %bitcast.12, bf16[128,2048]{1,0:T(8,128)(2,1)S(1)} %bitcast.16, ...), custom_call_target="tpu_custom_call" | custom-call | flops 150994944 | bytes 3637248 | tf_op jit(solution)/shard_map/pallas_call | solution.py:25
  34.2 1.2 %collective-permute-start.11 = (bf16[48,1024]{1,0:T(8,128)(2,1)S(1)}, bf16[48,1024]{1,0:T(8,128)(2,1)S(1)}, u32[]{:S(2)}, u32[]{:S(2)}) collective-permute-start(bf16[48,1024]{1,0:T(8,128)(2,1)S(1)} %get-tuple-element.52), channel_id=1, source_target_pairs={{0,2},{1,3},{2,0},{3,1},{4,6},{5,7},{6,4},{7,5},{8,10},{9,11},{10,... | collective-permute-start | bytes 294920 | tf_op jit(solution)/shard_map/ppermute | solution.py:336
  35.4 0.7 %shard_map.105 = (bf16[48,1024]{1,0:T(8,128)(2,1)S(1)}, f32[48,1024]{1,0:T(8,128)S(1)}) custom-call(bf16[48,2048]{1,0:T(8,128)(2,1)S(1)} %collective-permute-done.9.refs_0_, bf16[2048,128]{1,0:T(8,128)(2,1)S(1)} %bitcast.9, bf16[2048,128]{1,0:T(8,128)(2,1)S(1)} %bitcast.13, bf16[128,2048]{1,0:T(8,128)(2,1)S(1)} %bitcast.17, ...), custom_call_target="tpu_custom_call" | custom-call | flops 150994944 | bytes 3637248 | tf_op jit(solution)/shard_map/pallas_call | solution.py:25
  36.2 0.3 collective-permute-start.13
  36.5 0.1 shard_map.104
  36.6 1.2 %collective-permute-start.8 = (bf16[128,512]{1,0:T(8,128)(2,1)S(1)}, bf16[128,512]{1,0:T(8,128)(2,1)S(1)}, u32[]{:S(2)}, u32[]{:S(2)}) collective-permute-start(bf16[128,512]{1,0:T(8,128)(2,1)S(1)} %get-tuple-element.49), channel_id=1, source_target_pairs={{0,2},{1,3},{2,0},{3,1},{4,6},{5,7},{6,4},{7,5},{8,10},{9,11},{10,... | collective-permute-start | bytes 393224 | tf_op jit(solution)/shard_map/ppermute | solution.py:329
  37.8 2.6 %collective-permute-start.12 = (bf16[48,512]{1,0:T(8,128)(2,1)S(1)}, bf16[48,512]{1,0:T(8,128)(2,1)S(1)}, u32[]{:S(2)}, u32[]{:S(2)}) collective-permute-start(bf16[48,512]{1,0:T(8,128)(2,1)S(1)} %get-tuple-element.53), channel_id=1, source_target_pairs={{0,16},{1,29},{2,22},{3,27},{4,20},{5,25},{6,18},{7,31},{8,24},{9,... | collective-permute-start | bytes 147464 | tf_op jit(solution)/shard_map/ppermute | solution.py:269
  40.4 0.0 collective-permute-done.13.came
  40.5 0.9 %collective-permute-start.14 = (bf16[48,512]{1,0:T(8,128)(2,1)S(1)}, bf16[48,512]{1,0:T(8,128)(2,1)S(1)}, u32[]{:S(2)}, u32[]{:S(2)}) collective-permute-start(bf16[48,512]{1,0:T(8,128)(2,1)S(1)} %get-tuple-element.56), channel_id=1, source_target_pairs={{0,20},{1,25},{2,18},{3,31},{4,16},{5,29},{6,22},{7,27},{8,28},{9,... | collective-permute-start | bytes 147464 | tf_op jit(solution)/shard_map/ppermute | solution.py:269
  41.4 6.0 %collective-permute-start.15 = (bf16[48,512]{1,0:T(8,128)(2,1)S(1)}, bf16[48,512]{1,0:T(8,128)(2,1)S(1)}, u32[]{:S(2)}, u32[]{:S(2)}) collective-permute-start(bf16[48,512]{1,0:T(8,128)(2,1)S(1)} %get-tuple-element.57), channel_id=1, source_target_pairs={{0,17},{1,28},{2,23},{3,26},{4,21},{5,24},{6,19},{7,30},{8,25},{9,... | collective-permute-start | bytes 147464 | tf_op jit(solution)/shard_map/ppermute | solution.py:269
  47.4 0.6 %collective-permute-start.16 = (bf16[48,512]{1,0:T(8,128)(2,1)S(1)}, bf16[48,512]{1,0:T(8,128)(2,1)S(1)}, u32[]{:S(2)}, u32[]{:S(2)}) collective-permute-start(bf16[48,512]{1,0:T(8,128)(2,1)S(1)} %get-tuple-element.58), channel_id=1, source_target_pairs={{0,21},{1,24},{2,19},{3,30},{4,17},{5,28},{6,23},{7,26},{8,29},{9,... | collective-permute-start | bytes 147464 | tf_op jit(solution)/shard_map/ppermute | solution.py:269
  48.0 0.6 %collective-permute-done.15.refs_2_ = bf16[48,512]{1,0:T(8,128)(2,1)S(1)} collective-permute-done((bf16[48,512]{1,0:T(8,128)(2,1)S(1)}, bf16[48,512]{1,0:T(8,128)(2,1)S(1)}, u32[]{:S(2)}, u32[]{:S(2)}) %collective-permute-start.15) | collective-permute-done | bytes 49184 | tf_op jit(solution)/shard_map/ppermute | solution.py:269
  48.6 5.3 %collective-permute-done.16.refs_3_ = bf16[48,512]{1,0:T(8,128)(2,1)S(1)} collective-permute-done((bf16[48,512]{1,0:T(8,128)(2,1)S(1)}, bf16[48,512]{1,0:T(8,128)(2,1)S(1)}, u32[]{:S(2)}, u32[]{:S(2)}) %collective-permute-start.16) | collective-permute-done | bytes 49184 | tf_op jit(solution)/shard_map/ppermute | solution.py:269
  53.9 0.9 %shard_map.109 = bf16[128,512]{1,0:T(8,128)(2,1)} custom-call(bf16[128,192]{1,0:T(8,128)(2,1)S(1)} %get-tuple-element.37.high, bf16[128,192]{1,0:T(8,128)(2,1)S(1)} %get-tuple-element.38.low, f32[128,512]{1,0:T(8,128)S(1)} %get-tuple-element.48.mine, bf16[128,512]{1,0:T(8,128)(2,1)S(1)} %collective-permute-done.8.came, ...), custom_call_target="tpu_custom_call" | custom-call | flops 50331648 | bytes 819200 | tf_op jit(solution)/shard_map/pallas_call | solution.py:25
  (18 shorter events, 0.1 us)
Async XLA Ops:
  0.0 12.7 %collective-permute-start.2 = (bf16[2048,128]{1,0:T(8,128)(2,1)}, bf16[2048,128]{1,0:T(8,128)(2,1)S(1)}, u32[]{:S(2)}, u32[]{:S(2)}) collective-permute-start(bf16[2048,128]{1,0:T(8,128)(2,1)} %bitcast.6), channel_id=1, source_target_pairs={{0,1},{1,0},{2,3},{3,2},{4,5},{5,4},{6,7},{7,6},{8,9},{9,8},{10,11... | collective-permute-start | bytes 1572872 | tf_op jit(solution)/shard_map/ppermute | solution.py:259
  0.0 12.7 %collective-permute-start.3 = (bf16[2048,128]{1,0:T(8,128)(2,1)}, bf16[2048,128]{1,0:T(8,128)(2,1)S(1)}, u32[]{:S(2)}, u32[]{:S(2)}) collective-permute-start(bf16[2048,128]{1,0:T(8,128)(2,1)} %bitcast.10), channel_id=1, source_target_pairs={{0,1},{1,0},{2,3},{3,2},{4,5},{5,4},{6,7},{7,6},{8,9},{9,8},{10,11... | collective-permute-start | bytes 1572872 | tf_op jit(solution)/shard_map/ppermute | solution.py:259
  0.5 12.2 %collective-permute-start.4 = (bf16[128,2048]{1,0:T(8,128)(2,1)}, bf16[128,2048]{1,0:T(8,128)(2,1)S(1)}, u32[]{:S(2)}, u32[]{:S(2)}) collective-permute-start(bf16[128,2048]{1,0:T(8,128)(2,1)} %bitcast.14), channel_id=1, source_target_pairs={{0,1},{1,0},{2,3},{3,2},{4,5},{5,4},{6,7},{7,6},{8,9},{9,8},{10,11... | collective-permute-start | bytes 1572872 | tf_op jit(solution)/shard_map/ppermute | solution.py:259
  0.5 12.2 %copy-start = (bf16[1,2048,128]{2,1,0:T(8,128)(2,1)S(1)}, bf16[1,2048,128]{2,1,0:T(8,128)(2,1)}, u32[]{:S(2)}) copy-start(bf16[1,2048,128]{2,1,0:T(8,128)(2,1)} %param.14) | copy-start | bytes 1572868
  0.5 12.2 %copy-start.1 = (bf16[1,2048,128]{2,1,0:T(8,128)(2,1)S(1)}, bf16[1,2048,128]{2,1,0:T(8,128)(2,1)}, u32[]{:S(2)}) copy-start(bf16[1,2048,128]{2,1,0:T(8,128)(2,1)} %param.15) | copy-start | bytes 1572868
  0.5 12.2 %copy-start.2 = (bf16[1,128,2048]{2,1,0:T(8,128)(2,1)S(1)}, bf16[1,128,2048]{2,1,0:T(8,128)(2,1)}, u32[]{:S(2)}) copy-start(bf16[1,128,2048]{2,1,0:T(8,128)(2,1)} %param.16) | copy-start | bytes 1572868
  2.4 9.8 %collective-permute-start = (bf16[48,2048]{1,0:T(8,128)(2,1)S(1)}, bf16[48,2048]{1,0:T(8,128)(2,1)S(1)}, u32[]{:S(2)}, u32[]{:S(2)}) collective-permute-start(bf16[48,2048]{1,0:T(8,128)(2,1)S(1)} %get-tuple-element.42), channel_id=1, source_target_pairs={{0,0},{1,5},{2,2},{3,7},{4,4},{5,1},{6,6},{7,3},{8,8},{9,13},{10,1... | collective-permute-start | bytes 589832 | tf_op jit(solution)/shard_map/ppermute | solution.py:269
  7.0 5.7 %collective-permute-start.1 = (bf16[48,2048]{1,0:T(8,128)(2,1)S(1)}, bf16[48,2048]{1,0:T(8,128)(2,1)S(1)}, u32[]{:S(2)}, u32[]{:S(2)}) collective-permute-start(bf16[48,2048]{1,0:T(8,128)(2,1)S(1)} %get-tuple-element.43), channel_id=1, source_target_pairs={{0,12},{1,9},{2,14},{3,11},{4,8},{5,13},{6,10},{7,15},{8,4},{9,1},... | collective-permute-start | bytes 589832 | tf_op jit(solution)/shard_map/ppermute | solution.py:269
  13.5 8.3 %collective-permute-start.5 = (bf16[48,2048]{1,0:T(8,128)(2,1)S(1)}, bf16[48,2048]{1,0:T(8,128)(2,1)S(1)}, u32[]{:S(2)}, u32[]{:S(2)}) collective-permute-start(bf16[48,2048]{1,0:T(8,128)(2,1)S(1)} %get-tuple-element.44), channel_id=1, source_target_pairs={{0,0},{1,5},{2,2},{3,7},{4,4},{5,1},{6,6},{7,3},{8,8},{9,13},{10,1... | collective-permute-start | bytes 589832 | tf_op jit(solution)/shard_map/ppermute | solution.py:269
  16.3 7.9 %collective-permute-start.6 = (bf16[48,2048]{1,0:T(8,128)(2,1)S(1)}, bf16[48,2048]{1,0:T(8,128)(2,1)S(1)}, u32[]{:S(2)}, u32[]{:S(2)}) collective-permute-start(bf16[48,2048]{1,0:T(8,128)(2,1)S(1)} %get-tuple-element.45), channel_id=1, source_target_pairs={{0,12},{1,9},{2,14},{3,11},{4,8},{5,13},{6,10},{7,15},{8,4},{9,1},... | collective-permute-start | bytes 589832 | tf_op jit(solution)/shard_map/ppermute | solution.py:269
  17.7 10.5 %collective-permute-start.9 = (bf16[48,2048]{1,0:T(8,128)(2,1)S(1)}, bf16[48,2048]{1,0:T(8,128)(2,1)S(1)}, u32[]{:S(2)}, u32[]{:S(2)}) collective-permute-start(bf16[48,2048]{1,0:T(8,128)(2,1)S(1)} %get-tuple-element.50), channel_id=1, source_target_pairs={{0,16},{1,29},{2,22},{3,27},{4,20},{5,25},{6,18},{7,31},{8,24},{9,... | collective-permute-start | bytes 589832 | tf_op jit(solution)/shard_map/ppermute | solution.py:269
  24.7 11.8 %collective-permute-start.7 = (bf16[128,1024]{1,0:T(8,128)(2,1)S(1)}, bf16[128,1024]{1,0:T(8,128)(2,1)S(1)}, u32[]{:S(2)}, u32[]{:S(2)}) collective-permute-start(bf16[128,1024]{1,0:T(8,128)(2,1)S(1)} %get-tuple-element.47), channel_id=1, source_target_pairs={{0,1},{1,0},{2,3},{3,2},{4,5},{5,4},{6,7},{7,6},{8,9},{9,8},{10,11... | collective-permute-start | bytes 786440 | tf_op jit(solution)/shard_map/ppermute | solution.py:326
  28.2 5.3 %collective-permute-start.10 = (bf16[48,2048]{1,0:T(8,128)(2,1)S(1)}, bf16[48,2048]{1,0:T(8,128)(2,1)S(1)}, u32[]{:S(2)}, u32[]{:S(2)}) collective-permute-start(bf16[48,2048]{1,0:T(8,128)(2,1)S(1)} %collective-permute-done.9.refs_0_), channel_id=1, source_target_pairs={{0,2},{1,3},{2,0},{3,1},{4,6},{5,7},{6,4},{7,5},{8,10},{9,11},{10,... | collective-permute-start | bytes 589832 | tf_op jit(solution)/shard_map/ppermute | solution.py:296
  34.2 3.6 %collective-permute-start.11 = (bf16[48,1024]{1,0:T(8,128)(2,1)S(1)}, bf16[48,1024]{1,0:T(8,128)(2,1)S(1)}, u32[]{:S(2)}, u32[]{:S(2)}) collective-permute-start(bf16[48,1024]{1,0:T(8,128)(2,1)S(1)} %get-tuple-element.52), channel_id=1, source_target_pairs={{0,2},{1,3},{2,0},{3,1},{4,6},{5,7},{6,4},{7,5},{8,10},{9,11},{10,... | collective-permute-start | bytes 294920 | tf_op jit(solution)/shard_map/ppermute | solution.py:336
  36.2 4.3 %collective-permute-start.13 = (bf16[48,1024]{1,0:T(8,128)(2,1)S(1)}, bf16[48,1024]{1,0:T(8,128)(2,1)S(1)}, u32[]{:S(2)}, u32[]{:S(2)}) collective-permute-start(bf16[48,1024]{1,0:T(8,128)(2,1)S(1)} %get-tuple-element.55), channel_id=1, source_target_pairs={{0,2},{1,3},{2,0},{3,1},{4,6},{5,7},{6,4},{7,5},{8,10},{9,11},{10,... | collective-permute-start | bytes 294920 | tf_op jit(solution)/shard_map/ppermute | solution.py:336
  36.6 17.3 %collective-permute-start.8 = (bf16[128,512]{1,0:T(8,128)(2,1)S(1)}, bf16[128,512]{1,0:T(8,128)(2,1)S(1)}, u32[]{:S(2)}, u32[]{:S(2)}) collective-permute-start(bf16[128,512]{1,0:T(8,128)(2,1)S(1)} %get-tuple-element.49), channel_id=1, source_target_pairs={{0,2},{1,3},{2,0},{3,1},{4,6},{5,7},{6,4},{7,5},{8,10},{9,11},{10,... | collective-permute-start | bytes 393224 | tf_op jit(solution)/shard_map/ppermute | solution.py:329
  37.8 10.1 %collective-permute-start.12 = (bf16[48,512]{1,0:T(8,128)(2,1)S(1)}, bf16[48,512]{1,0:T(8,128)(2,1)S(1)}, u32[]{:S(2)}, u32[]{:S(2)}) collective-permute-start(bf16[48,512]{1,0:T(8,128)(2,1)S(1)} %get-tuple-element.53), channel_id=1, source_target_pairs={{0,16},{1,29},{2,22},{3,27},{4,20},{5,25},{6,18},{7,31},{8,24},{9,... | collective-permute-start | bytes 147464 | tf_op jit(solution)/shard_map/ppermute | solution.py:269
  40.5 7.5 %collective-permute-start.14 = (bf16[48,512]{1,0:T(8,128)(2,1)S(1)}, bf16[48,512]{1,0:T(8,128)(2,1)S(1)}, u32[]{:S(2)}, u32[]{:S(2)}) collective-permute-start(bf16[48,512]{1,0:T(8,128)(2,1)S(1)} %get-tuple-element.56), channel_id=1, source_target_pairs={{0,20},{1,25},{2,18},{3,31},{4,16},{5,29},{6,22},{7,27},{8,28},{9,... | collective-permute-start | bytes 147464 | tf_op jit(solution)/shard_map/ppermute | solution.py:269
  41.4 7.2 %collective-permute-start.15 = (bf16[48,512]{1,0:T(8,128)(2,1)S(1)}, bf16[48,512]{1,0:T(8,128)(2,1)S(1)}, u32[]{:S(2)}, u32[]{:S(2)}) collective-permute-start(bf16[48,512]{1,0:T(8,128)(2,1)S(1)} %get-tuple-element.57), channel_id=1, source_target_pairs={{0,17},{1,28},{2,23},{3,26},{4,21},{5,24},{6,19},{7,30},{8,25},{9,... | collective-permute-start | bytes 147464 | tf_op jit(solution)/shard_map/ppermute | solution.py:269
  47.4 6.5 %collective-permute-start.16 = (bf16[48,512]{1,0:T(8,128)(2,1)S(1)}, bf16[48,512]{1,0:T(8,128)(2,1)S(1)}, u32[]{:S(2)}, u32[]{:S(2)}) collective-permute-start(bf16[48,512]{1,0:T(8,128)(2,1)S(1)} %get-tuple-element.58), channel_id=1, source_target_pairs={{0,21},{1,24},{2,19},{3,30},{4,17},{5,28},{6,23},{7,26},{8,29},{9,... | collective-permute-start | bytes 147464 | tf_op jit(solution)/shard_map/ppermute | solution.py:269

commit v5 on v4

--- a/solution.py
+++ b/solution.py
@@ -92,7 +92,8 @@
         slots_out[j : j + 1, :] = where
         if direct:
             there = slot_of(label, rank, capacity, direct, 1)
-            there = jnp.where(there >= 2 * capacity, there + 2 * capacity, -1)
+            own_far = jnp.logical_and(there >= 2 * capacity, there < 3 * capacity)
+            there = jnp.where(own_far, there + 2 * capacity, -1)
             slots_out[j : j + 1, :] = jnp.maximum(where, there)
         hit = jnp.where(slot == where, 1.0, hit)
     pick = hit.astype(bf16)
@@ -123,26 +124,22 @@
     return (gate / (1.0 + jnp.exp(-gate)) * up).astype(bf16)
 
 
-def shared_body(slots, rows, *refs):
+def shared_body(groups, total, slots, rows, *refs):
     weights, gains_in, part, outs = refs[:3], refs[3], refs[4], refs[5:-2]
     gains, sems = refs[-2:]
     (copy,) = fetch((gains_in,), (gains,), sems)
     hidden = units_of(rows[...], weights)
     part[...] = jnp.dot(hidden, weights[2][...], preferred_element_type=f32)
-    total = sum(out.shape[1] for out in outs[::2])
     slot = lax.broadcasted_iota(jnp.int32, (total, rows.shape[0]), 0)
     weight = jnp.zeros(slot.shape, f32)
     copy.wait()
     for j in range(slots.shape[0]):
         weight = jnp.where(slot == slots[j : j + 1, :], gains[j : j + 1, :], weight)
-    at = 0
-    for high_out, low_out in zip(outs[::2], outs[1::2]):
-        n = high_out.shape[1]
-        turned = weight[at : at + n].T
-        high = turned.astype(bf16)
-        high_out[...] = high
-        low_out[...] = (turned - high.astype(f32)).astype(bf16)
-        at += n
+    high = weight.astype(bf16).astype(f32)
+    low = weight - high
+    for out, spans in zip(outs, groups):
+        parts = [half[a:b] for a, b in spans for half in (high, low)]
+        out[...] = jnp.concatenate(parts, axis=0).T.astype(bf16)
 
 
 def near_body(blocks, *refs):
@@ -168,20 +165,19 @@
     return room
 
 
-def picked(high, low, rows):
-    total = jnp.dot(high[...], rows, preferred_element_type=f32)
-    return total + jnp.dot(low[...], rows, preferred_element_type=f32)
-
-
-def first_body(blocks, high, low, part, *refs):
+def picked(weights, rows):
+    return jnp.dot(weights[...], rows, preferred_element_type=f32)
+
+
+def first_body(blocks, weights, part, *refs):
     rows_in, (send, keep) = refs[:blocks], refs[blocks : blocks + 2]
-    gathered = gather_rows(rows_in, refs[-1])
+    gathered = gather_rows((*rows_in, *rows_in), refs[-1])
     share = keep.shape[1] // 2
     core = lax.axis_index("tp") % 2
     for out, place in ((send, 1 - core), (keep, core)):
         for x in range(2):
             columns = pl.ds(pl.multiple_of((2 * x + place) * share, share), share)
-            total = part[:, columns] + picked(high, low, gathered[:, columns])
+            total = part[:, columns] + picked(weights, gathered[:, columns])
             out[:, x * share : (x + 1) * share] = total.astype(out.dtype)
 
 
@@ -226,10 +222,20 @@
         out[...] = (keep[:, columns] + came[:, columns].astype(f32)).astype(out.dtype)
 
 
-def mix_body(high, low, mine, came, *refs):
-    out, room = refs[-2:]
-    rows = gather_rows(refs[:-2], room)[...]
-    out[...] = (picked(high, low, rows) + mine[...] + came[...].astype(f32)).astype(out.dtype)
+def swap_body(weights, rows, mine, send, keep, room):
+    gathered = gather_rows((rows, rows), room)
+    width = keep.shape[1]
+    core = lax.axis_index("tp") % 2
+    columns = pl.ds(pl.multiple_of((1 - core) * width, width), width)
+    send[...] = picked(weights, gathered[:, columns])
+    columns = pl.ds(pl.multiple_of(core * width, width), width)
+    keep[...] = picked(weights, gathered[:, columns]) + mine[...]
+
+
+def mix_body(weights, rows, rows2, came, kept, swapped, out, room):
+    gathered = gather_rows((rows, rows, rows2, rows2), room)
+    total = came[...].astype(f32) + kept[...] + swapped[...]
+    out[...] = (total + picked(weights, gathered[...])).astype(out.dtype)
 
 
 def local(
@@ -295,14 +301,17 @@
     if direct:
         arrived["B"] = lax.ppermute(arrived["A"], "tp", neighbour)
     near = [k for k in sizes if k in ("P", "Q")]
-    spans = [sum(sizes[k] for k in near)]
+    n_near = sum(sizes[k] for k in near)
+    groups_of = [[(0, n_near)]]
     if direct:
-        spans.append(2 * (total - spans[0]))
+        at = [i * capacity for i in range(6)]
+        groups_of += [[(at[3], at[4])], [(at[2], at[3]), (at[4], at[5])]]
+        total = at[5]
     gains = route_weights.T
     part, *weights = call(
-        shared_body,
+        functools.partial(shared_body, groups_of, total),
         [shape(rows_here, width, f32)]
-        + [shape(rows_here, n, bf16) for n in spans for _ in range(2)],
+        + [shape(rows_here, 2 * sum(b - a for a, b in spans), bf16) for spans in groups_of],
         [slots, normed, *sh_weights, gains],
         6 * rows_here * width * shared_gate.shape[1],
         landing([gains]),
@@ -316,9 +325,9 @@
     send, keep = call(
         functools.partial(first_body, len(near)),
         [shape(rows_here, wide, bf16), shape(rows_here, wide, f32)],
-        [*weights[:2], part, *[returned[k] for k in near]],
-        4 * rows_here * width * spans[0],
-        [pltpu.VMEM((spans[0], width), bf16)] if direct else [],
+        [weights[0], part, *[returned[k] for k in near]],
+        4 * rows_here * width * n_near,
+        [pltpu.VMEM((2 * n_near, width), bf16)],
     )
     send, mine = call(
         halve_body,
@@ -334,20 +343,26 @@
             outs = [shape(capacity, wide, bf16), shape(capacity, wide, f32)]
             sent[k], kept[k] = products(product_body, [arrived[k]], [*own, *other], outs)
             sent[k] = lax.ppermute(sent[k], "tp", neighbour)
-        far_rows = {}
-        for k, other_k in ("AB", "BA"):
-            ins = [kept[k], sent[other_k]]
-            outs = [shape(capacity, share, bf16)] * 2
-            outs = call(add_body, outs, ins, kept[k].size)
-            for flip, out in enumerate(outs):
-                far_rows[k, flip] = hop(out, distances[k], flip)
-        rows = [far_rows[k, flip] for flip in range(2) for k in "AB"]
+        ins, outs = [kept["B"], sent["A"]], [shape(capacity, wide, bf16)]
+        (out,) = call(add_body, outs, ins, kept["B"].size)
+        out = hop(out, distances["B"])
+        send, swap_mine = call(
+            swap_body,
+            [shape(rows_here, share, f32)] * 2,
+            [weights[1], out, mine],
+            4 * rows_here * wide * capacity,
+            [pltpu.VMEM((2 * capacity, wide), bf16)],
+        )
+        swap_came = lax.ppermute(send, "tp", sibling)
+        ins, outs = [kept["A"], sent["B"]], [shape(capacity, share, bf16)] * 2
+        outs = call(add_body, outs, ins, kept["A"].size)
+        rows = [hop(out, distances["A"], flip) for flip, out in enumerate(outs)]
         (mixed,) = call(
             mix_body,
             [shape(rows_here, share, bf16)],
-            [*weights[2:], mine, came, *rows],
-            4 * rows_here * share * spans[1],
-            [pltpu.VMEM((spans[1], share), bf16)],
+            [weights[2], *rows, came, swap_mine, swap_came],
+            8 * rows_here * share * capacity,
+            [pltpu.VMEM((4 * capacity, share), bf16)],
         )
         return mixed
     (mixed,) = call(add_body, [shape(rows_here, share, bf16)], [mine, came], mine.size)

time: 54.9 us -> 54.4 us (level)
  the two profiles are of different devices: /device:TPU:1 before, /device:TPU:0 now
where the time goes in v5:
time: 54.4 us; the launch traced here: 54 us
  waiting for transfers between devices  26.5 us (49%)
  starting transfers between devices  20.7 us (38%)
  Pallas kernels  6.63 us (12%)
    ppermute x8, waiting for transfers between devices, hop(): return lax.ppermute(block, ('ep', 'tp'), pairs)  20.6 us
    ppermute x8, starting transfers between devices, hop(): return lax.ppermute(block, ('ep', 'tp'), pairs)  10.2 us
    pallas_call x11, Pallas kernels, call(): pl.pallas_call(body, out_shape=outs, in_specs=[hbm if i in far else vmem...  6.63 us
    ppermute x2, waiting for transfers between devices, local(): sent[k] = lax.ppermute(sent[k], 'tp', neighbour)  5.88 us
    ppermute x2, starting transfers between devices, local(): sent[k] = lax.ppermute(sent[k], 'tp', neighbour)  4.21 us
    ppermute x1, starting transfers between devices, local(): lax.ppermute(send, 'tp', sibling)  2.19 us
    ppermute x1, starting transfers between devices, local(): came = lax.ppermute(send, 'tp', neighbour)  1.54 us
    ppermute x1, starting transfers between devices, local(): arrived['B'] = lax.ppermute(arrived['A'], 'tp', neighbour)  1.49 us
  transfers between devices with their start and end apart: 17, of which 6 were waited for; matrix products, arithmetic and copies ran while one was open for 0% of the time, Pallas kernels for 10%

profile of v5, /device:TPU:0, one launch (start us, length us, event | category | flops | bytes accessed | tf_op | source)
XLA Modules:
  0.0 54.0 jit_solution(6303286217593134784)
XLA Ops:
  0.0 0.5 collective-permute-start.1
  0.5 0.0 collective-permute-start.2
  0.5 0.5 collective-permute-start.3
  1.0 1.8 %shard_map.100 = (bf16[128,2048]{1,0:T(8,128)(2,1)S(1)}, s32[2,128]{1,0:T(2,128)S(1)}, bf16[2048,128]{1,0:T(8,128)(2,1)S(1)}, bf16[2048,128]{1,0:T(8,128)(2,1)S(...) custom-call(s32[2,128]{1,0:T(2,128)} %bitcast.20, ...), custom_call_target="tpu_custom_call" | custom-call | flops 100663296 | bytes 4790272 | tf_op jit(solution)/shard_map/pallas_call | solution.py:25
  2.8 0.7 %collective-permute-start.8 = (bf16[48,2048]{1,0:T(8,128)(2,1)S(1)}, bf16[48,2048]{1,0:T(8,128)(2,1)S(1)}, u32[]{:S(2)}, u32[]{:S(2)}) collective-permute-start(bf16[48,2048]{1,0:T(8,128)(2,1)S(1)} %get-tuple-element.44), channel_id=1, source_target_pairs={{0,0},{1,5},{2,2},{3,7},{4,4},{5,1},{6,6},{7,3},{8,8},{9,13},{10,1... | collective-permute-start | bytes 589832 | tf_op jit(solution)/shard_map/ppermute | solution.py:275
  3.5 3.6 %collective-permute-start.9 = (bf16[48,2048]{1,0:T(8,128)(2,1)S(1)}, bf16[48,2048]{1,0:T(8,128)(2,1)S(1)}, u32[]{:S(2)}, u32[]{:S(2)}) collective-permute-start(bf16[48,2048]{1,0:T(8,128)(2,1)S(1)} %get-tuple-element.45), channel_id=1, source_target_pairs={{0,12},{1,9},{2,14},{3,11},{4,8},{5,13},{6,10},{7,15},{8,4},{9,1},... | collective-permute-start | bytes 589832 | tf_op jit(solution)/shard_map/ppermute | solution.py:275
  7.1 2.6 %collective-permute-start = (bf16[48,2048]{1,0:T(8,128)(2,1)S(1)}, bf16[48,2048]{1,0:T(8,128)(2,1)S(1)}, u32[]{:S(2)}, u32[]{:S(2)}) collective-permute-start(bf16[48,2048]{1,0:T(8,128)(2,1)S(1)} %get-tuple-element.37), channel_id=1, source_target_pairs={{0,16},{1,29},{2,22},{3,27},{4,20},{5,25},{6,18},{7,31},{8,24},{9,... | collective-permute-start | bytes 589832 | tf_op jit(solution)/shard_map/ppermute | solution.py:275
  9.7 4.1 %collective-permute-done.9.refs_1_ = bf16[48,2048]{1,0:T(8,128)(2,1)S(1)} collective-permute-done((bf16[48,2048]{1,0:T(8,128)(2,1)S(1)}, bf16[48,2048]{1,0:T(8,128)(2,1)S(1)}, u32[]{:S(2)}, u32[]{:S(2)}) %collective-permute-start.9) | collective-permute-done | bytes 196640 | tf_op jit(solution)/shard_map/ppermute | solution.py:275
  13.8 0.7 %shard_map.105 = (bf16[48,2048]{1,0:T(8,128)(2,1)S(1)}, bf16[48,2048]{1,0:T(8,128)(2,1)S(1)}) custom-call(bf16[48,2048]{1,0:T(8,128)(2,1)S(1)} %collective-permute-done.8.refs_0_, bf16[48,2048]{1,0:T(8,128)(2,1)S(1)} %collective-permute-done.9.refs_1_, bf16[2048,128]{1,0:T(8,128)(2,1)S(1)} %bitcast.7, bf16[2048,128]{1,0:T(8,128)(2,1)S(1)} %bitcast.11, ...), custom_call_target="tpu_custom_call" | custom-call | flops 301989888 | bytes 3932160 | tf_op jit(solution)/shard_map/pallas_call | solution.py:25
  14.6 0.7 %collective-permute-start.10 = (bf16[48,2048]{1,0:T(8,128)(2,1)S(1)}, bf16[48,2048]{1,0:T(8,128)(2,1)S(1)}, u32[]{:S(2)}, u32[]{:S(2)}) collective-permute-start(bf16[48,2048]{1,0:T(8,128)(2,1)S(1)} %get-tuple-element.46), channel_id=1, source_target_pairs={{0,0},{1,5},{2,2},{3,7},{4,4},{5,1},{6,6},{7,3},{8,8},{9,13},{10,1... | collective-permute-start | bytes 589832 | tf_op jit(solution)/shard_map/ppermute | solution.py:275
  15.2 1.1 %collective-permute-start.11 = (bf16[48,2048]{1,0:T(8,128)(2,1)S(1)}, bf16[48,2048]{1,0:T(8,128)(2,1)S(1)}, u32[]{:S(2)}, u32[]{:S(2)}) collective-permute-start(bf16[48,2048]{1,0:T(8,128)(2,1)S(1)} %get-tuple-element.47), channel_id=1, source_target_pairs={{0,12},{1,9},{2,14},{3,11},{4,8},{5,13},{6,10},{7,15},{8,4},{9,1},... | collective-permute-start | bytes 589832 | tf_op jit(solution)/shard_map/ppermute | solution.py:275
  16.3 1.5 %collective-permute-start.4 = (bf16[48,2048]{1,0:T(8,128)(2,1)S(1)}, bf16[48,2048]{1,0:T(8,128)(2,1)S(1)}, u32[]{:S(2)}, u32[]{:S(2)}) collective-permute-start(bf16[48,2048]{1,0:T(8,128)(2,1)S(1)} %collective-permute-done.refs_0_), channel_id=1, source_target_pairs={{0,2},{1,3},{2,0},{3,1},{4,6},{5,7},{6,4},{7,5},{8,10},{9,11},{10,... | collective-permute-start | bytes 589832 | tf_op jit(solution)/shard_map/ppermute | solution.py:302
  17.8 1.1 %shard_map.101 = (f32[128,2048]{1,0:T(8,128)S(1)}, bf16[128,192]{1,0:T(8,128)(2,1)S(1)}, bf16[128,96]{1,0:T(8,128)(2,1)S(1)}, bf16[128,192]{1,0:T(8,128)(2,1)S(1)}) custom-call(s32[2,128]{1,0:T(2,128)S(1)} %get-tuple-element.31.slots, bf16[128,2048]{1,0:T(8,128)(2,1)S(1)} %get-tuple-element.32.rows, bf16[2048,128]{1,0:T(8,128)(2,1)S(1)} %get-tuple-element.33.refs_0_, ...), custom_call_target="tpu_custom_call" | custom-call | flops 201326592 | bytes 3270656 | tf_op jit(solution)/shard_map/pallas_call | solution.py:25
  18.9 3.6 %collective-permute-done.11.refs_1_ = bf16[48,2048]{1,0:T(8,128)(2,1)S(1)} collective-permute-done((bf16[48,2048]{1,0:T(8,128)(2,1)S(1)}, bf16[48,2048]{1,0:T(8,128)(2,1)S(1)}, u32[]{:S(2)}, u32[]{:S(2)}) %collective-permute-start.11) | collective-permute-done | bytes 196640 | tf_op jit(solution)/shard_map/ppermute | solution.py:275
  22.6 0.4 shard_map.106
  22.9 2.2 %collective-permute-start.12 = (bf16[128,1024]{1,0:T(8,128)(2,1)S(1)}, bf16[128,1024]{1,0:T(8,128)(2,1)S(1)}, u32[]{:S(2)}, u32[]{:S(2)}) collective-permute-start(bf16[128,1024]{1,0:T(8,128)(2,1)S(1)} %get-tuple-element.49), channel_id=1, source_target_pairs={{0,1},{1,0},{2,3},{3,2},{4,5},{5,4},{6,7},{7,6},{8,9},{9,8},{10,11... | collective-permute-start | bytes 786440 | tf_op jit(solution)/shard_map/ppermute | solution.py:335
  25.1 0.7 %shard_map.102 = (bf16[48,1024]{1,0:T(8,128)(2,1)S(1)}, f32[48,1024]{1,0:T(8,128)S(1)}) custom-call(bf16[48,2048]{1,0:T(8,128)(2,1)S(1)} %collective-permute-done.refs_0_, bf16[2048,128]{1,0:T(8,128)(2,1)S(1)} %bitcast.8, bf16[2048,128]{1,0:T(8,128)(2,1)S(1)} %bitcast.12, bf16[128,2048]{1,0:T(8,128)(2,1)S(1)} %bitcast.16, ...), custom_call_target="tpu_custom_call" | custom-call | flops 150994944 | bytes 3637248 | tf_op jit(solution)/shard_map/pallas_call | solution.py:25
  25.9 3.7 %collective-permute-start.14 = (bf16[48,1024]{1,0:T(8,128)(2,1)S(1)}, bf16[48,1024]{1,0:T(8,128)(2,1)S(1)}, u32[]{:S(2)}, u32[]{:S(2)}) collective-permute-start(bf16[48,1024]{1,0:T(8,128)(2,1)S(1)} %get-tuple-element.53), channel_id=1, source_target_pairs={{0,2},{1,3},{2,0},{3,1},{4,6},{5,7},{6,4},{7,5},{8,10},{9,11},{10,... | collective-permute-start | bytes 294920 | tf_op jit(solution)/shard_map/ppermute | solution.py:345
  29.5 0.7 %shard_map.103 = (bf16[48,1024]{1,0:T(8,128)(2,1)S(1)}, f32[48,1024]{1,0:T(8,128)S(1)}) custom-call(bf16[48,2048]{1,0:T(8,128)(2,1)S(1)} %collective-permute-done.4.refs_0_, bf16[2048,128]{1,0:T(8,128)(2,1)S(1)} %bitcast.9, bf16[2048,128]{1,0:T(8,128)(2,1)S(1)} %bitcast.13, bf16[128,2048]{1,0:T(8,128)(2,1)S(1)} %bitcast.17, ...), custom_call_target="tpu_custom_call" | custom-call | flops 150994944 | bytes 3637248 | tf_op jit(solution)/shard_map/pallas_call | solution.py:25
  30.3 2.2 %collective-permute-done.14.came = bf16[48,1024]{1,0:T(8,128)(2,1)S(1)} collective-permute-done((bf16[48,1024]{1,0:T(8,128)(2,1)S(1)}, bf16[48,1024]{1,0:T(8,128)(2,1)S(1)}, u32[]{:S(2)}, u32[]{:S(2)}) %collective-permute-start.14) | collective-permute-done | bytes 98336 | tf_op jit(solution)/shard_map/ppermute | solution.py:345
  32.5 1.4 %collective-permute-start.15 = (bf16[48,1024]{1,0:T(8,128)(2,1)S(1)}, bf16[48,1024]{1,0:T(8,128)(2,1)S(1)}, u32[]{:S(2)}, u32[]{:S(2)}) collective-permute-start(bf16[48,1024]{1,0:T(8,128)(2,1)S(1)} %shard_map.108), channel_id=1, source_target_pairs={{0,20},{1,25},{2,18},{3,31},{4,16},{5,29},{6,22},{7,27},{8,28},{9,... | collective-permute-start | bytes 294920 | tf_op jit(solution)/shard_map/ppermute | solution.py:275
  34.0 0.1 shard_map.107
  34.0 6.4 %collective-permute-done.15.rows = bf16[48,1024]{1,0:T(8,128)(2,1)S(1)} collective-permute-done((bf16[48,1024]{1,0:T(8,128)(2,1)S(1)}, bf16[48,1024]{1,0:T(8,128)(2,1)S(1)}, u32[]{:S(2)}, u32[]{:S(2)}) %collective-permute-start.15) | collective-permute-done | bytes 98336 | tf_op jit(solution)/shard_map/ppermute | solution.py:275
  40.4 0.2 shard_map.109
  40.7 0.1 collective-permute-start.16
  40.8 0.6 %collective-permute-start.5 = (bf16[48,1024]{1,0:T(8,128)(2,1)S(1)}, bf16[48,1024]{1,0:T(8,128)(2,1)S(1)}, u32[]{:S(2)}, u32[]{:S(2)}) collective-permute-start(bf16[48,1024]{1,0:T(8,128)(2,1)S(1)} %get-tuple-element.39), channel_id=1, source_target_pairs={{0,2},{1,3},{2,0},{3,1},{4,6},{5,7},{6,4},{7,5},{8,10},{9,11},{10,... | collective-permute-start | bytes 294920 | tf_op jit(solution)/shard_map/ppermute | solution.py:345
  41.3 1.5 %collective-permute-start.13 = (bf16[128,512]{1,0:T(8,128)(2,1)S(1)}, bf16[128,512]{1,0:T(8,128)(2,1)S(1)}, u32[]{:S(2)}, u32[]{:S(2)}) collective-permute-start(bf16[128,512]{1,0:T(8,128)(2,1)S(1)} %get-tuple-element.50), channel_id=1, source_target_pairs={{0,2},{1,3},{2,0},{3,1},{4,6},{5,7},{6,4},{7,5},{8,10},{9,11},{10,... | collective-permute-start | bytes 393224 | tf_op jit(solution)/shard_map/ppermute | solution.py:338
  42.8 3.6 %collective-permute-done.5.came = bf16[48,1024]{1,0:T(8,128)(2,1)S(1)} collective-permute-done((bf16[48,1024]{1,0:T(8,128)(2,1)S(1)}, bf16[48,1024]{1,0:T(8,128)(2,1)S(1)}, u32[]{:S(2)}, u32[]{:S(2)}) %collective-permute-start.5) | collective-permute-done | bytes 98336 | tf_op jit(solution)/shard_map/ppermute | solution.py:345
  46.5 0.1 collective-permute-start.6
  46.6 0.0 collective-permute-start.7
  46.7 6.4 %collective-permute-done.6.rows = bf16[48,512]{1,0:T(8,128)(2,1)S(1)} collective-permute-done((bf16[48,512]{1,0:T(8,128)(2,1)S(1)}, bf16[48,512]{1,0:T(8,128)(2,1)S(1)}, u32[]{:S(2)}, u32[]{:S(2)}) %collective-permute-start.6) | collective-permute-done | bytes 49184 | tf_op jit(solution)/shard_map/ppermute | solution.py:275
  53.1 0.8 %shard_map.110 = bf16[128,512]{1,0:T(8,128)(2,1)} custom-call(bf16[128,192]{1,0:T(8,128)(2,1)S(1)} %get-tuple-element.36.weights, bf16[48,512]{1,0:T(8,128)(2,1)S(1)} %collective-permute-done.6.rows, bf16[48,512]{1,0:T(8,128)(2,1)S(1)} %collective-permute-done.7.rows2, bf16[128,512]{1,0:T(8,128)(2,1)S(1)} %collective-permute-done.13.came, ...), custom_call_target="tpu_custom_call" | custom-call | flops 25165824 | bytes 933888 | tf_op jit(solution)/shard_map/pallas_call | solution.py:25
  (19 shorter events, 0.1 us)
Async XLA Ops:
  0.0 13.8 %collective-permute-start.1 = (bf16[2048,128]{1,0:T(8,128)(2,1)}, bf16[2048,128]{1,0:T(8,128)(2,1)S(1)}, u32[]{:S(2)}, u32[]{:S(2)}) collective-permute-start(bf16[2048,128]{1,0:T(8,128)(2,1)} %bitcast.6), channel_id=1, source_target_pairs={{0,1},{1,0},{2,3},{3,2},{4,5},{5,4},{6,7},{7,6},{8,9},{9,8},{10,11... | collective-permute-start | bytes 1572872 | tf_op jit(solution)/shard_map/ppermute | solution.py:265
  0.5 13.3 %collective-permute-start.2 = (bf16[2048,128]{1,0:T(8,128)(2,1)}, bf16[2048,128]{1,0:T(8,128)(2,1)S(1)}, u32[]{:S(2)}, u32[]{:S(2)}) collective-permute-start(bf16[2048,128]{1,0:T(8,128)(2,1)} %bitcast.10), channel_id=1, source_target_pairs={{0,1},{1,0},{2,3},{3,2},{4,5},{5,4},{6,7},{7,6},{8,9},{9,8},{10,11... | collective-permute-start | bytes 1572872 | tf_op jit(solution)/shard_map/ppermute | solution.py:265
  0.5 13.3 %collective-permute-start.3 = (bf16[128,2048]{1,0:T(8,128)(2,1)}, bf16[128,2048]{1,0:T(8,128)(2,1)S(1)}, u32[]{:S(2)}, u32[]{:S(2)}) collective-permute-start(bf16[128,2048]{1,0:T(8,128)(2,1)} %bitcast.14), channel_id=1, source_target_pairs={{0,1},{1,0},{2,3},{3,2},{4,5},{5,4},{6,7},{7,6},{8,9},{9,8},{10,11... | collective-permute-start | bytes 1572872 | tf_op jit(solution)/shard_map/ppermute | solution.py:265
  1.0 12.8 %copy-start = (bf16[1,2048,128]{2,1,0:T(8,128)(2,1)S(1)}, bf16[1,2048,128]{2,1,0:T(8,128)(2,1)}, u32[]{:S(2)}) copy-start(bf16[1,2048,128]{2,1,0:T(8,128)(2,1)} %param.14) | copy-start | bytes 1572868
  1.0 12.8 %copy-start.1 = (bf16[1,2048,128]{2,1,0:T(8,128)(2,1)S(1)}, bf16[1,2048,128]{2,1,0:T(8,128)(2,1)}, u32[]{:S(2)}) copy-start(bf16[1,2048,128]{2,1,0:T(8,128)(2,1)} %param.15) | copy-start | bytes 1572868
  1.0 12.8 %copy-start.2 = (bf16[1,128,2048]{2,1,0:T(8,128)(2,1)S(1)}, bf16[1,128,2048]{2,1,0:T(8,128)(2,1)}, u32[]{:S(2)}) copy-start(bf16[1,128,2048]{2,1,0:T(8,128)(2,1)} %param.16) | copy-start | bytes 1572868
  2.8 4.3 %collective-permute-start.8 = (bf16[48,2048]{1,0:T(8,128)(2,1)S(1)}, bf16[48,2048]{1,0:T(8,128)(2,1)S(1)}, u32[]{:S(2)}, u32[]{:S(2)}) collective-permute-start(bf16[48,2048]{1,0:T(8,128)(2,1)S(1)} %get-tuple-element.44), channel_id=1, source_target_pairs={{0,0},{1,5},{2,2},{3,7},{4,4},{5,1},{6,6},{7,3},{8,8},{9,13},{10,1... | collective-permute-start | bytes 589832 | tf_op jit(solution)/shard_map/ppermute | solution.py:275
  3.5 10.3 %collective-permute-start.9 = (bf16[48,2048]{1,0:T(8,128)(2,1)S(1)}, bf16[48,2048]{1,0:T(8,128)(2,1)S(1)}, u32[]{:S(2)}, u32[]{:S(2)}) collective-permute-start(bf16[48,2048]{1,0:T(8,128)(2,1)S(1)} %get-tuple-element.45), channel_id=1, source_target_pairs={{0,12},{1,9},{2,14},{3,11},{4,8},{5,13},{6,10},{7,15},{8,4},{9,1},... | collective-permute-start | bytes 589832 | tf_op jit(solution)/shard_map/ppermute | solution.py:275
  7.1 9.2 %collective-permute-start = (bf16[48,2048]{1,0:T(8,128)(2,1)S(1)}, bf16[48,2048]{1,0:T(8,128)(2,1)S(1)}, u32[]{:S(2)}, u32[]{:S(2)}) collective-permute-start(bf16[48,2048]{1,0:T(8,128)(2,1)S(1)} %get-tuple-element.37), channel_id=1, source_target_pairs={{0,16},{1,29},{2,22},{3,27},{4,20},{5,25},{6,18},{7,31},{8,24},{9,... | collective-permute-start | bytes 589832 | tf_op jit(solution)/shard_map/ppermute | solution.py:275
  14.6 4.4 %collective-permute-start.10 = (bf16[48,2048]{1,0:T(8,128)(2,1)S(1)}, bf16[48,2048]{1,0:T(8,128)(2,1)S(1)}, u32[]{:S(2)}, u32[]{:S(2)}) collective-permute-start(bf16[48,2048]{1,0:T(8,128)(2,1)S(1)} %get-tuple-element.46), channel_id=1, source_target_pairs={{0,0},{1,5},{2,2},{3,7},{4,4},{5,1},{6,6},{7,3},{8,8},{9,13},{10,1... | collective-permute-start | bytes 589832 | tf_op jit(solution)/shard_map/ppermute | solution.py:275
  15.2 7.3 %collective-permute-start.11 = (bf16[48,2048]{1,0:T(8,128)(2,1)S(1)}, bf16[48,2048]{1,0:T(8,128)(2,1)S(1)}, u32[]{:S(2)}, u32[]{:S(2)}) collective-permute-start(bf16[48,2048]{1,0:T(8,128)(2,1)S(1)} %get-tuple-element.47), channel_id=1, source_target_pairs={{0,12},{1,9},{2,14},{3,11},{4,8},{5,13},{6,10},{7,15},{8,4},{9,1},... | collective-permute-start | bytes 589832 | tf_op jit(solution)/shard_map/ppermute | solution.py:275
  16.3 13.2 %collective-permute-start.4 = (bf16[48,2048]{1,0:T(8,128)(2,1)S(1)}, bf16[48,2048]{1,0:T(8,128)(2,1)S(1)}, u32[]{:S(2)}, u32[]{:S(2)}) collective-permute-start(bf16[48,2048]{1,0:T(8,128)(2,1)S(1)} %collective-permute-done.refs_0_), channel_id=1, source_target_pairs={{0,2},{1,3},{2,0},{3,1},{4,6},{5,7},{6,4},{7,5},{8,10},{9,11},{10,... | collective-permute-start | bytes 589832 | tf_op jit(solution)/shard_map/ppermute | solution.py:302
  22.9 11.0 %collective-permute-start.12 = (bf16[128,1024]{1,0:T(8,128)(2,1)S(1)}, bf16[128,1024]{1,0:T(8,128)(2,1)S(1)}, u32[]{:S(2)}, u32[]{:S(2)}) collective-permute-start(bf16[128,1024]{1,0:T(8,128)(2,1)S(1)} %get-tuple-element.49), channel_id=1, source_target_pairs={{0,1},{1,0},{2,3},{3,2},{4,5},{5,4},{6,7},{7,6},{8,9},{9,8},{10,11... | collective-permute-start | bytes 786440 | tf_op jit(solution)/shard_map/ppermute | solution.py:335
  25.9 6.6 %collective-permute-start.14 = (bf16[48,1024]{1,0:T(8,128)(2,1)S(1)}, bf16[48,1024]{1,0:T(8,128)(2,1)S(1)}, u32[]{:S(2)}, u32[]{:S(2)}) collective-permute-start(bf16[48,1024]{1,0:T(8,128)(2,1)S(1)} %get-tuple-element.53), channel_id=1, source_target_pairs={{0,2},{1,3},{2,0},{3,1},{4,6},{5,7},{6,4},{7,5},{8,10},{9,11},{10,... | collective-permute-start | bytes 294920 | tf_op jit(solution)/shard_map/ppermute | solution.py:345
  32.5 7.9 %collective-permute-start.15 = (bf16[48,1024]{1,0:T(8,128)(2,1)S(1)}, bf16[48,1024]{1,0:T(8,128)(2,1)S(1)}, u32[]{:S(2)}, u32[]{:S(2)}) collective-permute-start(bf16[48,1024]{1,0:T(8,128)(2,1)S(1)} %shard_map.108), channel_id=1, source_target_pairs={{0,20},{1,25},{2,18},{3,31},{4,16},{5,29},{6,22},{7,27},{8,28},{9,... | collective-permute-start | bytes 294920 | tf_op jit(solution)/shard_map/ppermute | solution.py:275
  40.7 12.4 %collective-permute-start.16 = (f32[128,512]{1,0:T(8,128)S(1)}, f32[128,512]{1,0:T(8,128)S(1)}, u32[]{:S(2)}, u32[]{:S(2)}) collective-permute-start(f32[128,512]{1,0:T(8,128)S(1)} %get-tuple-element.56), channel_id=1, source_target_pairs={{0,1},{1,0},{2,3},{3,2},{4,5},{5,4},{6,7},{7,6},{8,9},{9,8},{10,11... | collective-permute-start | bytes 786440 | tf_op jit(solution)/shard_map/ppermute | solution.py:356
  40.8 5.7 %collective-permute-start.5 = (bf16[48,1024]{1,0:T(8,128)(2,1)S(1)}, bf16[48,1024]{1,0:T(8,128)(2,1)S(1)}, u32[]{:S(2)}, u32[]{:S(2)}) collective-permute-start(bf16[48,1024]{1,0:T(8,128)(2,1)S(1)} %get-tuple-element.39), channel_id=1, source_target_pairs={{0,2},{1,3},{2,0},{3,1},{4,6},{5,7},{6,4},{7,5},{8,10},{9,11},{10,... | collective-permute-start | bytes 294920 | tf_op jit(solution)/shard_map/ppermute | solution.py:345
  41.3 11.8 %collective-permute-start.13 = (bf16[128,512]{1,0:T(8,128)(2,1)S(1)}, bf16[128,512]{1,0:T(8,128)(2,1)S(1)}, u32[]{:S(2)}, u32[]{:S(2)}) collective-permute-start(bf16[128,512]{1,0:T(8,128)(2,1)S(1)} %get-tuple-element.50), channel_id=1, source_target_pairs={{0,2},{1,3},{2,0},{3,1},{4,6},{5,7},{6,4},{7,5},{8,10},{9,11},{10,... | collective-permute-start | bytes 393224 | tf_op jit(solution)/shard_map/ppermute | solution.py:338
  46.5 6.6 %collective-permute-start.6 = (bf16[48,512]{1,0:T(8,128)(2,1)S(1)}, bf16[48,512]{1,0:T(8,128)(2,1)S(1)}, u32[]{:S(2)}, u32[]{:S(2)}) collective-permute-start(bf16[48,512]{1,0:T(8,128)(2,1)S(1)} %get-tuple-element.40), channel_id=1, source_target_pairs={{0,16},{1,29},{2,22},{3,27},{4,20},{5,25},{6,18},{7,31},{8,24},{9,... | collective-permute-start | bytes 147464 | tf_op jit(solution)/shard_map/ppermute | solution.py:275
  46.6 6.5 %collective-permute-start.7 = (bf16[48,512]{1,0:T(8,128)(2,1)S(1)}, bf16[48,512]{1,0:T(8,128)(2,1)S(1)}, u32[]{:S(2)}, u32[]{:S(2)}) collective-permute-start(bf16[48,512]{1,0:T(8,128)(2,1)S(1)} %get-tuple-element.41), channel_id=1, source_target_pairs={{0,17},{1,28},{2,23},{3,26},{4,21},{5,24},{6,19},{7,30},{8,25},{9,... | collective-permute-start | bytes 147464 | tf_op jit(solution)/shard_map/ppermute | solution.py:275

commit v6 on v5

--- a/solution.py
+++ b/solution.py
@@ -65,8 +65,8 @@
 
 
 def route_body(capacity, experts, direct, *refs):
-    sources, outs, (ids, gain, tokens, sems) = refs[:6], refs[6:-4], refs[-4:]
-    copies = fetch(sources, (ids, gain, tokens, *outs[2:5]), sems)
+    sources, outs, (ids, gain, tokens, sems) = refs[:3], refs[3:-4], refs[-4:]
+    copies = fetch(sources, (ids, gain, tokens), sems)
     normed_out, slots_out = outs[0], outs[1]
     rows, width = tokens.shape
     kinds = max(8, experts)
@@ -76,7 +76,7 @@
         < lax.broadcasted_iota(jnp.int32, (rows, rows), 1)
     ).astype(bf16)
     base = jnp.zeros((kinds, 1), f32)
-    total = sum(out.shape[0] for out in outs[5:])
+    total = sum(out.shape[0] for out in outs[2:])
     slot = lax.broadcasted_iota(jnp.int32, (total, rows), 0)
     hit = jnp.zeros((total, rows), f32)
     copies[0].wait()
@@ -105,14 +105,23 @@
     for c in range(width // lanes):
         at = slice(c * lanes, (c + 1) * lanes)
         normed_out[:, at] = (values[:, at] * scale * gain[c : c + 1].astype(f32)).astype(bf16)
-    normed = normed_out[...]
+    rest, far = outs[2], outs[3:]
+    n = rest.shape[0]
+    rest[...] = pick[:n]
+    for out in far:
+        out[...] = jnp.dot(pick[n:], normed_out[...], preferred_element_type=f32).astype(bf16)
+
+
+def spread_body(pick, normed, *refs):
+    sources, copied, outs, sems = refs[:3], refs[3:6], refs[6:-1], refs[-1]
+    copies = fetch(sources, copied, sems)
     at = 0
-    for out in outs[5:]:
+    for out in outs:
         n = out.shape[0]
         part = pick[at : at + n]
-        out[...] = jnp.dot(part, normed, preferred_element_type=f32).astype(bf16)
+        out[...] = jnp.dot(part, normed[...], preferred_element_type=f32).astype(bf16)
         at += n
-    for copy in copies[3:]:
+    for copy in copies:
         copy.wait()
 
 
@@ -286,17 +295,29 @@
     total = sum(sizes.values())
     args = [expert_ids.T, norm_gain.reshape(-1, 128), tokens]
     sh_weights = [shared_gate, shared_up, shared_down]
-    normed, slots, *rest = call(
+    ahead = ["A"] if direct else []
+    later = [k for k in sent_here if k not in ahead]
+    n_later = sum(sizes[k] for k in later)
+    normed, slots, pick, *sends = call(
         functools.partial(route_body, capacity, groups, direct),
         [shape(rows_here, width, bf16), shape(chosen, rows_here, jnp.int32)]
-        + [shape(*w.shape, w.dtype) for w in sh_weights]
-        + [shape(sizes[k], width, bf16) for k in sent_here],
-        args + sh_weights,
+        + [shape(n_later, rows_here, bf16)]
+        + [shape(sizes[k], width, bf16) for k in ahead],
+        args,
         2 * rows_here * width * total,
-        landing(args)[:-1] + [pltpu.SemaphoreType.DMA((6,))],
-        range(6),
-    )
-    sh_weights, sends = rest[:3], rest[3:]
+        landing(args),
+        range(3),
+    )
+    rest = call(
+        spread_body,
+        [shape(*w.shape, w.dtype) for w in sh_weights]
+        + [shape(sizes[k], width, bf16) for k in later],
+        [pick, normed, *sh_weights],
+        2 * rows_here * width * n_later,
+        [pltpu.SemaphoreType.DMA((3,))],
+        range(2, 5),
+    )
+    sh_weights, sends = rest[:3], [*rest[3:], *sends]
     arrived = {k: hop(block, distances[k]) for k, block in zip(sent_here, sends)}
     if direct:
         arrived["B"] = lax.ppermute(arrived["A"], "tp", neighbour)

time: 54.4 us -> 55.6 us (1.022)
  Pallas kernels: 6.63 us -> 7.84 us
    pallas_call x11 -> x12, Pallas kernels: 6.63 us -> 7.84 us  [call(): pl.pallas_call(body, out_shape=outs, in_specs=[hbm if i in far else vmem...]
  transfers between devices with their start and end apart: 17 -> 17, of which waited for: 6 -> 6; matrix products, arithmetic and copies ran while one was open for 0% -> 0% of each run, Pallas kernels for 10% -> 12%
where the time goes in v6:
time: 55.6 us; the launch traced here: 55.2 us
  waiting for transfers between devices  26.5 us (48%)
  starting transfers between devices  20.6 us (37%)
  Pallas kernels  7.84 us (14%)
    ppermute x8, waiting for transfers between devices, hop(): return lax.ppermute(block, ('ep', 'tp'), pairs)  20.6 us
    ppermute x8, starting transfers between devices, hop(): return lax.ppermute(block, ('ep', 'tp'), pairs)  10.1 us
    pallas_call x12, Pallas kernels, call(): pl.pallas_call(body, out_shape=outs, in_specs=[hbm if i in far else vmem...  7.84 us
    ppermute x2, waiting for transfers between devices, local(): sent[k] = lax.ppermute(sent[k], 'tp', neighbour)  5.88 us
    ppermute x2, starting transfers between devices, local(): sent[k] = lax.ppermute(sent[k], 'tp', neighbour)  4.2 us
    ppermute x1, starting transfers between devices, local(): lax.ppermute(send, 'tp', sibling)  2.22 us
    ppermute x1, starting transfers between devices, local(): came = lax.ppermute(send, 'tp', neighbour)  1.53 us
    ppermute x1, starting transfers between devices, local(): arrived['B'] = lax.ppermute(arrived['A'], 'tp', neighbour)  1.5 us
  transfers between devices with their start and end apart: 17, of which 6 were waited for; matrix products, arithmetic and copies ran while one was open for 0% of the time, Pallas kernels for 12%

profile of v6, /device:TPU:0, one launch (start us, length us, event | category | flops | bytes accessed | tf_op | source)
XLA Modules:
  0.0 55.2 jit_solution(11128415199555562965)
XLA Ops:
  0.0 0.5 collective-permute-start.1
  0.5 0.0 collective-permute-start.2
  0.5 0.5 collective-permute-start.3
  1.0 1.5 %shard_map.100 = (bf16[128,2048]{1,0:T(8,128)(2,1)S(1)}, s32[2,128]{1,0:T(2,128)S(1)}, bf16[96,128]{1,0:T(8,128)(2,1)S(1)}, bf16[48,2048]{1,0:T(8,128)(2,1)S(1)}) custom-call(s32[2,128]{1,0:T(2,128)} %bitcast.20, bf16[16,128]{1,0:T(8,128)(2,1)} %bitcast.18, bf16[128,2048]{1,0:T(8,128)(2,1)} %refs_2_.2), custom_call_target="tpu_custom_call" | custom-call | flops 100663296 | bytes 1275904 | tf_op jit(solution)/shard_map/pallas_call | solution.py:25
  2.6 1.5 %shard_map.101 = (bf16[2048,128]{1,0:T(8,128)(2,1)S(1)}, bf16[2048,128]{1,0:T(8,128)(2,1)S(1)}, bf16[128,2048]{1,0:T(8,128)(2,1)S(1)}, bf16[48,2048]{1,0:T(8,128)(2,1)S(1)}, bf16[48,2048]{1,0:T(8,128)(2,1)S(1)}) custom-call(bf16[96,128]{1,0:T(8,128)(2,1)S(1)} %get-tuple-element.34.pick, bf16[128,2048]{1,0:T(8,128)(2,1)S(1)} %get-tuple-element.33.normed.rows, ...), custom_call_target="tpu_custom_call" | custom-call | flops 50331648 | bytes 4087808 | tf_op jit(solution)/shard_map/pallas_call | solution.py:25
  4.1 0.7 %collective-permute-start.8 = (bf16[48,2048]{1,0:T(8,128)(2,1)S(1)}, bf16[48,2048]{1,0:T(8,128)(2,1)S(1)}, u32[]{:S(2)}, u32[]{:S(2)}) collective-permute-start(bf16[48,2048]{1,0:T(8,128)(2,1)S(1)} %get-tuple-element.46), channel_id=1, source_target_pairs={{0,0},{1,5},{2,2},{3,7},{4,4},{5,1},{6,6},{7,3},{8,8},{9,13},{10,1... | collective-permute-start | bytes 589832 | tf_op jit(solution)/shard_map/ppermute | solution.py:284
  4.8 3.6 %collective-permute-start.9 = (bf16[48,2048]{1,0:T(8,128)(2,1)S(1)}, bf16[48,2048]{1,0:T(8,128)(2,1)S(1)}, u32[]{:S(2)}, u32[]{:S(2)}) collective-permute-start(bf16[48,2048]{1,0:T(8,128)(2,1)S(1)} %get-tuple-element.47), channel_id=1, source_target_pairs={{0,12},{1,9},{2,14},{3,11},{4,8},{5,13},{6,10},{7,15},{8,4},{9,1},... | collective-permute-start | bytes 589832 | tf_op jit(solution)/shard_map/ppermute | solution.py:284
  8.3 2.6 %collective-permute-start = (bf16[48,2048]{1,0:T(8,128)(2,1)S(1)}, bf16[48,2048]{1,0:T(8,128)(2,1)S(1)}, u32[]{:S(2)}, u32[]{:S(2)}) collective-permute-start(bf16[48,2048]{1,0:T(8,128)(2,1)S(1)} %get-tuple-element.39), channel_id=1, source_target_pairs={{0,16},{1,29},{2,22},{3,27},{4,20},{5,25},{6,18},{7,31},{8,24},{9,... | collective-permute-start | bytes 589832 | tf_op jit(solution)/shard_map/ppermute | solution.py:284
  10.9 4.1 %collective-permute-done.9.refs_1_ = bf16[48,2048]{1,0:T(8,128)(2,1)S(1)} collective-permute-done((bf16[48,2048]{1,0:T(8,128)(2,1)S(1)}, bf16[48,2048]{1,0:T(8,128)(2,1)S(1)}, u32[]{:S(2)}, u32[]{:S(2)}) %collective-permute-start.9) | collective-permute-done | bytes 196640 | tf_op jit(solution)/shard_map/ppermute | solution.py:284
  15.1 0.7 %shard_map.106 = (bf16[48,2048]{1,0:T(8,128)(2,1)S(1)}, bf16[48,2048]{1,0:T(8,128)(2,1)S(1)}) custom-call(bf16[48,2048]{1,0:T(8,128)(2,1)S(1)} %collective-permute-done.8.refs_0_, bf16[48,2048]{1,0:T(8,128)(2,1)S(1)} %collective-permute-done.9.refs_1_, bf16[2048,128]{1,0:T(8,128)(2,1)S(1)} %bitcast.7, bf16[2048,128]{1,0:T(8,128)(2,1)S(1)} %bitcast.11, ...), custom_call_target="tpu_custom_call" | custom-call | flops 301989888 | bytes 3932160 | tf_op jit(solution)/shard_map/pallas_call | solution.py:25
  15.8 0.7 %collective-permute-start.10 = (bf16[48,2048]{1,0:T(8,128)(2,1)S(1)}, bf16[48,2048]{1,0:T(8,128)(2,1)S(1)}, u32[]{:S(2)}, u32[]{:S(2)}) collective-permute-start(bf16[48,2048]{1,0:T(8,128)(2,1)S(1)} %get-tuple-element.48), channel_id=1, source_target_pairs={{0,0},{1,5},{2,2},{3,7},{4,4},{5,1},{6,6},{7,3},{8,8},{9,13},{10,1... | collective-permute-start | bytes 589832 | tf_op jit(solution)/shard_map/ppermute | solution.py:284
  16.5 1.1 %collective-permute-start.11 = (bf16[48,2048]{1,0:T(8,128)(2,1)S(1)}, bf16[48,2048]{1,0:T(8,128)(2,1)S(1)}, u32[]{:S(2)}, u32[]{:S(2)}) collective-permute-start(bf16[48,2048]{1,0:T(8,128)(2,1)S(1)} %get-tuple-element.49), channel_id=1, source_target_pairs={{0,12},{1,9},{2,14},{3,11},{4,8},{5,13},{6,10},{7,15},{8,4},{9,1},... | collective-permute-start | bytes 589832 | tf_op jit(solution)/shard_map/ppermute | solution.py:284
  17.6 1.5 %collective-permute-start.4 = (bf16[48,2048]{1,0:T(8,128)(2,1)S(1)}, bf16[48,2048]{1,0:T(8,128)(2,1)S(1)}, u32[]{:S(2)}, u32[]{:S(2)}) collective-permute-start(bf16[48,2048]{1,0:T(8,128)(2,1)S(1)} %collective-permute-done.refs_0_), channel_id=1, source_target_pairs={{0,2},{1,3},{2,0},{3,1},{4,6},{5,7},{6,4},{7,5},{8,10},{9,11},{10,... | collective-permute-start | bytes 589832 | tf_op jit(solution)/shard_map/ppermute | solution.py:323
  19.1 1.1 %shard_map.102 = (f32[128,2048]{1,0:T(8,128)S(1)}, bf16[128,192]{1,0:T(8,128)(2,1)S(1)}, bf16[128,96]{1,0:T(8,128)(2,1)S(1)}, bf16[128,192]{1,0:T(8,128)(2,1)S(1)}) custom-call(s32[2,128]{1,0:T(2,128)S(1)} %get-tuple-element.32.slots, bf16[128,2048]{1,0:T(8,128)(2,1)S(1)} %get-tuple-element.33.normed.rows, bf16[2048,128]{1,0:T(8,128)(2,1)S(1)} %get-tuple-element.35.refs_0_, ...), custom_call_target="tpu_custom_call" | custom-call | flops 201326592 | bytes 3270656 | tf_op jit(solution)/shard_map/pallas_call | solution.py:25
  20.2 3.6 %collective-permute-done.11.refs_1_ = bf16[48,2048]{1,0:T(8,128)(2,1)S(1)} collective-permute-done((bf16[48,2048]{1,0:T(8,128)(2,1)S(1)}, bf16[48,2048]{1,0:T(8,128)(2,1)S(1)}, u32[]{:S(2)}, u32[]{:S(2)}) %collective-permute-start.11) | collective-permute-done | bytes 196640 | tf_op jit(solution)/shard_map/ppermute | solution.py:284
  23.8 0.4 shard_map.107
  24.2 2.2 %collective-permute-start.12 = (bf16[128,1024]{1,0:T(8,128)(2,1)S(1)}, bf16[128,1024]{1,0:T(8,128)(2,1)S(1)}, u32[]{:S(2)}, u32[]{:S(2)}) collective-permute-start(bf16[128,1024]{1,0:T(8,128)(2,1)S(1)} %get-tuple-element.51), channel_id=1, source_target_pairs={{0,1},{1,0},{2,3},{3,2},{4,5},{5,4},{6,7},{7,6},{8,9},{9,8},{10,11... | collective-permute-start | bytes 786440 | tf_op jit(solution)/shard_map/ppermute | solution.py:356
  26.4 0.7 %shard_map.103 = (bf16[48,1024]{1,0:T(8,128)(2,1)S(1)}, f32[48,1024]{1,0:T(8,128)S(1)}) custom-call(bf16[48,2048]{1,0:T(8,128)(2,1)S(1)} %collective-permute-done.refs_0_, bf16[2048,128]{1,0:T(8,128)(2,1)S(1)} %bitcast.8, bf16[2048,128]{1,0:T(8,128)(2,1)S(1)} %bitcast.12, bf16[128,2048]{1,0:T(8,128)(2,1)S(1)} %bitcast.16, ...), custom_call_target="tpu_custom_call" | custom-call | flops 150994944 | bytes 3637248 | tf_op jit(solution)/shard_map/pallas_call | solution.py:25
  27.1 3.6 %collective-permute-start.14 = (bf16[48,1024]{1,0:T(8,128)(2,1)S(1)}, bf16[48,1024]{1,0:T(8,128)(2,1)S(1)}, u32[]{:S(2)}, u32[]{:S(2)}) collective-permute-start(bf16[48,1024]{1,0:T(8,128)(2,1)S(1)} %get-tuple-element.55), channel_id=1, source_target_pairs={{0,2},{1,3},{2,0},{3,1},{4,6},{5,7},{6,4},{7,5},{8,10},{9,11},{10,... | collective-permute-start | bytes 294920 | tf_op jit(solution)/shard_map/ppermute | solution.py:366
  30.8 0.7 %shard_map.104 = (bf16[48,1024]{1,0:T(8,128)(2,1)S(1)}, f32[48,1024]{1,0:T(8,128)S(1)}) custom-call(bf16[48,2048]{1,0:T(8,128)(2,1)S(1)} %collective-permute-done.4.refs_0_, bf16[2048,128]{1,0:T(8,128)(2,1)S(1)} %bitcast.9, bf16[2048,128]{1,0:T(8,128)(2,1)S(1)} %bitcast.13, bf16[128,2048]{1,0:T(8,128)(2,1)S(1)} %bitcast.17, ...), custom_call_target="tpu_custom_call" | custom-call | flops 150994944 | bytes 3637248 | tf_op jit(solution)/shard_map/pallas_call | solution.py:25
  31.5 2.2 %collective-permute-done.14.came = bf16[48,1024]{1,0:T(8,128)(2,1)S(1)} collective-permute-done((bf16[48,1024]{1,0:T(8,128)(2,1)S(1)}, bf16[48,1024]{1,0:T(8,128)(2,1)S(1)}, u32[]{:S(2)}, u32[]{:S(2)}) %collective-permute-start.14) | collective-permute-done | bytes 98336 | tf_op jit(solution)/shard_map/ppermute | solution.py:366
  33.8 1.3 %collective-permute-start.15 = (bf16[48,1024]{1,0:T(8,128)(2,1)S(1)}, bf16[48,1024]{1,0:T(8,128)(2,1)S(1)}, u32[]{:S(2)}, u32[]{:S(2)}) collective-permute-start(bf16[48,1024]{1,0:T(8,128)(2,1)S(1)} %shard_map.109), channel_id=1, source_target_pairs={{0,20},{1,25},{2,18},{3,31},{4,16},{5,29},{6,22},{7,27},{8,28},{9,... | collective-permute-start | bytes 294920 | tf_op jit(solution)/shard_map/ppermute | solution.py:284
  35.1 0.1 shard_map.108
  35.1 6.5 %collective-permute-done.15.rows = bf16[48,1024]{1,0:T(8,128)(2,1)S(1)} collective-permute-done((bf16[48,1024]{1,0:T(8,128)(2,1)S(1)}, bf16[48,1024]{1,0:T(8,128)(2,1)S(1)}, u32[]{:S(2)}, u32[]{:S(2)}) %collective-permute-start.15) | collective-permute-done | bytes 98336 | tf_op jit(solution)/shard_map/ppermute | solution.py:284
  41.6 0.2 shard_map.110
  41.8 0.1 collective-permute-start.16
  41.9 0.6 %collective-permute-start.5 = (bf16[48,1024]{1,0:T(8,128)(2,1)S(1)}, bf16[48,1024]{1,0:T(8,128)(2,1)S(1)}, u32[]{:S(2)}, u32[]{:S(2)}) collective-permute-start(bf16[48,1024]{1,0:T(8,128)(2,1)S(1)} %get-tuple-element.41), channel_id=1, source_target_pairs={{0,2},{1,3},{2,0},{3,1},{4,6},{5,7},{6,4},{7,5},{8,10},{9,11},{10,... | collective-permute-start | bytes 294920 | tf_op jit(solution)/shard_map/ppermute | solution.py:366
  42.5 1.5 %collective-permute-start.13 = (bf16[128,512]{1,0:T(8,128)(2,1)S(1)}, bf16[128,512]{1,0:T(8,128)(2,1)S(1)}, u32[]{:S(2)}, u32[]{:S(2)}) collective-permute-start(bf16[128,512]{1,0:T(8,128)(2,1)S(1)} %get-tuple-element.52), channel_id=1, source_target_pairs={{0,2},{1,3},{2,0},{3,1},{4,6},{5,7},{6,4},{7,5},{8,10},{9,11},{10,... | collective-permute-start | bytes 393224 | tf_op jit(solution)/shard_map/ppermute | solution.py:359
  44.0 3.6 %collective-permute-done.5.came = bf16[48,1024]{1,0:T(8,128)(2,1)S(1)} collective-permute-done((bf16[48,1024]{1,0:T(8,128)(2,1)S(1)}, bf16[48,1024]{1,0:T(8,128)(2,1)S(1)}, u32[]{:S(2)}, u32[]{:S(2)}) %collective-permute-start.5) | collective-permute-done | bytes 98336 | tf_op jit(solution)/shard_map/ppermute | solution.py:366
  47.7 0.2 collective-permute-start.6
  47.9 6.5 %collective-permute-done.6.rows = bf16[48,512]{1,0:T(8,128)(2,1)S(1)} collective-permute-done((bf16[48,512]{1,0:T(8,128)(2,1)S(1)}, bf16[48,512]{1,0:T(8,128)(2,1)S(1)}, u32[]{:S(2)}, u32[]{:S(2)}) %collective-permute-start.6) | collective-permute-done | bytes 49184 | tf_op jit(solution)/shard_map/ppermute | solution.py:284
  54.3 0.8 %shard_map.111 = bf16[128,512]{1,0:T(8,128)(2,1)} custom-call(bf16[128,192]{1,0:T(8,128)(2,1)S(1)} %get-tuple-element.38.weights, bf16[48,512]{1,0:T(8,128)(2,1)S(1)} %collective-permute-done.6.rows, bf16[48,512]{1,0:T(8,128)(2,1)S(1)} %collective-permute-done.7.rows2, bf16[128,512]{1,0:T(8,128)(2,1)S(1)} %collective-permute-done.13.came, ...), custom_call_target="tpu_custom_call" | custom-call | flops 25165824 | bytes 933888 | tf_op jit(solution)/shard_map/pallas_call | solution.py:25
  (20 shorter events, 0.1 us)
Async XLA Ops:
  0.0 15.0 %collective-permute-start.1 = (bf16[2048,128]{1,0:T(8,128)(2,1)}, bf16[2048,128]{1,0:T(8,128)(2,1)S(1)}, u32[]{:S(2)}, u32[]{:S(2)}) collective-permute-start(bf16[2048,128]{1,0:T(8,128)(2,1)} %bitcast.6), channel_id=1, source_target_pairs={{0,1},{1,0},{2,3},{3,2},{4,5},{5,4},{6,7},{7,6},{8,9},{9,8},{10,11... | collective-permute-start | bytes 1572872 | tf_op jit(solution)/shard_map/ppermute | solution.py:274
  0.5 14.5 %collective-permute-start.2 = (bf16[2048,128]{1,0:T(8,128)(2,1)}, bf16[2048,128]{1,0:T(8,128)(2,1)S(1)}, u32[]{:S(2)}, u32[]{:S(2)}) collective-permute-start(bf16[2048,128]{1,0:T(8,128)(2,1)} %bitcast.10), channel_id=1, source_target_pairs={{0,1},{1,0},{2,3},{3,2},{4,5},{5,4},{6,7},{7,6},{8,9},{9,8},{10,11... | collective-permute-start | bytes 1572872 | tf_op jit(solution)/shard_map/ppermute | solution.py:274
  0.5 14.5 %collective-permute-start.3 = (bf16[128,2048]{1,0:T(8,128)(2,1)}, bf16[128,2048]{1,0:T(8,128)(2,1)S(1)}, u32[]{:S(2)}, u32[]{:S(2)}) collective-permute-start(bf16[128,2048]{1,0:T(8,128)(2,1)} %bitcast.14), channel_id=1, source_target_pairs={{0,1},{1,0},{2,3},{3,2},{4,5},{5,4},{6,7},{7,6},{8,9},{9,8},{10,11... | collective-permute-start | bytes 1572872 | tf_op jit(solution)/shard_map/ppermute | solution.py:274
  2.5 12.5 %copy-start = (bf16[1,2048,128]{2,1,0:T(8,128)(2,1)S(1)}, bf16[1,2048,128]{2,1,0:T(8,128)(2,1)}, u32[]{:S(2)}) copy-start(bf16[1,2048,128]{2,1,0:T(8,128)(2,1)} %param.14) | copy-start | bytes 1572868
  2.5 12.5 %copy-start.1 = (bf16[1,2048,128]{2,1,0:T(8,128)(2,1)S(1)}, bf16[1,2048,128]{2,1,0:T(8,128)(2,1)}, u32[]{:S(2)}) copy-start(bf16[1,2048,128]{2,1,0:T(8,128)(2,1)} %param.15) | copy-start | bytes 1572868
  2.6 12.5 %copy-start.2 = (bf16[1,128,2048]{2,1,0:T(8,128)(2,1)S(1)}, bf16[1,128,2048]{2,1,0:T(8,128)(2,1)}, u32[]{:S(2)}) copy-start(bf16[1,128,2048]{2,1,0:T(8,128)(2,1)} %param.16) | copy-start | bytes 1572868
  4.1 4.3 %collective-permute-start.8 = (bf16[48,2048]{1,0:T(8,128)(2,1)S(1)}, bf16[48,2048]{1,0:T(8,128)(2,1)S(1)}, u32[]{:S(2)}, u32[]{:S(2)}) collective-permute-start(bf16[48,2048]{1,0:T(8,128)(2,1)S(1)} %get-tuple-element.46), channel_id=1, source_target_pairs={{0,0},{1,5},{2,2},{3,7},{4,4},{5,1},{6,6},{7,3},{8,8},{9,13},{10,1... | collective-permute-start | bytes 589832 | tf_op jit(solution)/shard_map/ppermute | solution.py:284
  4.8 10.3 %collective-permute-start.9 = (bf16[48,2048]{1,0:T(8,128)(2,1)S(1)}, bf16[48,2048]{1,0:T(8,128)(2,1)S(1)}, u32[]{:S(2)}, u32[]{:S(2)}) collective-permute-start(bf16[48,2048]{1,0:T(8,128)(2,1)S(1)} %get-tuple-element.47), channel_id=1, source_target_pairs={{0,12},{1,9},{2,14},{3,11},{4,8},{5,13},{6,10},{7,15},{8,4},{9,1},... | collective-permute-start | bytes 589832 | tf_op jit(solution)/shard_map/ppermute | solution.py:284
  8.3 9.2 %collective-permute-start = (bf16[48,2048]{1,0:T(8,128)(2,1)S(1)}, bf16[48,2048]{1,0:T(8,128)(2,1)S(1)}, u32[]{:S(2)}, u32[]{:S(2)}) collective-permute-start(bf16[48,2048]{1,0:T(8,128)(2,1)S(1)} %get-tuple-element.39), channel_id=1, source_target_pairs={{0,16},{1,29},{2,22},{3,27},{4,20},{5,25},{6,18},{7,31},{8,24},{9,... | collective-permute-start | bytes 589832 | tf_op jit(solution)/shard_map/ppermute | solution.py:284
  15.8 4.4 %collective-permute-start.10 = (bf16[48,2048]{1,0:T(8,128)(2,1)S(1)}, bf16[48,2048]{1,0:T(8,128)(2,1)S(1)}, u32[]{:S(2)}, u32[]{:S(2)}) collective-permute-start(bf16[48,2048]{1,0:T(8,128)(2,1)S(1)} %get-tuple-element.48), channel_id=1, source_target_pairs={{0,0},{1,5},{2,2},{3,7},{4,4},{5,1},{6,6},{7,3},{8,8},{9,13},{10,1... | collective-permute-start | bytes 589832 | tf_op jit(solution)/shard_map/ppermute | solution.py:284
  16.5 7.3 %collective-permute-start.11 = (bf16[48,2048]{1,0:T(8,128)(2,1)S(1)}, bf16[48,2048]{1,0:T(8,128)(2,1)S(1)}, u32[]{:S(2)}, u32[]{:S(2)}) collective-permute-start(bf16[48,2048]{1,0:T(8,128)(2,1)S(1)} %get-tuple-element.49), channel_id=1, source_target_pairs={{0,12},{1,9},{2,14},{3,11},{4,8},{5,13},{6,10},{7,15},{8,4},{9,1},... | collective-permute-start | bytes 589832 | tf_op jit(solution)/shard_map/ppermute | solution.py:284
  17.6 13.2 %collective-permute-start.4 = (bf16[48,2048]{1,0:T(8,128)(2,1)S(1)}, bf16[48,2048]{1,0:T(8,128)(2,1)S(1)}, u32[]{:S(2)}, u32[]{:S(2)}) collective-permute-start(bf16[48,2048]{1,0:T(8,128)(2,1)S(1)} %collective-permute-done.refs_0_), channel_id=1, source_target_pairs={{0,2},{1,3},{2,0},{3,1},{4,6},{5,7},{6,4},{7,5},{8,10},{9,11},{10,... | collective-permute-start | bytes 589832 | tf_op jit(solution)/shard_map/ppermute | solution.py:323
  24.2 10.9 %collective-permute-start.12 = (bf16[128,1024]{1,0:T(8,128)(2,1)S(1)}, bf16[128,1024]{1,0:T(8,128)(2,1)S(1)}, u32[]{:S(2)}, u32[]{:S(2)}) collective-permute-start(bf16[128,1024]{1,0:T(8,128)(2,1)S(1)} %get-tuple-element.51), channel_id=1, source_target_pairs={{0,1},{1,0},{2,3},{3,2},{4,5},{5,4},{6,7},{7,6},{8,9},{9,8},{10,11... | collective-permute-start | bytes 786440 | tf_op jit(solution)/shard_map/ppermute | solution.py:356
  27.1 6.6 %collective-permute-start.14 = (bf16[48,1024]{1,0:T(8,128)(2,1)S(1)}, bf16[48,1024]{1,0:T(8,128)(2,1)S(1)}, u32[]{:S(2)}, u32[]{:S(2)}) collective-permute-start(bf16[48,1024]{1,0:T(8,128)(2,1)S(1)} %get-tuple-element.55), channel_id=1, source_target_pairs={{0,2},{1,3},{2,0},{3,1},{4,6},{5,7},{6,4},{7,5},{8,10},{9,11},{10,... | collective-permute-start | bytes 294920 | tf_op jit(solution)/shard_map/ppermute | solution.py:366
  33.8 7.8 %collective-permute-start.15 = (bf16[48,1024]{1,0:T(8,128)(2,1)S(1)}, bf16[48,1024]{1,0:T(8,128)(2,1)S(1)}, u32[]{:S(2)}, u32[]{:S(2)}) collective-permute-start(bf16[48,1024]{1,0:T(8,128)(2,1)S(1)} %shard_map.109), channel_id=1, source_target_pairs={{0,20},{1,25},{2,18},{3,31},{4,16},{5,29},{6,22},{7,27},{8,28},{9,... | collective-permute-start | bytes 294920 | tf_op jit(solution)/shard_map/ppermute | solution.py:284
  41.8 12.5 %collective-permute-start.16 = (f32[128,512]{1,0:T(8,128)S(1)}, f32[128,512]{1,0:T(8,128)S(1)}, u32[]{:S(2)}, u32[]{:S(2)}) collective-permute-start(f32[128,512]{1,0:T(8,128)S(1)} %get-tuple-element.58), channel_id=1, source_target_pairs={{0,1},{1,0},{2,3},{3,2},{4,5},{5,4},{6,7},{7,6},{8,9},{9,8},{10,11... | collective-permute-start | bytes 786440 | tf_op jit(solution)/shard_map/ppermute | solution.py:377
  41.9 5.7 %collective-permute-start.5 = (bf16[48,1024]{1,0:T(8,128)(2,1)S(1)}, bf16[48,1024]{1,0:T(8,128)(2,1)S(1)}, u32[]{:S(2)}, u32[]{:S(2)}) collective-permute-start(bf16[48,1024]{1,0:T(8,128)(2,1)S(1)} %get-tuple-element.41), channel_id=1, source_target_pairs={{0,2},{1,3},{2,0},{3,1},{4,6},{5,7},{6,4},{7,5},{8,10},{9,11},{10,... | collective-permute-start | bytes 294920 | tf_op jit(solution)/shard_map/ppermute | solution.py:366
  42.5 11.9 %collective-permute-start.13 = (bf16[128,512]{1,0:T(8,128)(2,1)S(1)}, bf16[128,512]{1,0:T(8,128)(2,1)S(1)}, u32[]{:S(2)}, u32[]{:S(2)}) collective-permute-start(bf16[128,512]{1,0:T(8,128)(2,1)S(1)} %get-tuple-element.52), channel_id=1, source_target_pairs={{0,2},{1,3},{2,0},{3,1},{4,6},{5,7},{6,4},{7,5},{8,10},{9,11},{10,... | collective-permute-start | bytes 393224 | tf_op jit(solution)/shard_map/ppermute | solution.py:359
  47.7 6.7 %collective-permute-start.6 = (bf16[48,512]{1,0:T(8,128)(2,1)S(1)}, bf16[48,512]{1,0:T(8,128)(2,1)S(1)}, u32[]{:S(2)}, u32[]{:S(2)}) collective-permute-start(bf16[48,512]{1,0:T(8,128)(2,1)S(1)} %get-tuple-element.42), channel_id=1, source_target_pairs={{0,16},{1,29},{2,22},{3,27},{4,20},{5,25},{6,18},{7,31},{8,24},{9,... | collective-permute-start | bytes 147464 | tf_op jit(solution)/shard_map/ppermute | solution.py:284
  47.9 6.5 %collective-permute-start.7 = (bf16[48,512]{1,0:T(8,128)(2,1)S(1)}, bf16[48,512]{1,0:T(8,128)(2,1)S(1)}, u32[]{:S(2)}, u32[]{:S(2)}) collective-permute-start(bf16[48,512]{1,0:T(8,128)(2,1)S(1)} %get-tuple-element.43), channel_id=1, source_target_pairs={{0,17},{1,28},{2,23},{3,26},{4,21},{5,24},{6,19},{7,30},{8,25},{9,... | collective-permute-start | bytes 147464 | tf_op jit(solution)/shard_map/ppermute | solution.py:284
